TPU v7x, 256 devices: a whole 4x4x8 slice. The times are simulated.
256 devices in a mesh: ep: 64 (over z, x, core), tp: 4 (over y).
Axes of the slice: x: 4, y: 4, z: 8, core: 2. Of those that a mesh axis runs over, the one named last changes fastest.
Arguments:
- mixer_input: bfloat16 [32768, 2048], P('ep'), may hold values from -5.5 to 5.5
- expert_input: bfloat16 [32768, 2048], P('ep'), may hold values from -6 to 6
- gain_mixer: float32 [2048], replicated, may hold values from 0.1 to 1.9
- gain_expert: float32 [2048], replicated, may hold values from 0.1 to 1.9
- query_weight: bfloat16 [2048, 1536], P(None, 'tp')
- key_weight: bfloat16 [2048, 256], P(None, 'tp')
- value_weight: bfloat16 [2048, 256], P(None, 'tp'), may hold values from -0.125 to 0.125
- sink_logits: float32 [24], P('tp'), may hold values from 2 to 6
- output_weight: bfloat16 [1536, 2048], P('tp'), may hold values from -0.75 to 0.75
- expert_choice: int32 [32768, 2], P('ep'), may hold values from 0 to 63, all different within a row; in each aligned block of 128 rows (0 to 127, 128 to 255, ...) at most 8 rows name the same one
- route_weights: float32 [32768, 2], P('ep'), may hold values from 0.2 to 1.2
- expert_gate: bfloat16 [64, 2048, 1024], P('ep', None, 'tp'), may hold values from -0.125 to 0.125
- expert_up: bfloat16 [64, 2048, 1024], P('ep', None, 'tp'), may hold values from -0.125 to 0.125
- expert_down: bfloat16 [64, 1024, 2048], P('ep', 'tp'), may hold values from -0.1875 to 0.1875
- shared_gate: bfloat16 [2048, 512], P(None, 'tp'), may hold values from -0.125 to 0.125
- shared_up: bfloat16 [2048, 512], P(None, 'tp'), may hold values from -0.125 to 0.125
- shared_down: bfloat16 [512, 2048], P('tp'), may hold values from -0.25 to 0.25
Outputs:
- mixer_output: bfloat16 [32768, 2048], P(('ep', 'tp'))
- expert_output: bfloat16 [32768, 2048], P(('ep', 'tp'))
Inputs may be any that keep to these rules, and one draw needn't show every extreme that they name: `expert_choice`: in each aligned block of 128 rows no expert is named by more than 8 rows, and in some block some expert is named by exactly 8 rows; the 2 entries of a row differ.
All inputs are finite; a program needn't handle non-finite values.
Results may differ from a plain program's by a relative error of at most 0.019.
Values may be sent and summed in bfloat16 or wider, within the bound.
No kernel may reach another device: no remote copies, remote signals or barrier semaphores. Data moves between devices by JAX's collectives and lax.ppermute only.
A program may use at most 128 MiB of HBM per device.

v0:
```python
import math

import jax
import jax.numpy as jnp
from jax import lax
from jax.sharding import PartitionSpec as P

HEAD_DIM = 64
WINDOW = 128
SEQS = 1


norm_eps = 1e-06
rope_base = 500000.0


def from_behind(value, axis, steps):
    count = lax.axis_size(axis)
    first, last = (max(0, -steps), min(count, count - steps))
    return lax.ppermute(value, axis, [(source, source + steps) for source in range(first, last)])


def cut_along(shard, dim, count):
    lengths = shard.shape
    pieces = shard.reshape(*lengths[:dim], count, lengths[dim] // count, *lengths[dim + 1 :])
    return jnp.moveaxis(pieces, dim, 0)


def sent_and_summed(shard, axis, dim):
    pieces = cut_along(shard, dim, lax.axis_size(axis))
    arrived = lax.all_to_all(pieces, axis, split_axis=0, concat_axis=0, tiled=True)
    return arrived.astype(jnp.float32).sum(axis=0)


def rounded(value):
    return lax.optimization_barrier(value.astype(jnp.bfloat16)).astype(jnp.float32)


def rms_scale(matrix, scaling):
    widened = matrix.astype(jnp.float32)
    scaled = widened * lax.rsqrt(jnp.mean(widened * widened, axis=-1, keepdims=True) + norm_eps)
    return (scaled * scaling).astype(jnp.bfloat16)


def frequencies(head_size):
    half_steps = jnp.arange(head_size // 2, dtype=jnp.float32)
    return rope_base ** (-(2.0 * half_steps) / head_size)


def rotate(heads, angles):
    middle = heads.shape[-1] // 2
    widened = heads.astype(jnp.float32)
    cosine = jnp.cos(angles)[:, None, :]
    sine_val = jnp.sin(angles)[:, None, :]
    leading = widened[..., :middle]
    trailing = widened[..., middle:]
    turned = jnp.concatenate(
        [leading * cosine - trailing * sine_val, trailing * cosine + leading * sine_val], axis=-1
    )
    return turned.astype(jnp.bfloat16)


def attend(
    query_heads, key_heads, value_heads, prior_keys, prior_values, first_position, sink_logits
):
    window = prior_keys.shape[0]
    total_rows, kv_count, head_size = key_heads.shape
    group_size = query_heads.shape[1] // kv_count
    blocks = total_rows // window

    def banded(earlier, current):
        joined = jnp.concatenate([earlier, current], axis=0).reshape(
            blocks + 1, window, kv_count, head_size
        )
        return jnp.concatenate([joined[:-1], joined[1:]], axis=1)

    band_keys = banded(prior_keys, key_heads)
    band_values = banded(prior_values, value_heads)
    query_blocks = query_heads.reshape(blocks, window, kv_count, group_size, head_size)
    scores = jnp.einsum(
        "nqhgd,nkhd->nhgqk", query_blocks, band_keys, preferred_element_type=jnp.float32
    ) / math.sqrt(head_size)
    query_index = jnp.arange(window, dtype=jnp.int32)[:, None]
    key_index = jnp.arange(2 * window, dtype=jnp.int32)[None, :]
    distance = query_index + window - key_index
    block_start = first_position + jnp.arange(blocks, dtype=jnp.int32)[:, None, None] * window
    allowed = (distance >= 0) & (distance < window) & (block_start - window + key_index >= 0)
    scores = jnp.where(allowed[:, None, None, :, :], scores, -jnp.inf)
    sink_grid = sink_logits.reshape(kv_count, group_size)[None, :, :, None, None]
    row_peak = jnp.maximum(jnp.max(scores, axis=-1, keepdims=True), sink_grid)
    shifted_exp = jnp.exp(scores - row_peak)
    denominator = jnp.sum(shifted_exp, axis=-1, keepdims=True) + jnp.exp(sink_grid - row_peak)
    probs = (shifted_exp / denominator).astype(jnp.bfloat16)
    attended = jnp.einsum(
        "nhgqk,nkhd->nqhgd", probs, band_values, preferred_element_type=jnp.float32
    )
    return attended.astype(jnp.bfloat16).reshape(total_rows, kv_count * group_size * head_size)


def local(
    mixer_input,
    expert_input,
    gain_mixer,
    gain_expert,
    query_weight,
    key_weight,
    value_weight,
    sink_logits,
    output_weight,
    expert_choice,
    route_weights,
    expert_gate,
    expert_up,
    expert_down,
    shared_gate,
    shared_up,
    shared_down,
):
    tp_count = lax.axis_size("tp")
    ep_count = lax.axis_size("ep")
    tp_rank = lax.axis_index("tp")
    group_rows, model_width = mixer_input.shape
    normed = rms_scale(mixer_input, gain_mixer)
    queries = jnp.dot(normed, query_weight, preferred_element_type=jnp.float32).astype(jnp.bfloat16)
    key_rows = jnp.dot(normed, key_weight, preferred_element_type=jnp.float32).astype(jnp.bfloat16)
    value_rows = jnp.dot(normed, value_weight, preferred_element_type=jnp.float32).astype(
        jnp.bfloat16
    )
    first_position = lax.axis_index("ep") % (ep_count // SEQS) * group_rows
    positions = (first_position + jnp.arange(group_rows, dtype=jnp.int32)).astype(jnp.float32)
    angles = positions[:, None] * frequencies(HEAD_DIM)[None, :]
    rot_queries = rotate(queries.reshape(group_rows, -1, HEAD_DIM), angles)
    rot_keys = rotate(key_rows.reshape(group_rows, -1, HEAD_DIM), angles)
    key_width = key_rows.shape[1]
    tail_start = group_rows - WINDOW
    tail_pair = jnp.concatenate(
        [rot_keys.reshape(group_rows, key_width)[tail_start:], value_rows[tail_start:]], axis=1
    )
    earlier_pair = from_behind(tail_pair, "ep", 1)
    prior_keys = earlier_pair[:, :key_width].reshape(WINDOW, -1, HEAD_DIM)
    prior_values = earlier_pair[:, key_width:].reshape(WINDOW, -1, HEAD_DIM)
    attended = attend(
        rot_queries,
        rot_keys,
        value_rows.reshape(group_rows, -1, HEAD_DIM),
        prior_keys,
        prior_values,
        first_position,
        sink_logits,
    )
    picked = attended
    mixer_output = lax.psum_scatter(
        rounded(jnp.dot(picked, output_weight, preferred_element_type=jnp.float32)).astype(
            jnp.bfloat16
        ),
        "tp",
        scatter_dimension=0,
        tiled=True,
    )
    normed_rows = rms_scale(expert_input, gain_expert)
    group_tokens = normed_rows.shape[0]
    own_tokens = group_tokens // tp_count
    top_count = expert_choice.shape[1]
    local_experts = expert_gate.shape[0]
    experts_all = local_experts * ep_count
    capacity = 2 * own_tokens * top_count // experts_all
    assigned = own_tokens * top_count
    picked_experts = expert_choice.reshape(tp_count, assigned)
    onehot = (
        picked_experts[:, :, None] == jnp.arange(experts_all, dtype=jnp.int32)[None, None, :]
    ).astype(jnp.int32)
    slot_ranks = jnp.sum(jnp.cumsum(onehot, axis=1) * onehot, axis=-1) - 1
    padded_rows = jnp.concatenate([normed_rows, jnp.zeros((1, model_width), jnp.bfloat16)], axis=0)

    def own_slot_index():
        own_experts = lax.dynamic_index_in_dim(picked_experts, tp_rank, 0, keepdims=False)
        own_ranks = lax.dynamic_index_in_dim(slot_ranks, tp_rank, 0, keepdims=False)
        return own_experts * capacity + own_ranks

    own_owner = tp_rank * own_tokens + jnp.arange(assigned, dtype=jnp.int32) // top_count
    slot_table = (
        jnp.full((experts_all * capacity,), group_tokens, jnp.int32)
        .at[own_slot_index()]
        .set(own_owner)
    )
    outgoing = padded_rows[slot_table].reshape(experts_all, 1, capacity, model_width)
    arrived = lax.all_gather(
        lax.all_to_all(outgoing, "ep", split_axis=0, concat_axis=0, tiled=True),
        "tp",
        axis=1,
        tiled=True,
    )
    sources = arrived.shape[0] // local_experts
    shaped = arrived.reshape(
        sources, local_experts, arrived.shape[1], arrived.shape[2], arrived.shape[3]
    )
    gate_values = jnp.einsum(
        "iejcd,edf->iejcf", shaped, expert_gate, preferred_element_type=jnp.float32
    )
    up_values = jnp.einsum(
        "iejcd,edf->iejcf", shaped, expert_up, preferred_element_type=jnp.float32
    )
    hidden = (jax.nn.silu(gate_values) * up_values).astype(jnp.bfloat16)
    result = jnp.einsum("iejcf,efd->iejcd", hidden, expert_down, preferred_element_type=jnp.float32)
    partials = result.astype(jnp.bfloat16).reshape(arrived.shape)
    summed = sent_and_summed(partials.astype(jnp.float32).astype(jnp.bfloat16), "tp", 1)
    returned = (
        lax.all_to_all(summed.astype(jnp.bfloat16), "ep", split_axis=0, concat_axis=0, tiled=True)
        .astype(summed.dtype)
        .reshape(-1, model_width)
    )
    own_weights = lax.dynamic_slice_in_dim(route_weights, tp_rank * own_tokens, own_tokens, 0)
    gathered = returned[own_slot_index().reshape(own_tokens, top_count)]
    routed = jnp.sum(gathered * own_weights[:, :, None], axis=1)
    picked = normed_rows
    gate_values = jnp.dot(picked, shared_gate, preferred_element_type=jnp.float32)
    up_values = jnp.dot(picked, shared_up, preferred_element_type=jnp.float32)
    hidden = (jax.nn.silu(gate_values) * up_values).astype(jnp.bfloat16)
    shared_part = lax.psum_scatter(
        rounded(jnp.dot(hidden, shared_down, preferred_element_type=jnp.float32)).astype(
            jnp.bfloat16
        ),
        "tp",
        scatter_dimension=0,
        tiled=True,
    ).astype(jnp.float32)
    expert_output = (routed + shared_part).astype(jnp.bfloat16)
    return (mixer_output, expert_output)


def solution(mesh):
    placed = (
        P("ep", None),
        P("ep", None),
        P(),
        P(),
        P(None, "tp"),
        P(None, "tp"),
        P(None, "tp"),
        P("tp"),
        P("tp", None),
        P("ep", None),
        P("ep", None),
        P("ep", None, "tp"),
        P("ep", None, "tp"),
        P("ep", "tp", None),
        P(None, "tp"),
        P(None, "tp"),
        P("tp", None),
    )
    return jax.shard_map(
        local,
        mesh=mesh,
        in_specs=placed,
        out_specs=(P(("ep", "tp"), None), P(("ep", "tp"), None)),
        check_vma=False,
    )
```

profile of v0, /device:TPU:2, one launch (start us, length us, event | category | flops | bytes accessed | tf_op | source)
XLA Modules:
  0.0 415.3 jit_solution(7231487003897511812)
XLA Ops:
  7.2 0.0 copy-start
  7.2 0.0 all-gather.2.cloned.1.call-start
  7.2 0.9 copy.50
  8.2 0.2 reshape.445
  8.4 0.2 eq.28
  8.5 2.1 fusion.3
  10.7 2.4 reduce-window.6
  13.1 0.1 slice.78
  13.2 0.1 copy.52
  13.4 0.2 fusion.38
  13.5 0.5 broadcast.319
  14.0 0.7 fusion.83
  14.7 1.4 scatter_custom_fusion
  16.1 2.1 fusion.5
  18.3 1.4 copy-done.1
  19.7 1.5 concatenate.64
  21.2 7.1 %gather_fusion = bf16[512,2048]{1,0:T(8,128)(2,1)} fusion(bf16[513,2048]{1,0:T(8,128)(2,1)} %concatenate.64, s32[1024]{0:T(1024)S(1)} %pad_clamp_fusion.1), kind=kCustom, calls=%fused_computation | custom fusion | bytes 4196352 | tf_op jit(solution)/shard_map/gather | solution.py:186
  28.3 63.5 %all_to_all.15 = bf16[64,1,8,2048]{3,2,1,0:T(8,128)(2,1)} all-to-all(bf16[64,1,8,2048]{3,2,1,0:T(8,128)(2,1)} %bitcast.203), channel_id=1, replica_groups=mesh['ep'=64,'tp'=4] {'ep'}, dimensions={0} | all-to-all | bytes 4194304 | tf_op jit(solution)/shard_map/all_to_all | solution.py:188
  91.8 0.0 all-gather.2.cloned.1.call-update
  91.8 82.2 %all-gather.2.cloned.1.call-done = bf16[64,4,8,2048]{3,2,1,0:T(8,128)(2,1)} async-done(((bf16[64,1,8,2048]{3,2,1,0:T(8,128)(2,1)}), bf16[64,4,8,2048]{3,2,1,0:T(8,128)(2,1)}) %all-gather.2.cloned.1.call-update) | async-done | bytes 8388624 | tf_op jit(solution)/shard_map/all_gather | solution.py:187
  174.0 7.1 %fusion.27 = f32[64,4,8,256]{3,2,1,0:T(8,128)} fusion(bf16[64,4,8,2048]{3,2,1,0:T(8,128)(2,1)} %all-gather.2.cloned.1.call-done, bf16[1,2048,256]{2,1,0:T(8,128)(2,1)S(1)} %copy-done.10), kind=kOutput, calls=%fused_computation.45 | convolution fusion | flops 2147483648 | bytes 11534336 | tf_op jit(solution)/shard_map/iejcd,edf->iejcf/dot_general | solution.py:197
  181.1 13.7 %convert_bitcast_fusion = bf16[4,64,1,8,2048]{4,3,0,1,2:T(8,128)(2,1)} fusion(bf16[1,256,2048]{2,1,0:T(8,128)(2,1)} %param.30, bf16[64,4,8,2048]{3,2,1,0:T(8,128)(2,1)} %all-gather.2.cloned.1.call-done, f32[64,4,8,256]{3,2,1,0:T(8,128)} %fusion.27, bf16[1,2048,256]{2,1,0:T(8,128)(2,1)} %param.29), kind=kOutput, calls=%fused_computation.3 | convolution fusion | flops 4302307328 | bytes 20971520 | tf_op jit(solution)/shard_map/iejcf,efd->iejcd/dot_general | solution.py:204
  194.8 8.3 %copy.55 = bf16[4,64,1,8,2048]{4,3,1,2,0:T(8,128)(2,1)} copy(bf16[4,64,1,8,2048]{4,3,0,1,2:T(8,128)(2,1)} %convert_bitcast_fusion) | data formatting | bytes 16777216 | tf_op jit(solution)/shard_map/transpose | solution.py:26
  203.1 5.7 %all-to-all-start.1 = ((bf16[4,64,1,8,2048]{4,3,1,2,0:T(8,128)(2,1)}), bf16[4,64,1,8,2048]{4,3,1,2,0:T(8,128)(2,1)}, u32[]{:S(2)}, u32[]{:S(2)}) async-start(bf16[4,64,1,8,2048]{4,3,1,2,0:T(8,128)(2,1)} %copy.55), calls=%async_computation.2 | async-start | bytes 16777216 | tf_op jit(solution)/shard_map/all_to_all | solution.py:31
  208.8 0.0 reduce-scatter.5.cloned.1.call-start
  208.8 2.1 fusion
  211.0 2.6 convolution_convert_fusion.3
  213.6 0.8 fusion.24
  214.5 0.3 fusion.62
  214.8 2.1 collective-permute-start
  217.0 0.7 fusion.85
  217.7 5.3 %convolution_convert_fusion = bf16[512,2048]{1,0:T(8,128)(2,1)} fusion(bf16[128,2048]{1,0:T(8,128)(2,1)S(1)} %copy-done.6, bf16[512,2048]{1,0:T(8,128)(2,1)} %copy-done.1, bf16[2048,128]{1,0:T(8,128)(2,1)S(1)} %copy-done.7, f32[512,128]{1,0:T(8,128)S(1)} %fusion.85), kind=kOutput, calls=%fused_computation.17 | convolution fusion | flops 538312704 | bytes 5505024 | tf_op jit(solution)/shard_map/dot_general | solution.py:220
  223.0 0.0 reduce-scatter.5.cloned.1.call-update
  223.0 3.2 convolution_convert_fusion.2
  226.2 0.1 convert.27
  226.3 0.1 add_compare_fusion
  226.4 0.3 multiply_cosine_fusion
  226.7 0.2 broadcast_and_fusion
  227.0 0.1 fusion.45
  227.1 0.1 copy_bitcast_fusion
  227.3 2.3 fusion.7
  229.6 0.1 broadcast_maximum_fusion
  229.7 89.8 %all-to-all-done.1 = bf16[4,64,1,8,2048]{4,3,1,2,0:T(8,128)(2,1)} async-done(((bf16[4,64,1,8,2048]{4,3,1,2,0:T(8,128)(2,1)}), bf16[4,64,1,8,2048]{4,3,1,2,0:T(8,128)(2,1)}, u32[]{:S(2)}, u32[]{:S(2)}) %all-to-all-start.1) | async-done | bytes 8388640 | tf_op jit(solution)/shard_map/all_to_all | solution.py:31
  319.5 7.3 %reduce_sum.63 = bf16[64,8,2048]{2,1,0:T(8,128)(2,1)} reduce(bf16[4,64,1,8,2048]{4,3,1,2,0:T(8,128)(2,1)} %all-to-all-done.1, bf16[]{:T(256)} %constant.96.clone.1), dimensions={0,2}, to_apply=%region_9.10 | reduce | flops 3145728 | bytes 10485762 | tf_op jit(solution)/shard_map/reduce_sum | solution.py:32
  326.8 10.7 %all-to-all-start.2 = ((bf16[64,1,8,2048]{3,2,1,0:T(8,128)(2,1)}), bf16[64,1,8,2048]{3,2,1,0:T(8,128)(2,1)}, u32[]{:S(2)}, u32[]{:S(2)}) async-start(bf16[64,1,8,2048]{3,2,1,0:T(8,128)(2,1)} %bitcast.204), calls=%async_computation.3 | async-start | bytes 4194304 | tf_op jit(solution)/shard_map/all_to_all | solution.py:208
  337.5 0.3 reduce-scatter.3.cloned.1.call-start
  337.8 2.7 fusion.6
  340.5 0.1 exponential_add_fusion
  340.6 0.0 copy-done.3
  340.7 1.0 fusion.19
  341.6 0.3 copy.49
  341.9 2.6 convolution_convert_fusion.1
  344.6 0.0 reduce-scatter.3.cloned.1.call-update
  344.6 0.7 constant_dynamic-slice_fusion
  345.3 0.1 copy.56
  345.4 0.1 add.207
  345.5 0.1 reshape.469
  345.7 43.0 %all-to-all-done.2 = bf16[64,1,8,2048]{3,2,1,0:T(8,128)(2,1)} async-done(((bf16[64,1,8,2048]{3,2,1,0:T(8,128)(2,1)}), bf16[64,1,8,2048]{3,2,1,0:T(8,128)(2,1)}, u32[]{:S(2)}, u32[]{:S(2)}) %all-to-all-start.2) | async-done | bytes 2097184 | tf_op jit(solution)/shard_map/all_to_all | solution.py:208
  388.7 4.0 bitcast_convert_fusion
  392.7 5.8 %gather_fusion.1 = f32[256,2048]{1,0:T(8,128)} fusion(f32[512,2048]{1,0:T(8,128)} %bitcast_convert_fusion, s32[1024]{0:T(1024)S(1)} %pad_clamp_fusion), kind=kCustom, calls=%fused_computation.1 | custom fusion | bytes 4195328 | tf_op jit(solution)/shard_map/gather | solution.py:213
  398.5 3.5 reshape.468
  402.0 4.7 %multiply_reduce_fusion = f32[128,2048]{1,0:T(8,128)S(1)} fusion(f32[128,2,2048]{2,1,0:T(2,128)} %reshape.468, f32[128,2]{1,0:T(8,128)S(1)} %copy.56), kind=kLoop, calls=%fused_computation.29 | loop fusion | flops 786432 | bytes 3146752 | tf_op jit(solution)/shard_map/reduce_sum | solution.py:214
  406.8 0.0 reduce-scatter.5.cloned.1.call-done
  406.8 1.9 add_convert_fusion
  (54 shorter events, 0.3 us)
Async XLA Ops:
  7.2 334.8 %copy-start = (bf16[384,2048]{1,0:T(8,128)(2,1)S(1)}, bf16[384,2048]{1,0:T(8,128)(2,1)}, u32[]{:S(2)}) copy-start(bf16[384,2048]{1,0:T(8,128)(2,1)} %param.25) | copy-start | bytes 4718596
  7.2 166.8 %all-gather.2.cloned.1.call-start = ((), (), s32[]{:S(2)}) async-start(), calls=%async_computation.6 | async-start | bytes 10485760 | tf_op jit(solution)/shard_map/all_gather | solution.py:187
  8.3 7.8 %copy-start.8 = (f32[2048]{0:T(1024)S(1)}, f32[2048]{0:T(1024)}, u32[]{:S(2)}) copy-start(f32[2048]{0:T(1024)} %param.20) | copy-start | bytes 24580
  18.3 1.4 copy-start.1
  28.3 145.7 %copy-start.10 = (bf16[1,2048,256]{2,1,0:T(8,128)(2,1)S(1)}, bf16[1,2048,256]{2,1,0:T(8,128)(2,1)}, u32[]{:S(2)}) copy-start(bf16[1,2048,256]{2,1,0:T(8,128)(2,1)} %param.28) | copy-start | bytes 3145732
  203.1 116.4 %all-to-all-start.1 = ((bf16[4,64,1,8,2048]{4,3,1,2,0:T(8,128)(2,1)}), bf16[4,64,1,8,2048]{4,3,1,2,0:T(8,128)(2,1)}, u32[]{:S(2)}, u32[]{:S(2)}) async-start(bf16[4,64,1,8,2048]{4,3,1,2,0:T(8,128)(2,1)} %copy.55), calls=%async_computation.2 | async-start | bytes 16777216 | tf_op jit(solution)/shard_map/all_to_all | solution.py:31
  208.7 2.2 copy-start.11
  208.7 2.2 copy-start.13
  208.8 198.0 %reduce-scatter.5.cloned.1.call-start = ((), (), s32[]{:S(2)}) async-start(), calls=%async_computation.7 | async-start | bytes 2621440 | tf_op jit(solution)/shard_map/reduce_scatter | solution.py:219
  210.9 2.7 copy-start.4
  210.9 2.7 copy-start.12
  213.6 3.4 copy-start.2
  213.6 3.4 copy-start.5
  214.4 3.3 copy-start.6
  214.4 3.3 copy-start.7
  214.8 12.4 %collective-permute-start = (bf16[128,128]{0,1:T(8,128)(2,1)S(1)}, bf16[128,128]{0,1:T(8,128)(2,1)S(1)}, u32[]{:S(2)}, u32[]{:S(2)}) collective-permute-start(bf16[128,128]{0,1:T(8,128)(2,1)S(1)} %pad_maximum_fusion.3), channel_id=1, source_target_pairs={{0,4},{4,8},{8,12},{12,16},{16,20},{20,24},{24,28},{28,32},{32,36}... | collective-permute-start | bytes 98312 | tf_op jit(solution)/shard_map/ppermute | solution.py:20
  227.3 2.3 copy-start.9
  326.8 61.9 %all-to-all-start.2 = ((bf16[64,1,8,2048]{3,2,1,0:T(8,128)(2,1)}), bf16[64,1,8,2048]{3,2,1,0:T(8,128)(2,1)}, u32[]{:S(2)}, u32[]{:S(2)}) async-start(bf16[64,1,8,2048]{3,2,1,0:T(8,128)(2,1)} %bitcast.204), calls=%async_computation.3 | async-start | bytes 4194304 | tf_op jit(solution)/shard_map/all_to_all | solution.py:208
  337.5 71.2 %reduce-scatter.3.cloned.1.call-start = ((), (), s32[]{:S(2)}) async-start(), calls=%async_computation.5 | async-start | bytes 2621440 | tf_op jit(solution)/shard_map/reduce_scatter | solution.py:152
  337.8 2.8 copy-start.3
Sparse Core Ops, SparseCore 0:
  91.9 81.9 all-gather.1
  223.1 51.7 reduce-scatter.4
  344.7 31.4 reduce-scatter.2
where the time goes:
time: 416 us; the launch traced here: 415 us
  waiting for transfers between devices  215 us (52%)
  blocking collectives  63.5 us (15%)
  matrix products  39.2 us (9%)
  local copies, waits for them, and re-layouts  32.7 us (8%)
  other arithmetic  31.7 us (8%)
  starting transfers between devices  18.9 us (5%)
  between operations  14.3 us (3%)
    all_to_all x1, waiting for transfers between devices, sent_and_summed(): lax.all_to_all(pieces, axis, split_axis=0, concat_axis=0, tiled=True)  89.8 us
    all_gather x1, waiting for transfers between devices, local(): lax.all_gather(lax.all_to_all(outgoing, 'ep', split_axis=0, concat_axis=0...  82.2 us
    all_to_all x1, blocking collectives, local(): lax.all_to_all(outgoing, 'ep', split_axis=0, concat_axis=0, tiled=True)  63.5 us
    all_to_all x1, waiting for transfers between devices, local(): lax.all_to_all(summed.astype(jnp.bfloat16), 'ep', split_axis=0, concat_ax...  43 us
    dot_general x1, matrix products, local(): jnp.einsum('iejcf,efd->iejcd', hidden, expert_down, preferred_element_typ...  13.7 us
    all_to_all x1, starting transfers between devices, local(): lax.all_to_all(summed.astype(jnp.bfloat16), 'ep', split_axis=0, concat_ax...  10.7 us
    gather x2, local copies, waits for them, and re-layouts, local(): gathered = returned[own_slot_index().reshape(own_tokens, top_count)]  9.32 us
  transfers between devices with their start and end apart: 6, of which 3 were waited for; matrix products, arithmetic and copies ran while one was open for 13% of the time, Pallas kernels for 0%

commit v1 on v0

--- a/solution.py
+++ b/solution.py
@@ -3,11 +3,14 @@
 import jax
 import jax.numpy as jnp
 from jax import lax
+from jax.experimental import pallas as pl
+from jax.experimental.pallas import tpu as pltpu
 from jax.sharding import PartitionSpec as P
 
 HEAD_DIM = 64
 WINDOW = 128
 SEQS = 1
+CHUNKS = 2
 
 
 norm_eps = 1e-06
@@ -18,22 +21,6 @@
     count = lax.axis_size(axis)
     first, last = (max(0, -steps), min(count, count - steps))
     return lax.ppermute(value, axis, [(source, source + steps) for source in range(first, last)])
-
-
-def cut_along(shard, dim, count):
-    lengths = shard.shape
-    pieces = shard.reshape(*lengths[:dim], count, lengths[dim] // count, *lengths[dim + 1 :])
-    return jnp.moveaxis(pieces, dim, 0)
-
-
-def sent_and_summed(shard, axis, dim):
-    pieces = cut_along(shard, dim, lax.axis_size(axis))
-    arrived = lax.all_to_all(pieces, axis, split_axis=0, concat_axis=0, tiled=True)
-    return arrived.astype(jnp.float32).sum(axis=0)
-
-
-def rounded(value):
-    return lax.optimization_barrier(value.astype(jnp.bfloat16)).astype(jnp.float32)
 
 
 def rms_scale(matrix, scaling):
@@ -95,6 +82,128 @@
         "nhgqk,nkhd->nqhgd", probs, band_values, preferred_element_type=jnp.float32
     )
     return attended.astype(jnp.bfloat16).reshape(total_rows, kv_count * group_size * head_size)
+
+
+def dispatch_kernel(capacity, experts):
+    def body(rank_ref, rows_ref, gain_ref, choice_ref, out_ref, pick_ref):
+        rows = rows_ref[...].astype(jnp.float32)
+        tokens = rows.shape[0]
+        slots = experts * capacity
+        scale = lax.rsqrt(jnp.mean(rows * rows, axis=-1, keepdims=True) + norm_eps)
+        normed = (rows * scale * gain_ref[...]).astype(jnp.bfloat16)
+        first = choice_ref[:, 0:1]
+        second = choice_ref[:, 1:2]
+        expert = lax.broadcasted_iota(jnp.int32, (tokens, experts), 1)
+        named = jnp.where((first == expert) | (second == expert), 1.0, 0.0).astype(jnp.bfloat16)
+        row = lax.broadcasted_iota(jnp.int32, (tokens, tokens), 0)
+        col = lax.broadcasted_iota(jnp.int32, (tokens, tokens), 1)
+        earlier = jnp.where(row > col, 1.0, 0.0).astype(jnp.bfloat16)
+        ranks = jnp.dot(earlier, named, preferred_element_type=jnp.float32)
+        spread_e = lax.broadcasted_iota(jnp.int32, (experts, slots), 0)
+        spread_s = lax.broadcasted_iota(jnp.int32, (experts, slots), 1)
+        spread = jnp.where(spread_s // capacity == spread_e, 1.0, 0.0).astype(jnp.bfloat16)
+        slot_rank = jnp.dot(ranks.astype(jnp.bfloat16), spread, preferred_element_type=jnp.float32)
+        slot = lax.broadcasted_iota(jnp.int32, (tokens, slots), 1)
+        fits = slot_rank.astype(jnp.int32) == slot % capacity
+        owner = slot // capacity
+        pick_first = jnp.where((owner == first) & fits, 1.0, 0.0).astype(jnp.bfloat16)
+        pick_second = jnp.where((owner == second) & fits, 1.0, 0.0).astype(jnp.bfloat16)
+        pick_ref[0] = pick_first
+        pick_ref[1] = pick_second
+        out_ref[...] = lax.dot_general(
+            pick_first + pick_second,
+            normed,
+            (((0,), (0,)), ((), ())),
+            preferred_element_type=jnp.float32,
+        ).astype(jnp.bfloat16)
+
+    return body
+
+
+def dispatched(rank, rows, gain, choice, tokens, capacity, experts):
+    width = rows.shape[1]
+    slots = experts * capacity
+    return pl.pallas_call(
+        dispatch_kernel(capacity, experts),
+        grid_spec=pltpu.PrefetchScalarGridSpec(
+            num_scalar_prefetch=1,
+            grid=(1,),
+            in_specs=[
+                pl.BlockSpec((tokens, width), lambda i, r: (r[0], 0)),
+                pl.BlockSpec((1, width), lambda i, r: (0, 0)),
+                pl.BlockSpec((tokens, 2), lambda i, r: (r[0], 0)),
+            ],
+            out_specs=[
+                pl.BlockSpec((slots, width), lambda i, r: (0, 0)),
+                pl.BlockSpec((2, tokens, slots), lambda i, r: (0, 0, 0)),
+            ],
+        ),
+        out_shape=[
+            jax.ShapeDtypeStruct((slots, width), jnp.bfloat16),
+            jax.ShapeDtypeStruct((2, tokens, slots), jnp.bfloat16),
+        ],
+        name="dispatch",
+    )(rank, rows, gain, choice)
+
+
+def hidden_body(rows_ref, gate_ref, up_ref, out_ref):
+    gate = jnp.dot(rows_ref[...], gate_ref[0], preferred_element_type=jnp.float32)
+    up = jnp.dot(rows_ref[...], up_ref[0], preferred_element_type=jnp.float32)
+    out_ref[...] = (gate / (1.0 + jnp.exp(-gate)) * up).astype(jnp.bfloat16)
+
+
+def expert_hidden(rows, gate, up):
+    slots, width = rows.shape
+    parts, _, units = gate.shape
+    return pl.pallas_call(
+        hidden_body,
+        grid=(parts,),
+        in_specs=[
+            pl.BlockSpec((slots, width), lambda i: (0, 0)),
+            pl.BlockSpec((1, width, units), lambda i: (i, 0, 0)),
+            pl.BlockSpec((1, width, units), lambda i: (i, 0, 0)),
+        ],
+        out_specs=pl.BlockSpec((slots, units), lambda i: (0, i)),
+        out_shape=jax.ShapeDtypeStruct((slots, parts * units), jnp.bfloat16),
+        name="hidden",
+    )(rows, gate, up)
+
+
+def combine_body(rank_ref, pick_ref, weight_ref, shared_ref, *rest):
+    parts = rest[:-1]
+    out_ref = rest[-1]
+    first = weight_ref[:, 0:1]
+    second = weight_ref[:, 1:2]
+    at = 0
+    for part in parts:
+        returned = part[...]
+        span = returned.shape[1]
+        total = first * jnp.dot(pick_ref[0], returned, preferred_element_type=jnp.float32)
+        total = total + second * jnp.dot(pick_ref[1], returned, preferred_element_type=jnp.float32)
+        total = total + shared_ref[:, at : at + span].astype(jnp.float32)
+        out_ref[:, at : at + span] = total.astype(jnp.bfloat16)
+        at += span
+
+
+def combined(rank, pick, weights, shared, parts):
+    tokens, width = shared.shape
+    whole = lambda shape: pl.BlockSpec(shape, lambda i, r: (0,) * len(shape))
+    return pl.pallas_call(
+        combine_body,
+        grid_spec=pltpu.PrefetchScalarGridSpec(
+            num_scalar_prefetch=1,
+            grid=(1,),
+            in_specs=[
+                whole(pick.shape),
+                pl.BlockSpec((tokens, 2), lambda i, r: (r[0], 0)),
+                whole(shared.shape),
+                *[whole(part.shape) for part in parts],
+            ],
+            out_specs=whole((tokens, width)),
+        ),
+        out_shape=jax.ShapeDtypeStruct((tokens, width), jnp.bfloat16),
+        name="combine",
+    )(rank, pick, weights, shared, *parts)
 
 
 def local(
@@ -119,7 +228,33 @@
     tp_count = lax.axis_size("tp")
     ep_count = lax.axis_size("ep")
     tp_rank = lax.axis_index("tp")
+    rank = tp_rank.astype(jnp.int32).reshape(1)
     group_rows, model_width = mixer_input.shape
+    group_tokens = expert_input.shape[0]
+    own_tokens = group_tokens // tp_count
+    top_count = expert_choice.shape[1]
+    experts_all = ep_count
+    capacity = 2 * own_tokens * top_count // experts_all
+
+    gate_all = lax.all_gather(expert_gate[0], "tp", axis=0)
+    up_all = lax.all_gather(expert_up[0], "tp", axis=0)
+    span = model_width // CHUNKS
+    down_parts = [
+        lax.all_gather(expert_down[0][:, at * span : (at + 1) * span], "tp", axis=0, tiled=True)
+        for at in range(CHUNKS)
+    ]
+
+    outgoing, pick = dispatched(
+        rank, expert_input, gain_expert[None, :], expert_choice, own_tokens, capacity, experts_all
+    )
+    arrived = lax.all_to_all(
+        outgoing.reshape(experts_all, capacity, model_width),
+        "ep",
+        split_axis=0,
+        concat_axis=0,
+        tiled=True,
+    ).reshape(experts_all * capacity, model_width)
+
     normed = rms_scale(mixer_input, gain_mixer)
     queries = jnp.dot(normed, query_weight, preferred_element_type=jnp.float32).astype(jnp.bfloat16)
     key_rows = jnp.dot(normed, key_weight, preferred_element_type=jnp.float32).astype(jnp.bfloat16)
@@ -148,83 +283,36 @@
         first_position,
         sink_logits,
     )
-    picked = attended
+    mixer_part = jnp.dot(attended, output_weight, preferred_element_type=jnp.float32)
     mixer_output = lax.psum_scatter(
-        rounded(jnp.dot(picked, output_weight, preferred_element_type=jnp.float32)).astype(
-            jnp.bfloat16
-        ),
+        mixer_part.astype(jnp.bfloat16), "tp", scatter_dimension=0, tiled=True
+    )
+
+    normed_rows = rms_scale(expert_input, gain_expert)
+    gate_values = jnp.dot(normed_rows, shared_gate, preferred_element_type=jnp.float32)
+    up_values = jnp.dot(normed_rows, shared_up, preferred_element_type=jnp.float32)
+    hidden = (jax.nn.silu(gate_values) * up_values).astype(jnp.bfloat16)
+    shared_part = lax.psum_scatter(
+        jnp.dot(hidden, shared_down, preferred_element_type=jnp.float32).astype(jnp.bfloat16),
         "tp",
         scatter_dimension=0,
         tiled=True,
     )
-    normed_rows = rms_scale(expert_input, gain_expert)
-    group_tokens = normed_rows.shape[0]
-    own_tokens = group_tokens // tp_count
-    top_count = expert_choice.shape[1]
-    local_experts = expert_gate.shape[0]
-    experts_all = local_experts * ep_count
-    capacity = 2 * own_tokens * top_count // experts_all
-    assigned = own_tokens * top_count
-    picked_experts = expert_choice.reshape(tp_count, assigned)
-    onehot = (
-        picked_experts[:, :, None] == jnp.arange(experts_all, dtype=jnp.int32)[None, None, :]
-    ).astype(jnp.int32)
-    slot_ranks = jnp.sum(jnp.cumsum(onehot, axis=1) * onehot, axis=-1) - 1
-    padded_rows = jnp.concatenate([normed_rows, jnp.zeros((1, model_width), jnp.bfloat16)], axis=0)
-
-    def own_slot_index():
-        own_experts = lax.dynamic_index_in_dim(picked_experts, tp_rank, 0, keepdims=False)
-        own_ranks = lax.dynamic_index_in_dim(slot_ranks, tp_rank, 0, keepdims=False)
-        return own_experts * capacity + own_ranks
-
-    own_owner = tp_rank * own_tokens + jnp.arange(assigned, dtype=jnp.int32) // top_count
-    slot_table = (
-        jnp.full((experts_all * capacity,), group_tokens, jnp.int32)
-        .at[own_slot_index()]
-        .set(own_owner)
-    )
-    outgoing = padded_rows[slot_table].reshape(experts_all, 1, capacity, model_width)
-    arrived = lax.all_gather(
-        lax.all_to_all(outgoing, "ep", split_axis=0, concat_axis=0, tiled=True),
-        "tp",
-        axis=1,
-        tiled=True,
-    )
-    sources = arrived.shape[0] // local_experts
-    shaped = arrived.reshape(
-        sources, local_experts, arrived.shape[1], arrived.shape[2], arrived.shape[3]
-    )
-    gate_values = jnp.einsum(
-        "iejcd,edf->iejcf", shaped, expert_gate, preferred_element_type=jnp.float32
-    )
-    up_values = jnp.einsum(
-        "iejcd,edf->iejcf", shaped, expert_up, preferred_element_type=jnp.float32
-    )
-    hidden = (jax.nn.silu(gate_values) * up_values).astype(jnp.bfloat16)
-    result = jnp.einsum("iejcf,efd->iejcd", hidden, expert_down, preferred_element_type=jnp.float32)
-    partials = result.astype(jnp.bfloat16).reshape(arrived.shape)
-    summed = sent_and_summed(partials.astype(jnp.float32).astype(jnp.bfloat16), "tp", 1)
-    returned = (
-        lax.all_to_all(summed.astype(jnp.bfloat16), "ep", split_axis=0, concat_axis=0, tiled=True)
-        .astype(summed.dtype)
-        .reshape(-1, model_width)
-    )
-    own_weights = lax.dynamic_slice_in_dim(route_weights, tp_rank * own_tokens, own_tokens, 0)
-    gathered = returned[own_slot_index().reshape(own_tokens, top_count)]
-    routed = jnp.sum(gathered * own_weights[:, :, None], axis=1)
-    picked = normed_rows
-    gate_values = jnp.dot(picked, shared_gate, preferred_element_type=jnp.float32)
-    up_values = jnp.dot(picked, shared_up, preferred_element_type=jnp.float32)
-    hidden = (jax.nn.silu(gate_values) * up_values).astype(jnp.bfloat16)
-    shared_part = lax.psum_scatter(
-        rounded(jnp.dot(hidden, shared_down, preferred_element_type=jnp.float32)).astype(
-            jnp.bfloat16
-        ),
-        "tp",
-        scatter_dimension=0,
-        tiled=True,
-    ).astype(jnp.float32)
-    expert_output = (routed + shared_part).astype(jnp.bfloat16)
+
+    routed_hidden = expert_hidden(arrived, gate_all, up_all)
+    returned = []
+    for down in down_parts:
+        result = jnp.dot(routed_hidden, down, preferred_element_type=jnp.float32).astype(jnp.bfloat16)
+        returned.append(
+            lax.all_to_all(
+                result.reshape(experts_all, capacity, -1),
+                "ep",
+                split_axis=0,
+                concat_axis=0,
+                tiled=True,
+            ).reshape(experts_all * capacity, -1)
+        )
+    expert_output = combined(rank, pick, route_weights, shared_part, returned)
     return (mixer_output, expert_output)
 
 

time: 416 us -> 266 us (0.64)
  blocking collectives: 63.5 us -> 0 us
  waiting for transfers between devices: 215 us -> 162 us
  local copies, waits for them, and re-layouts: 32.7 us -> 4.47 us
  other arithmetic: 31.7 us -> 6.33 us
  Pallas kernels: 0 us -> 15.5 us
  starting transfers between devices: 18.9 us -> 33.3 us
  matrix products: 39.2 us -> 28.4 us
    all_to_all x2 -> x3, waiting for transfers between devices: 133 us -> 43.6 us  [the longest x1 31.1 us: local(): lax.all_to_all(outgoing.reshape(experts_all, capacity, model_width), 'ep'...]
    all_to_all x1 -> x0, blocking collectives: 63.5 us -> none  [local(): lax.all_to_all(outgoing, 'ep', split_axis=0, concat_axis=0, tiled=True)]
    reduce_scatter x2, waiting for transfers between devices: 0.02 us -> 41.7 us  [the longest x1 22.8 us: local(): lax.psum_scatter(mixer_part.astype(jnp.bfloat16), 'tp', scatter_dimension...]
    gather x3 -> x0, local copies, waits for them, and re-layouts: 16.4 us -> none  [the longest x2 9.32 us: local(): gathered = returned[own_slot_index().reshape(own_tokens, top_count)]]
    pallas_call x0 -> x3, Pallas kernels: none -> 15.5 us  [the longest x1 8.53 us: expert_hidden(): pl.pallas_call(hidden_body, grid=(parts,), in_specs=[pl.BlockSpec((slots,...]
    all_to_all x2 -> x3, starting transfers between devices: 16.4 us -> 30.9 us  [the longest x2 17.6 us: local(): lax.all_to_all(result.reshape(experts_all, capacity, -1), 'ep', split_axi...]
    reduce_sum x3 -> x0, other arithmetic: 12.2 us -> none  [the longest x1 7.27 us: sent_and_summed(): return arrived.astype(jnp.float32).sum(axis=0)]
    dot_general x4, matrix products: 24.2 us -> 13.4 us  [the longest x2 8.36 us: local(): jnp.dot(routed_hidden, down, preferred_element_type=jnp.float32)]
  transfers between devices with their start and end apart: 6 -> 10, of which waited for: 3 -> 8; matrix products, arithmetic and copies ran while one was open for 13% -> 15% of each run, Pallas kernels for 0% -> 6%
where the time goes in v1:
time: 266 us; the launch traced here: 264 us
  waiting for transfers between devices  162 us (61%)
  starting transfers between devices  33.3 us (13%)
  matrix products  28.4 us (11%)
  Pallas kernels  15.5 us (6%)
  between operations  14.5 us (5%)
  other arithmetic  6.33 us (2%)
  local copies, waits for them, and re-layouts  4.47 us (2%)
    all_gather x2, waiting for transfers between devices, local(): lax.all_gather(expert_down[0][:, at * span:(at + 1) * span], 'tp', axis=0...  47.9 us
    all_to_all x1, waiting for transfers between devices, local(): lax.all_to_all(outgoing.reshape(experts_all, capacity, model_width), 'ep'...  31.1 us
    all_gather x1, waiting for transfers between devices, local(): up_all = lax.all_gather(expert_up[0], 'tp', axis=0)  26.7 us
    reduce_scatter x1, waiting for transfers between devices, local(): lax.psum_scatter(mixer_part.astype(jnp.bfloat16), 'tp', scatter_dimension...  22.8 us
    reduce_scatter x1, waiting for transfers between devices, local(): lax.psum_scatter(jnp.dot(hidden, shared_down, preferred_element_type=jnp....  19 us
    all_to_all x2, starting transfers between devices, local(): lax.all_to_all(result.reshape(experts_all, capacity, -1), 'ep', split_axi...  17.6 us
    all_to_all x1, starting transfers between devices, local(): lax.all_to_all(outgoing.reshape(experts_all, capacity, model_width), 'ep'...  13.3 us
    all_to_all x2, waiting for transfers between devices, local(): lax.all_to_all(result.reshape(experts_all, capacity, -1), 'ep', split_axi...  12.5 us
  transfers between devices with their start and end apart: 10, of which 8 were waited for; matrix products, arithmetic and copies ran while one was open for 15% of the time, Pallas kernels for 6%

profile of v1, /device:TPU:2, one launch (start us, length us, event | category | flops | bytes accessed | tf_op | source)
XLA Modules:
  0.0 264.3 jit_solution(6417594620546820039)
XLA Ops:
  7.2 0.0 copy-start
  7.2 0.0 all-gather.5.cloned.1.call-start
  7.2 0.7 all-gather.5.cloned.1.call-update
  7.9 0.0 all-gather.7.cloned.1.call-start
  8.0 0.7 all-gather.7.cloned.1.call-update
  8.7 0.0 all-gather.9.cloned.1.call-start
  8.7 2.2 fusion.68
  11.0 0.0 all-gather.9.cloned.1.call-update
  11.0 0.0 all-gather.11.cloned.1.call-start
  11.0 0.5 all-gather.11.cloned.1.call-update
  11.6 0.0 copy-start.9
  11.6 2.1 fusion
  13.7 0.0 copy-done.8
  13.7 2.4 convolution_convert_fusion.5
  16.2 0.0 copy-start.3
  16.2 0.0 copy-done.9
  16.2 2.4 fusion.21
  18.6 0.3 fusion.54
  19.0 1.9 collective-permute-start
  20.9 0.0 copy-done.3
  20.9 0.9 copy.47.choice_ref
  21.8 3.6 %dispatch.1 = (bf16[512,2048]{1,0:T(8,128)(2,1)}, bf16[2,128,512]{2,1,0:T(8,128)(2,1)}) custom-call(s32[1]{0:T(128)} %bitcast.19.rank_ref, bf16[512,2048]{1,0:T(8,128)(2,1)} %rows_ref.1, f32[1,2048]{1,0:T(1,128)} %bitcast.123, s32[512,2]{1,0:T(8,128)} %copy.47.choice_ref), custom_call_target="tpu_custom_call" | custom-call | tf_op jit(solution)/shard_map/dispatch/pallas_call | solution.py:126
  25.4 13.3 %all-to-all-start = ((bf16[64,8,2048]{2,1,0:T(8,128)(2,1)}), bf16[64,8,2048]{2,1,0:T(8,128)(2,1)}, u32[]{:S(2)}, u32[]{:S(2)}) async-start(bf16[64,8,2048]{2,1,0:T(8,128)(2,1)} %bitcast.116), calls=%async_computation.2 | async-start | bytes 4194304 | tf_op jit(solution)/shard_map/all_to_all | solution.py:250
  38.7 0.0 copy-start.7
  38.7 0.0 reduce-scatter.5.cloned.1.call-start
  38.7 2.2 fusion.3
  40.9 0.0 copy-done.6
  40.9 2.4 fusion.24
  43.3 5.4 %convolution_convert_fusion = bf16[512,2048]{1,0:T(8,128)(2,1)} fusion(bf16[128,2048]{1,0:T(8,128)(2,1)S(1)} %copy-done.7, bf16[2048,128]{1,0:T(8,128)(2,1)} %param.32, bf16[512,2048]{1,0:T(8,128)(2,1)} %rows_ref.1, f32[2048]{0:T(1024)S(1)} %copy-done.2, f32[512]{0:T(512)S(1)} %add_rsqrt_fusion, f32[512,128]{1,0:T(8,128)S(1)} %fusion.24), kind=kOutput, calls=%fused_computation.13 | convolution fusion | flops 542507008 | bytes 5515264 | tf_op jit(solution)/shard_map/dot_general | solution.py:296
  48.7 0.0 reduce-scatter.5.cloned.1.call-update
  48.7 0.2 reduce-scatter.3.cloned.1.call-start
  48.9 3.2 %convolution_convert_fusion.4 = bf16[512,384]{0,1:T(8,128)(2,1)S(1)} fusion(bf16[2048,384]{1,0:T(8,128)(2,1)} %param.21, bf16[512,2048]{1,0:T(8,128)(2,1)} %param.17, f32[2048]{0:T(1024)S(1)} %copy-done.10, f32[512]{0:T(512)S(1)} %add_rsqrt_fusion.1), kind=kOutput, calls=%fused_computation.24 | convolution fusion | flops 809697280 | bytes 4073472 | tf_op jit(solution)/shard_map/dot_general | solution.py:259
  52.1 0.1 convert.25
  52.2 0.1 add_compare_fusion
  52.4 0.3 multiply_cosine_fusion
  52.7 0.2 broadcast_and_fusion
  52.9 0.1 fusion.37
  53.0 0.0 copy-start.5
  53.0 0.1 copy_bitcast_fusion
  53.2 0.0 collective-permute-done
  53.3 0.6 fusion.7
  53.9 0.1 broadcast_maximum_fusion
  54.0 0.7 fusion.6
  54.7 0.1 exponential_add_fusion
  54.7 0.9 fusion.16
  55.7 0.3 copy.46
  56.0 2.7 %convolution_convert_fusion.1 = bf16[512,2048]{1,0:T(8,128)(2,1)} fusion(bf16[384,2048]{1,0:T(8,128)(2,1)S(1)} %copy-done, bf16[48,8,4,128]{3,2,1,0:T(4,128)(2,1)S(1)} %bitcast.118), kind=kOutput, calls=%fused_computation.14 | convolution fusion | flops 806354944 | bytes 4063232 | tf_op jit(solution)/shard_map/dot_general | solution.py:286
  58.7 0.0 reduce-scatter.3.cloned.1.call-update
  58.7 31.1 %all-to-all-done = bf16[64,8,2048]{2,1,0:T(8,128)(2,1)} async-done(((bf16[64,8,2048]{2,1,0:T(8,128)(2,1)}), bf16[64,8,2048]{2,1,0:T(8,128)(2,1)}, u32[]{:S(2)}, u32[]{:S(2)}) %all-to-all-start) | async-done | bytes 2097184 | tf_op jit(solution)/shard_map/all_to_all | solution.py:250
  89.8 26.7 %all-gather.7.cloned.1.call-done.up_ref = bf16[4,2048,256]{2,1,0:T(8,128)(2,1)} async-done(((bf16[1,2048,256]{2,1,0:T(8,128)(2,1)}), bf16[4,2048,256]{2,1,0:T(8,128)(2,1)}) %all-gather.7.cloned.1.call-update) | async-done | bytes 4194320 | tf_op jit(solution)/shard_map/all_gather | solution.py:240
  116.5 8.5 %hidden.1 = bf16[512,1024]{1,0:T(8,128)(2,1)} custom-call(bf16[512,2048]{1,0:T(8,128)(2,1)} %bitcast.22.rows_ref, bf16[4,2048,256]{2,1,0:T(8,128)(2,1)} %all-gather.5.cloned.1.call-done.gate_ref, bf16[4,2048,256]{2,1,0:T(8,128)(2,1)} %all-gather.7.cloned.1.call-done.up_ref), custom_call_target="tpu_custom_call" | custom-call | tf_op jit(solution)/shard_map/hidden/pallas_call | solution.py:158
  125.1 27.0 %all-gather.9.cloned.1.call-done = bf16[1024,1024]{1,0:T(8,128)(2,1)} async-done(((bf16[256,1024]{1,0:T(8,128)(2,1)}), bf16[1024,1024]{1,0:T(8,128)(2,1)}) %all-gather.9.cloned.1.call-update) | async-done | bytes 2097168 | tf_op jit(solution)/shard_map/all_gather | solution.py:243
  152.1 4.2 %fusion.11 = bf16[64,8,1024]{2,1,0:T(8,128)(2,1)} fusion(bf16[512,1024]{1,0:T(8,128)(2,1)} %hidden.1, bf16[1024,1024]{1,0:T(8,128)(2,1)} %all-gather.9.cloned.1.call-done), kind=kOutput, calls=%fused_computation.22 | convolution fusion | flops 1074266112 | bytes 4194304 | tf_op jit(solution)/shard_map/dot_general | solution.py:305
  156.2 10.5 %all-to-all-start.1 = ((bf16[64,8,1024]{2,1,0:T(8,128)(2,1)}), bf16[64,8,1024]{2,1,0:T(8,128)(2,1)S(1)}, u32[]{:S(2)}, u32[]{:S(2)}) async-start(bf16[64,8,1024]{2,1,0:T(8,128)(2,1)} %fusion.11), calls=%async_computation.3 | async-start | bytes 2097152 | tf_op jit(solution)/shard_map/all_to_all | solution.py:307
  166.8 0.0 copy-start.4
  166.8 20.9 %all-gather.11.cloned.1.call-done = bf16[1024,1024]{1,0:T(8,128)(2,1)} async-done(((bf16[256,1024]{1,0:T(8,128)(2,1)}), bf16[1024,1024]{1,0:T(8,128)(2,1)}) %all-gather.11.cloned.1.call-update) | async-done | bytes 2097168 | tf_op jit(solution)/shard_map/all_gather | solution.py:243
  187.7 4.2 %fusion.12 = bf16[64,8,1024]{2,1,0:T(8,128)(2,1)} fusion(bf16[512,1024]{1,0:T(8,128)(2,1)} %hidden.1, bf16[1024,1024]{1,0:T(8,128)(2,1)} %all-gather.11.cloned.1.call-done), kind=kOutput, calls=%fused_computation.23 | convolution fusion | flops 1074266112 | bytes 4194304 | tf_op jit(solution)/shard_map/dot_general | solution.py:305
  191.9 3.7 %all-to-all-done.1 = bf16[64,8,1024]{2,1,0:T(8,128)(2,1)S(1)} async-done(((bf16[64,8,1024]{2,1,0:T(8,128)(2,1)}), bf16[64,8,1024]{2,1,0:T(8,128)(2,1)S(1)}, u32[]{:S(2)}, u32[]{:S(2)}) %all-to-all-start.1) | async-done | bytes 1048608 | tf_op jit(solution)/shard_map/all_to_all | solution.py:307
  195.6 7.1 %all-to-all-start.2 = ((bf16[64,8,1024]{2,1,0:T(8,128)(2,1)}), bf16[64,8,1024]{2,1,0:T(8,128)(2,1)}, u32[]{:S(2)}, u32[]{:S(2)}) async-start(bf16[64,8,1024]{2,1,0:T(8,128)(2,1)} %fusion.12), calls=%async_computation.4 | async-start | bytes 2097152 | tf_op jit(solution)/shard_map/all_to_all | solution.py:307
  202.6 0.8 copy.48.weight_ref
  203.5 19.0 %reduce-scatter.5.cloned.1.call-done.shared_ref = bf16[128,2048]{1,0:T(8,128)(2,1)} async-done(((bf16[512,2048]{1,0:T(8,128)(2,1)}), bf16[128,2048]{1,0:T(8,128)(2,1)}) %reduce-scatter.5.cloned.1.call-update) | async-done | bytes 524304 | tf_op jit(solution)/shard_map/reduce_scatter | solution.py:295
  222.5 8.9 %all-to-all-done.2 = bf16[64,8,1024]{2,1,0:T(8,128)(2,1)} async-done(((bf16[64,8,1024]{2,1,0:T(8,128)(2,1)}), bf16[64,8,1024]{2,1,0:T(8,128)(2,1)}, u32[]{:S(2)}, u32[]{:S(2)}) %all-to-all-start.2) | async-done | bytes 1048608 | tf_op jit(solution)/shard_map/all_to_all | solution.py:307
  231.3 3.4 %combine.1 = bf16[128,2048]{1,0:T(8,128)(2,1)} custom-call(s32[1]{0:T(128)} %bitcast.19.rank_ref, bf16[2,128,512]{2,1,0:T(8,128)(2,1)} %get-tuple-element.4.pick_ref, f32[512,2]{1,0:T(8,128)} %copy.48.weight_ref, bf16[128,2048]{1,0:T(8,128)(2,1)} %reduce-scatter.5.cloned.1.call-done.shared_ref, bf16[512,1024]{1,0:T(8,128)(2,1)} %bitcast.115, ...), custom_call_target="tpu_custom_call" | custom-call | tf_op jit(solution)/shard_map/combine/pallas_call | solution.py:191
  234.7 22.8 %reduce-scatter.3.cloned.1.call-done = bf16[128,2048]{1,0:T(8,128)(2,1)} async-done(((bf16[512,2048]{1,0:T(8,128)(2,1)}), bf16[128,2048]{1,0:T(8,128)(2,1)}) %reduce-scatter.3.cloned.1.call-update) | async-done | bytes 524304 | tf_op jit(solution)/shard_map/reduce_scatter | solution.py:287
  (30 shorter events, 0.2 us)
Async XLA Ops:
  7.2 48.8 %copy-start = (bf16[384,2048]{1,0:T(8,128)(2,1)S(1)}, bf16[384,2048]{1,0:T(8,128)(2,1)}, u32[]{:S(2)}) copy-start(bf16[384,2048]{1,0:T(8,128)(2,1)} %param.25) | copy-start | bytes 4718596
  7.2 82.6 %all-gather.5.cloned.1.call-start = ((), (), s32[]{:S(2)}) async-start(), calls=%async_computation.7 | async-start | bytes 5242880 | tf_op jit(solution)/shard_map/all_gather | solution.py:239
  7.9 5.8 %copy-start.8 = (bf16[2048,64]{0,1:T(8,128)(2,1)S(1)}, bf16[2048,64]{0,1:T(8,128)(2,1)}, u32[]{:S(2)}) copy-start(bf16[2048,64]{0,1:T(8,128)(2,1)} %param.23) | copy-start | bytes 786436
  7.9 5.8 %copy-start.10 = (f32[2048]{0:T(1024)S(1)}, f32[2048]{0:T(1024)}, u32[]{:S(2)}) copy-start(f32[2048]{0:T(1024)} %param.19) | copy-start | bytes 24580
  7.9 108.6 %all-gather.7.cloned.1.call-start = ((), (), s32[]{:S(2)}) async-start(), calls=%async_computation.8 | async-start | bytes 5242880 | tf_op jit(solution)/shard_map/all_gather | solution.py:240
  8.7 143.4 %all-gather.9.cloned.1.call-start = ((), (), s32[]{:S(2)}) async-start(), calls=%async_computation.9 | async-start | bytes 2621440 | tf_op jit(solution)/shard_map/all_gather | solution.py:243
  11.0 176.7 %all-gather.11.cloned.1.call-start = ((), (), s32[]{:S(2)}) async-start(), calls=%async_computation.10 | async-start | bytes 2621440 | tf_op jit(solution)/shard_map/all_gather | solution.py:243
  11.6 4.6 %copy-start.9 = (bf16[2048,64]{0,1:T(8,128)(2,1)S(1)}, bf16[2048,64]{0,1:T(8,128)(2,1)}, u32[]{:S(2)}) copy-start(bf16[2048,64]{0,1:T(8,128)(2,1)} %param.22) | copy-start | bytes 786436
  16.2 4.8 %copy-start.3 = (s32[512,2]{0,1:T(2,128)S(1)}, s32[512,2]{0,1:T(2,128)}, u32[]{:S(2)}) copy-start(s32[512,2]{0,1:T(2,128)} %param.26) | copy-start | bytes 12292
  19.0 34.2 %collective-permute-start = (bf16[128,128]{0,1:T(8,128)(2,1)S(1)}, bf16[128,128]{0,1:T(8,128)(2,1)S(1)}, u32[]{:S(2)}, u32[]{:S(2)}) collective-permute-start(bf16[128,128]{0,1:T(8,128)(2,1)S(1)} %pad_maximum_fusion.3), channel_id=1, source_target_pairs={{0,4},{4,8},{8,12},{12,16},{16,20},{20,24},{24,28},{28,32},{32,36}... | collective-permute-start | bytes 98312 | tf_op jit(solution)/shard_map/ppermute | solution.py:23
  25.3 15.6 %copy-start.2 = (f32[2048]{0:T(1024)S(1)}, f32[2048]{0:T(1024)}, u32[]{:S(2)}) copy-start(f32[2048]{0:T(1024)} %param.20) | copy-start | bytes 24580
  25.4 15.6 %copy-start.6 = (bf16[2048,128]{1,0:T(8,128)(2,1)S(1)}, bf16[2048,128]{1,0:T(8,128)(2,1)}, u32[]{:S(2)}) copy-start(bf16[2048,128]{1,0:T(8,128)(2,1)} %param.31) | copy-start | bytes 1572868
  25.4 64.5 %all-to-all-start = ((bf16[64,8,2048]{2,1,0:T(8,128)(2,1)}), bf16[64,8,2048]{2,1,0:T(8,128)(2,1)}, u32[]{:S(2)}, u32[]{:S(2)}) async-start(bf16[64,8,2048]{2,1,0:T(8,128)(2,1)} %bitcast.116), calls=%async_computation.2 | async-start | bytes 4194304 | tf_op jit(solution)/shard_map/all_to_all | solution.py:250
  38.7 4.6 %copy-start.7 = (bf16[128,2048]{1,0:T(8,128)(2,1)S(1)}, bf16[128,2048]{1,0:T(8,128)(2,1)}, u32[]{:S(2)}) copy-start(bf16[128,2048]{1,0:T(8,128)(2,1)} %param.33) | copy-start | bytes 1572868
  38.7 183.8 %reduce-scatter.5.cloned.1.call-start = ((), (), s32[]{:S(2)}) async-start(), calls=%async_computation.6 | async-start | bytes 2621440 | tf_op jit(solution)/shard_map/reduce_scatter | solution.py:295
  48.7 208.8 %reduce-scatter.3.cloned.1.call-start = ((), (), s32[]{:S(2)}) async-start(), calls=%async_computation.5 | async-start | bytes 2621440 | tf_op jit(solution)/shard_map/reduce_scatter | solution.py:287
  53.0 0.9 copy-start.5
  156.2 39.3 %all-to-all-start.1 = ((bf16[64,8,1024]{2,1,0:T(8,128)(2,1)}), bf16[64,8,1024]{2,1,0:T(8,128)(2,1)S(1)}, u32[]{:S(2)}, u32[]{:S(2)}) async-start(bf16[64,8,1024]{2,1,0:T(8,128)(2,1)} %fusion.11), calls=%async_computation.3 | async-start | bytes 2097152 | tf_op jit(solution)/shard_map/all_to_all | solution.py:307
  166.8 35.9 %copy-start.4 = (f32[512,2]{0,1:T(2,128)S(1)}, f32[512,2]{0,1:T(2,128)}, u32[]{:S(2)}) copy-start(f32[512,2]{0,1:T(2,128)} %param.27) | copy-start | bytes 12292
  195.6 35.8 %copy-start.1 = (bf16[64,8,1024]{2,1,0:T(8,128)(2,1)}, bf16[64,8,1024]{2,1,0:T(8,128)(2,1)S(1)}, u32[]{:S(2)}) copy-start(bf16[64,8,1024]{2,1,0:T(8,128)(2,1)S(1)} %all-to-all-done.1) | copy-start | bytes 3145732
  195.6 35.8 %all-to-all-start.2 = ((bf16[64,8,1024]{2,1,0:T(8,128)(2,1)}), bf16[64,8,1024]{2,1,0:T(8,128)(2,1)}, u32[]{:S(2)}, u32[]{:S(2)}) async-start(bf16[64,8,1024]{2,1,0:T(8,128)(2,1)} %fusion.12), calls=%async_computation.4 | async-start | bytes 2097152 | tf_op jit(solution)/shard_map/all_to_all | solution.py:307
Sparse Core Ops, SparseCore 0:
  9.8 53.7 all-gather.4
  65.4 51.1 all-gather.6
  118.3 33.6 all-gather.8
  154.3 33.3 all-gather.10
  190.1 32.3 reduce-scatter.4
  225.4 31.9 reduce-scatter.2

commit v2 on v1

--- a/solution.py
+++ b/solution.py
@@ -7,10 +7,11 @@
 from jax.experimental.pallas import tpu as pltpu
 from jax.sharding import PartitionSpec as P
 
+
 HEAD_DIM = 64
 WINDOW = 128
 SEQS = 1
-CHUNKS = 2
+PIECES = ((256, 256), (768, 768))
 
 
 norm_eps = 1e-06
@@ -21,6 +22,44 @@
     count = lax.axis_size(axis)
     first, last = (max(0, -steps), min(count, count - steps))
     return lax.ppermute(value, axis, [(source, source + steps) for source in range(first, last)])
+
+
+def shifted(value, steps):
+    count = lax.axis_size("tp")
+    return lax.ppermute(value, "tp", [(at, (at + steps) % count) for at in range(count)])
+
+
+def crossed(value, mask):
+    return lax.ppermute(value, "tp", [(at, at ^ mask) for at in range(lax.axis_size("tp"))])
+
+
+def exchanged(rows, experts):
+    slots, width = rows.shape
+    return lax.all_to_all(
+        rows.reshape(experts, slots // experts, width),
+        "ep",
+        split_axis=0,
+        concat_axis=0,
+        tiled=True,
+    ).reshape(slots, width)
+
+
+def halved_sum(rows, weight, own_rows, mask):
+    rank = lax.axis_index("tp")
+    other = mask ^ 2
+
+    def product(*masks):
+        blocks = [
+            lax.dynamic_slice_in_dim(rows, (rank ^ each) * own_rows, own_rows, 0) for each in masks
+        ]
+        joined = jnp.concatenate(blocks, axis=0)
+        return jnp.dot(joined, weight, preferred_element_type=jnp.float32).astype(jnp.bfloat16)
+
+    got = crossed(product(mask, 2), mask)
+    kept = product(0, other)
+    half = kept.astype(jnp.float32) + got.astype(jnp.float32)
+    last = crossed(half[own_rows:].astype(jnp.bfloat16), other)
+    return half[:own_rows] + last.astype(jnp.float32)
 
 
 def rms_scale(matrix, scaling):
@@ -146,27 +185,68 @@
     )(rank, rows, gain, choice)
 
 
-def hidden_body(rows_ref, gate_ref, up_ref, out_ref):
-    gate = jnp.dot(rows_ref[...], gate_ref[0], preferred_element_type=jnp.float32)
-    up = jnp.dot(rows_ref[...], up_ref[0], preferred_element_type=jnp.float32)
-    out_ref[...] = (gate / (1.0 + jnp.exp(-gate)) * up).astype(jnp.bfloat16)
-
-
-def expert_hidden(rows, gate, up):
+def hidden_body(rows_ref, *refs):
+    out_ref = refs[-1]
+    weights = refs[:-1]
+    at = 0
+    for gate_ref, up_ref in zip(weights[0::2], weights[1::2]):
+        units = gate_ref.shape[1]
+        gate = jnp.dot(rows_ref[...], gate_ref[...], preferred_element_type=jnp.float32)
+        up = jnp.dot(rows_ref[...], up_ref[...], preferred_element_type=jnp.float32)
+        out_ref[:, at : at + units] = (gate / (1.0 + jnp.exp(-gate)) * up).astype(jnp.bfloat16)
+        at += units
+
+
+def expert_hidden(rows, pairs, steps=2):
     slots, width = rows.shape
-    parts, _, units = gate.shape
+    units = pairs[0][0].shape[1]
+    block = slots // steps
+    flat = [matrix for pair in pairs for matrix in pair]
     return pl.pallas_call(
         hidden_body,
-        grid=(parts,),
-        in_specs=[
-            pl.BlockSpec((slots, width), lambda i: (0, 0)),
-            pl.BlockSpec((1, width, units), lambda i: (i, 0, 0)),
-            pl.BlockSpec((1, width, units), lambda i: (i, 0, 0)),
-        ],
-        out_specs=pl.BlockSpec((slots, units), lambda i: (0, i)),
-        out_shape=jax.ShapeDtypeStruct((slots, parts * units), jnp.bfloat16),
+        grid=(steps,),
+        in_specs=[pl.BlockSpec((block, width), lambda i: (i, 0))]
+        + [pl.BlockSpec((width, units), lambda i: (0, 0))] * len(flat),
+        out_specs=pl.BlockSpec((block, len(pairs) * units), lambda i: (i, 0)),
+        out_shape=jax.ShapeDtypeStruct((slots, len(pairs) * units), jnp.bfloat16),
         name="hidden",
-    )(rows, gate, up)
+    )(rows, *flat)
+
+
+def down_body(hidden_ref, *refs):
+    out_ref = refs[-1]
+    weights = refs[:-1]
+    slices = 4
+    units = weights[0].shape[0]
+    at = 0
+    for piece in range(len(weights) // slices):
+        group = weights[piece * slices : (piece + 1) * slices]
+        span = group[0].shape[1]
+        total = 0.0
+        for index, weight in enumerate(group):
+            total = total + jnp.dot(
+                hidden_ref[:, index * units : (index + 1) * units],
+                weight[...],
+                preferred_element_type=jnp.float32,
+            )
+        out_ref[:, at : at + span] = total.astype(jnp.bfloat16)
+        at += span
+
+
+def expert_result(hidden, groups, steps=2):
+    slots, units_all = hidden.shape
+    block = slots // steps
+    flat = [matrix for group in groups for matrix in group]
+    width = sum(group[0].shape[1] for group in groups)
+    return pl.pallas_call(
+        down_body,
+        grid=(steps,),
+        in_specs=[pl.BlockSpec((block, units_all), lambda i: (i, 0))]
+        + [pl.BlockSpec(matrix.shape, lambda i: (0, 0)) for matrix in flat],
+        out_specs=pl.BlockSpec((block, width), lambda i: (i, 0)),
+        out_shape=jax.ShapeDtypeStruct((slots, width), jnp.bfloat16),
+        name="down",
+    )(hidden, *flat)
 
 
 def combine_body(rank_ref, pick_ref, weight_ref, shared_ref, *rest):
@@ -206,7 +286,7 @@
     )(rank, pick, weights, shared, *parts)
 
 
-def local(
+def both(
     mixer_input,
     expert_input,
     gain_mixer,
@@ -229,31 +309,36 @@
     ep_count = lax.axis_size("ep")
     tp_rank = lax.axis_index("tp")
     rank = tp_rank.astype(jnp.int32).reshape(1)
-    group_rows, model_width = mixer_input.shape
+    group_rows, _ = mixer_input.shape
     group_tokens = expert_input.shape[0]
     own_tokens = group_tokens // tp_count
     top_count = expert_choice.shape[1]
     experts_all = ep_count
     capacity = 2 * own_tokens * top_count // experts_all
 
-    gate_all = lax.all_gather(expert_gate[0], "tp", axis=0)
-    up_all = lax.all_gather(expert_up[0], "tp", axis=0)
-    span = model_width // CHUNKS
-    down_parts = [
-        lax.all_gather(expert_down[0][:, at * span : (at + 1) * span], "tp", axis=0, tiled=True)
-        for at in range(CHUNKS)
-    ]
+    gate, up, down = expert_gate[0], expert_up[0], expert_down[0]
+    gate_left, gate_right = shifted(gate, 1), shifted(gate, -1)
+    up_left, up_right = shifted(up, 1), shifted(up, -1)
+    gate_far, up_far = shifted(gate_left, 1), shifted(up_right, -1)
+    chunks = []
+    at = 0
+    for spans in PIECES:
+        groups = []
+        for index, span in enumerate(spans):
+            piece = down[:, at : at + span]
+            at += span
+            left, right = shifted(piece, 1), shifted(piece, -1)
+            if index == 0:
+                far = shifted(left, 1)
+            else:
+                far = shifted(right, -1)
+            groups.append((piece, left, right, far))
+        chunks.append(groups)
 
     outgoing, pick = dispatched(
         rank, expert_input, gain_expert[None, :], expert_choice, own_tokens, capacity, experts_all
     )
-    arrived = lax.all_to_all(
-        outgoing.reshape(experts_all, capacity, model_width),
-        "ep",
-        split_axis=0,
-        concat_axis=0,
-        tiled=True,
-    ).reshape(experts_all * capacity, model_width)
+    arrived = exchanged(outgoing, experts_all)
 
     normed = rms_scale(mixer_input, gain_mixer)
     queries = jnp.dot(normed, query_weight, preferred_element_type=jnp.float32).astype(jnp.bfloat16)
@@ -283,35 +368,21 @@
         first_position,
         sink_logits,
     )
-    mixer_part = jnp.dot(attended, output_weight, preferred_element_type=jnp.float32)
-    mixer_output = lax.psum_scatter(
-        mixer_part.astype(jnp.bfloat16), "tp", scatter_dimension=0, tiled=True
-    )
+    mixer_output = halved_sum(attended, output_weight, own_tokens, 1).astype(jnp.bfloat16)
 
     normed_rows = rms_scale(expert_input, gain_expert)
     gate_values = jnp.dot(normed_rows, shared_gate, preferred_element_type=jnp.float32)
     up_values = jnp.dot(normed_rows, shared_up, preferred_element_type=jnp.float32)
     hidden = (jax.nn.silu(gate_values) * up_values).astype(jnp.bfloat16)
-    shared_part = lax.psum_scatter(
-        jnp.dot(hidden, shared_down, preferred_element_type=jnp.float32).astype(jnp.bfloat16),
-        "tp",
-        scatter_dimension=0,
-        tiled=True,
-    )
-
-    routed_hidden = expert_hidden(arrived, gate_all, up_all)
+    shared_part = halved_sum(hidden, shared_down, own_tokens, 3)
+
+    routed_hidden = expert_hidden(
+        arrived, [(gate, up), (gate_left, up_left), (gate_right, up_right), (gate_far, up_far)]
+    )
     returned = []
-    for down in down_parts:
-        result = jnp.dot(routed_hidden, down, preferred_element_type=jnp.float32).astype(jnp.bfloat16)
-        returned.append(
-            lax.all_to_all(
-                result.reshape(experts_all, capacity, -1),
-                "ep",
-                split_axis=0,
-                concat_axis=0,
-                tiled=True,
-            ).reshape(experts_all * capacity, -1)
-        )
+    for groups in chunks:
+        result = expert_result(routed_hidden, groups)
+        returned.append(exchanged(result, experts_all))
     expert_output = combined(rank, pick, route_weights, shared_part, returned)
     return (mixer_output, expert_output)
 
@@ -337,7 +408,7 @@
         P("tp", None),
     )
     return jax.shard_map(
-        local,
+        both,
         mesh=mesh,
         in_specs=placed,
         out_specs=(P(("ep", "tp"), None), P(("ep", "tp"), None)),

time: 266 us -> 221 us (0.83)
  waiting for transfers between devices: 162 us -> 85.4 us
  starting transfers between devices: 33.3 us -> 67.7 us
  between operations: 14.5 us -> 1.28 us
  matrix products: 28.4 us -> 16.4 us
  local copies, waits for them, and re-layouts: 4.47 us -> 13.5 us
  Pallas kernels: 15.5 us -> 24.3 us
  other arithmetic: 6.33 us -> 11.5 us
    ppermute x0 -> x22, waiting for transfers between devices: none -> 85.4 us  [the longest x18 57.8 us: shifted(): lax.ppermute(value, 'tp', [(at, (at + steps) % count) for at in range(cou...]
    all_gather x4 -> x0, waiting for transfers between devices: 74.6 us -> none  [the longest x2 47.9 us: local(): lax.all_gather(expert_down[0][:, at * span:(at + 1) * span], 'tp', axis=0...]
    all_to_all x3, waiting for transfers between devices: 43.6 us -> 0.01 us  [exchanged(): lax.all_to_all(rows.reshape(experts, slots // experts, width), 'ep', spli...]
    reduce_scatter x2 -> x0, waiting for transfers between devices: 41.7 us -> none  [the longest x1 22.8 us: local(): lax.psum_scatter(mixer_part.astype(jnp.bfloat16), 'tp', scatter_dimension...]
    ppermute x0 -> x22, starting transfers between devices: none -> 29.3 us  [the longest x18 22.2 us: shifted(): lax.ppermute(value, 'tp', [(at, (at + steps) % count) for at in range(cou...]
    dot_general x8 -> x9, matrix products: 26.8 us -> 12 us  [the longest x4 4.48 us: product(): jnp.dot(joined, weight, preferred_element_type=jnp.float32)]
    pallas_call x1 -> x3, Pallas kernels: 8.53 us -> 17.1 us  [the longest x1 9.28 us: expert_hidden(): pl.pallas_call(hidden_body, grid=(steps,), in_specs=[pl.BlockSpec((block,...]
    unnamed x24 -> x65, local copies, waits for them, and re-layouts: 1.77 us -> 7.78 us
  transfers between devices with their start and end apart: 10 -> 26, of which waited for: 8 -> 8; matrix products, arithmetic and copies ran while one was open for 15% -> 16% of each run, Pallas kernels for 6% -> 9%
where the time goes in v2:
time: 221 us; the launch traced here: 220 us
  waiting for transfers between devices  85.4 us (39%)
  starting transfers between devices  67.7 us (31%)
  Pallas kernels  24.3 us (11%)
  matrix products  16.4 us (7%)
  local copies, waits for them, and re-layouts  13.5 us (6%)
  other arithmetic  11.5 us (5%)
    ppermute x18, waiting for transfers between devices, shifted(): lax.ppermute(value, 'tp', [(at, (at + steps) % count) for at in range(cou...  57.8 us
    all_to_all x3, starting transfers between devices, exchanged(): lax.all_to_all(rows.reshape(experts, slots // experts, width), 'ep', spli...  36.4 us
    ppermute x4, waiting for transfers between devices, crossed(): lax.ppermute(value, 'tp', [(at, at ^ mask) for at in range(lax.axis_size(...  27.6 us
    ppermute x18, starting transfers between devices, shifted(): lax.ppermute(value, 'tp', [(at, (at + steps) % count) for at in range(cou...  22.2 us
    pallas_call x1, Pallas kernels, expert_hidden(): pl.pallas_call(hidden_body, grid=(steps,), in_specs=[pl.BlockSpec((block,...  9.28 us
    pallas_call x2, Pallas kernels, expert_result(): pl.pallas_call(down_body, grid=(steps,), in_specs=[pl.BlockSpec((block, u...  7.84 us
    unnamed x65, local copies, waits for them, and re-layouts  7.78 us
    ppermute x4, starting transfers between devices, crossed(): lax.ppermute(value, 'tp', [(at, at ^ mask) for at in range(lax.axis_size(...  7.12 us
  transfers between devices with their start and end apart: 26, of which 8 were waited for; matrix products, arithmetic and copies ran while one was open for 16% of the time, Pallas kernels for 9%

profile of v2, /device:TPU:2, one launch (start us, length us, event | category | flops | bytes accessed | tf_op | source)
XLA Modules:
  0.0 220.1 jit_solution(624906221947305500)
XLA Ops:
  0.6 3.1 %collective-permute-start.8 = (bf16[2048,256]{1,0:T(8,128)(2,1)}, bf16[2048,256]{1,0:T(8,128)(2,1)}, u32[]{:S(2)}, u32[]{:S(2)}) collective-permute-start(bf16[2048,256]{1,0:T(8,128)(2,1)} %bitcast.125), channel_id=1, source_target_pairs={{0,3},{1,0},{2,1},{3,2},{4,7},{5,4},{6,5},{7,6},{8,11},{9,8},{10,9... | collective-permute-start | bytes 3145736 | tf_op jit(solution)/shard_map/ppermute | solution.py:29
  3.7 0.6 collective-permute-start.5
  4.3 2.7 %collective-permute-start.7 = (bf16[2048,256]{1,0:T(8,128)(2,1)}, bf16[2048,256]{1,0:T(8,128)(2,1)}, u32[]{:S(2)}, u32[]{:S(2)}) collective-permute-start(bf16[2048,256]{1,0:T(8,128)(2,1)} %bitcast.123), channel_id=1, source_target_pairs={{0,3},{1,0},{2,1},{3,2},{4,7},{5,4},{6,5},{7,6},{8,11},{9,8},{10,9... | collective-permute-start | bytes 3145736 | tf_op jit(solution)/shard_map/ppermute | solution.py:29
  7.0 1.5 copy.36.choice_ref
  8.5 3.6 %dispatch.1 = (bf16[512,2048]{1,0:T(8,128)(2,1)}, bf16[2,128,512]{2,1,0:T(8,128)(2,1)}) custom-call(s32[1]{0:T(128)} %bitcast.19.rank_ref, bf16[512,2048]{1,0:T(8,128)(2,1)} %rows_ref.1, f32[1,2048]{1,0:T(1,128)} %bitcast.132, s32[512,2]{1,0:T(8,128)} %copy.36.choice_ref), custom_call_target="tpu_custom_call" | custom-call | tf_op jit(solution)/shard_map/dispatch/pallas_call | solution.py:165
  12.1 12.3 %all-to-all-start = ((bf16[64,8,2048]{2,1,0:T(8,128)(2,1)}), bf16[64,8,2048]{2,1,0:T(8,128)(2,1)}, u32[]{:S(2)}, u32[]{:S(2)}) async-start(bf16[64,8,2048]{2,1,0:T(8,128)(2,1)} %bitcast.117), calls=%async_computation | async-start | bytes 4194304 | tf_op jit(solution)/shard_map/all_to_all | solution.py:38
  24.6 2.2 %fusion = f32[512]{0:T(512)S(1)} fusion(bf16[512,2048]{1,0:T(8,128)(2,1)} %param.17), kind=kLoop, calls=%fused_computation.4 | loop fusion | flops 3145216 | bytes 2099200 | tf_op jit(solution)/shard_map/reduce_sum | solution.py:67
  26.8 0.8 fusion.21
  27.7 0.8 convolution_convert_fusion.5
  28.6 0.3 fusion.54
  28.9 0.6 pad_maximum_fusion.3
  29.6 2.0 collective-permute-start
  31.6 3.2 %convolution_convert_fusion.4 = bf16[512,384]{0,1:T(8,128)(2,1)S(1)} fusion(bf16[2048,384]{1,0:T(8,128)(2,1)} %param.21, bf16[512,2048]{1,0:T(8,128)(2,1)} %param.17, f32[2048]{0:T(1024)S(1)} %copy-done.30, f32[512]{0:T(512)S(1)} %add_rsqrt_fusion.1), kind=kOutput, calls=%fused_computation.26 | convolution fusion | flops 809697280 | bytes 4073472 | tf_op jit(solution)/shard_map/dot_general | solution.py:344
  34.9 2.2 %fusion.3 = f32[512]{0:T(512)S(1)} fusion(bf16[512,2048]{1,0:T(8,128)(2,1)} %rows_ref.1), kind=kLoop, calls=%fused_computation.7 | loop fusion | flops 3145216 | bytes 2099200 | tf_op jit(solution)/shard_map/reduce_sum | solution.py:67
  37.2 1.9 fusion.24
  39.1 0.8 fusion.19
  39.9 0.4 copy-done.13
  40.8 0.8 copy_bitcast_fusion.1
  41.7 1.4 convolution_convert_fusion
  43.0 2.0 collective-permute-start.10
  45.2 7.2 %collective-permute-done.5.refs_2_ = bf16[2048,256]{1,0:T(8,128)(2,1)} collective-permute-done((bf16[2048,256]{1,0:T(8,128)(2,1)}, bf16[2048,256]{1,0:T(8,128)(2,1)}, u32[]{:S(2)}, u32[]{:S(2)}) %collective-permute-start.5) | collective-permute-done | bytes 1048608 | tf_op jit(solution)/shard_map/ppermute | solution.py:29
  52.5 0.6 copy.28
  53.3 27.0 %collective-permute-done.11.refs_1_ = bf16[256,256]{1,0:T(8,128)(2,1)S(1)} collective-permute-done((bf16[256,256]{1,0:T(8,128)(2,1)S(1)}, bf16[256,256]{1,0:T(8,128)(2,1)S(1)}, u32[]{:S(2)}, u32[]{:S(2)}) %collective-permute-start.11) | collective-permute-done | bytes 131104 | tf_op jit(solution)/shard_map/ppermute | solution.py:29
  80.4 0.7 copy_bitcast_fusion.5
  81.0 4.9 %collective-permute-done.15.refs_6_ = bf16[256,256]{1,0:T(8,128)(2,1)S(1)} collective-permute-done((bf16[256,256]{1,0:T(8,128)(2,1)S(1)}, bf16[256,256]{1,0:T(8,128)(2,1)S(1)}, u32[]{:S(2)}, u32[]{:S(2)}) %collective-permute-start.15) | collective-permute-done | bytes 131104 | tf_op jit(solution)/shard_map/ppermute | solution.py:29
  85.9 0.6 collective-permute-start.12
  86.5 1.4 collective-permute-start.14
  88.1 3.1 %collective-permute-start.16 = (bf16[256,256]{1,0:T(8,128)(2,1)S(1)}, bf16[256,256]{1,0:T(8,128)(2,1)}, u32[]{:S(2)}, u32[]{:S(2)}) collective-permute-start(bf16[256,256]{1,0:T(8,128)(2,1)S(1)} %collective-permute-done.15.refs_6_), channel_id=1, source_target_pairs={{0,3},{1,0},{2,1},{3,2},{4,7},{5,4},{6,5},{7,6},{8,11},{9,8},{10,9... | collective-permute-start | bytes 393224 | tf_op jit(solution)/shard_map/ppermute | solution.py:29
  91.2 0.7 slice_bitcast_fusion.1
  92.0 0.6 copy.57
  92.6 9.3 %hidden.1.hidden_ref = bf16[512,1024]{1,0:T(8,128)(2,1)} custom-call(bf16[512,2048]{1,0:T(8,128)(2,1)} %bitcast.22.rows_ref, bf16[2048,256]{1,0:T(8,128)(2,1)} %bitcast.124, bf16[2048,256]{1,0:T(8,128)(2,1)} %bitcast.127, bf16[2048,256]{1,0:T(8,128)(2,1)} %collective-permute-done.5.refs_2_, bf16[2048,256]{1,0:T(8,128)(2,1)} %collective-permute-done.6.refs_3_, ...), custom_call_target="tpu_custom_call" | custom-call | tf_op jit(solution)/shard_map/hidden/pallas_call | solution.py:205
  102.0 3.3 %collective-permute-start.18 = (bf16[256,768]{1,0:T(8,128)(2,1)S(1)}, bf16[256,768]{1,0:T(8,128)(2,1)}, u32[]{:S(2)}, u32[]{:S(2)}) collective-permute-start(bf16[256,768]{1,0:T(8,128)(2,1)S(1)} %get-tuple-element.7.refs_0_), channel_id=1, source_target_pairs={{0,3},{1,0},{2,1},{3,2},{4,7},{5,4},{6,5},{7,6},{8,11},{9,8},{10,9... | collective-permute-start | bytes 1179656 | tf_op jit(solution)/shard_map/ppermute | solution.py:29
  105.4 1.9 collective-permute-start.20
  107.3 1.3 collective-permute-start.3
  108.6 3.0 %down.2 = bf16[512,512]{1,0:T(8,128)(2,1)} custom-call(bf16[512,1024]{1,0:T(8,128)(2,1)} %hidden.1.hidden_ref, bf16[256,256]{1,0:T(8,128)(2,1)} %copy-done.15, bf16[256,256]{1,0:T(8,128)(2,1)} %copy-done.17, bf16[256,256]{1,0:T(8,128)(2,1)} %copy-done.19, bf16[256,256]{1,0:T(8,128)(2,1)} %collective-permute-done.13.refs_3_, bf16[256,256]{1,0:T(8,128)(2,1)} %copy-done.14, ...), custom_call_target="tpu_custom_call" | custom-call | tf_op jit(solution)/shard_map/down/pallas_call | solution.py:241
  111.6 12.0 %all-to-all-start.1 = ((bf16[64,8,512]{2,1,0:T(8,128)(2,1)}), bf16[64,8,512]{2,1,0:T(8,128)(2,1)S(1)}, u32[]{:S(2)}, u32[]{:S(2)}) async-start(bf16[64,8,512]{2,1,0:T(8,128)(2,1)} %bitcast.116), calls=%async_computation.1 | async-start | bytes 1048576 | tf_op jit(solution)/shard_map/all_to_all | solution.py:38
  123.7 1.6 fusion.9
  125.4 3.2 %collective-permute-start.22 = (bf16[256,768]{1,0:T(8,128)(2,1)}, bf16[256,768]{1,0:T(8,128)(2,1)}, u32[]{:S(2)}, u32[]{:S(2)}) collective-permute-start(bf16[256,768]{1,0:T(8,128)(2,1)} %collective-permute-done.21.refs_6_), channel_id=1, source_target_pairs={{0,3},{1,0},{2,1},{3,2},{4,7},{5,4},{6,5},{7,6},{8,11},{9,8},{10,9... | collective-permute-start | bytes 1179656 | tf_op jit(solution)/shard_map/ppermute | solution.py:29
  128.6 0.7 fusion.6
  129.4 13.7 %collective-permute-done.19.refs_3_ = bf16[256,768]{1,0:T(8,128)(2,1)} collective-permute-done((bf16[256,768]{1,0:T(8,128)(2,1)}, bf16[256,768]{1,0:T(8,128)(2,1)}, u32[]{:S(2)}, u32[]{:S(2)}) %collective-permute-start.19) | collective-permute-done | bytes 393248 | tf_op jit(solution)/shard_map/ppermute | solution.py:29
  143.1 4.9 %collective-permute-done.22.refs_7_ = bf16[256,768]{1,0:T(8,128)(2,1)} collective-permute-done((bf16[256,768]{1,0:T(8,128)(2,1)}, bf16[256,768]{1,0:T(8,128)(2,1)}, u32[]{:S(2)}, u32[]{:S(2)}) %collective-permute-start.22) | collective-permute-done | bytes 393248 | tf_op jit(solution)/shard_map/ppermute | solution.py:29
  148.0 4.9 %down.3 = bf16[512,1536]{1,0:T(8,128)(2,1)} custom-call(bf16[512,1024]{1,0:T(8,128)(2,1)} %hidden.1.hidden_ref, bf16[256,768]{1,0:T(8,128)(2,1)} %copy-done.12, bf16[256,768]{1,0:T(8,128)(2,1)} %collective-permute-done.17.refs_1_, bf16[256,768]{1,0:T(8,128)(2,1)} %collective-permute-done.18.refs_2_, bf16[256,768]{1,0:T(8,128)(2,1)} %collective-permute-done.19.refs_3_, ...), custom_call_target="tpu_custom_call" | custom-call | tf_op jit(solution)/shard_map/down/pallas_call | solution.py:241
  152.9 0.9 copy-done.9
  153.8 12.0 %all-to-all-start.2 = ((bf16[64,8,1536]{2,1,0:T(8,128)(2,1)}), bf16[64,8,1536]{2,1,0:T(8,128)(2,1)S(1)}, u32[]{:S(2)}, u32[]{:S(2)}) async-start(bf16[64,8,1536]{2,1,0:T(8,128)(2,1)} %bitcast.114), calls=%async_computation.2 | async-start | bytes 3145728 | tf_op jit(solution)/shard_map/all_to_all | solution.py:38
  165.8 2.8 %fusion.16 = bf16[4,128,1,6,64]{1,4,3,0,2:T(8,128)(2,1)S(1)} fusion(f32[4,6,128]{2,1,0:T(8,128)S(1)} %exponential_add_fusion, f32[4,6,128]{2,1,0:T(8,128)S(1)} %broadcast_maximum_fusion, f32[4,256,128,6]{2,1,3,0:T(8,128)} %copy-done.6, pred[4,128,256]{1,2,0:T(8,128)(4,1)S(1)} %broadcast_and_fusion, bf16[4,128,1,64]{1,3,0,2:T(8,128)(2,1)S(1)} %copy-done.21, ...), kind=kOutput, calls=%fused_computation.28 | convolution fusion | flops 105054208 | bytes 3825664 | tf_op jit(solution)/shard_map/nhgqk,nkhd->nqhgd/dot_general | solution.py:120
  168.7 0.3 copy.35
  169.2 0.7 convolution_convert_fusion.2
  169.9 0.5 collective-permute-start.1
  170.4 1.6 convert_add_fusion
  172.1 1.4 copy-done.2
  173.4 0.9 slice.132
  174.3 1.6 collective-permute-start.4
  175.9 20.1 %collective-permute-done.1 = bf16[256,2048]{1,0:T(8,128)(2,1)S(1)} collective-permute-done((bf16[256,2048]{1,0:T(8,128)(2,1)S(1)}, bf16[256,2048]{1,0:T(8,128)(2,1)S(1)}, u32[]{:S(2)}, u32[]{:S(2)}) %collective-permute-start.1) | collective-permute-done | bytes 1048608 | tf_op jit(solution)/shard_map/ppermute | solution.py:33
  196.0 0.7 convert_add_fusion.1
  196.8 1.4 copy-done.3
  198.1 0.9 slice.133
  199.0 3.7 %collective-permute-start.2 = (bf16[128,2048]{1,0:T(8,128)(2,1)}, bf16[128,2048]{1,0:T(8,128)(2,1)}, u32[]{:S(2)}, u32[]{:S(2)}) collective-permute-start(bf16[128,2048]{1,0:T(8,128)(2,1)} %slice.133), channel_id=1, source_target_pairs={{0,3},{1,2},{2,1},{3,0},{4,7},{5,6},{6,5},{7,4},{8,11},{9,10},{10,... | collective-permute-start | bytes 1572872 | tf_op jit(solution)/shard_map/ppermute | solution.py:33
  202.7 0.9 copy.37.weight_ref
  203.5 3.0 %collective-permute-done.4 = bf16[128,2048]{1,0:T(8,128)(2,1)} collective-permute-done((bf16[128,2048]{1,0:T(8,128)(2,1)}, bf16[128,2048]{1,0:T(8,128)(2,1)}, u32[]{:S(2)}, u32[]{:S(2)}) %collective-permute-start.4) | collective-permute-done | bytes 524320 | tf_op jit(solution)/shard_map/ppermute | solution.py:33
  206.5 2.4 %slice_add_fusion.shared_ref = f32[128,2048]{1,0:T(8,128)} fusion(f32[256,2048]{1,0:T(8,128)} %copy-done.2, bf16[128,2048]{1,0:T(8,128)(2,1)} %collective-permute-done.4), kind=kLoop, calls=%fused_computation.36 | loop fusion | flops 524288 | bytes 2621440 | tf_op jit(solution)/shard_map/add | solution.py:62
  208.9 4.5 %collective-permute-done.2 = bf16[128,2048]{1,0:T(8,128)(2,1)} collective-permute-done((bf16[128,2048]{1,0:T(8,128)(2,1)}, bf16[128,2048]{1,0:T(8,128)(2,1)}, u32[]{:S(2)}, u32[]{:S(2)}) %collective-permute-start.2) | collective-permute-done | bytes 524320 | tf_op jit(solution)/shard_map/ppermute | solution.py:33
  213.5 1.9 fusion.22
  215.4 1.2 copy-done.5
  216.6 3.5 %combine.1 = bf16[128,2048]{1,0:T(8,128)(2,1)} custom-call(s32[1]{0:T(128)} %bitcast.19.rank_ref, bf16[2,128,512]{2,1,0:T(8,128)(2,1)} %get-tuple-element.4.pick_ref, f32[512,2]{1,0:T(8,128)} %copy.37.weight_ref, f32[128,2048]{1,0:T(8,128)} %slice_add_fusion.shared_ref, bf16[512,512]{1,0:T(8,128)(2,1)} %bitcast.115, bf16[512,1536]{1,0:T(8,128)(2,1)} %bitcast.113), custom_call_target="tpu_custom_call" | custom-call | tf_op jit(solution)/shard_map/combine/pallas_call | solution.py:271
  (107 shorter events, 1.8 us)
Async XLA Ops:
  0.6 168.5 %copy-start = (bf16[384,2048]{1,0:T(8,128)(2,1)S(1)}, bf16[384,2048]{1,0:T(8,128)(2,1)}, u32[]{:S(2)}) copy-start(bf16[384,2048]{1,0:T(8,128)(2,1)} %param.25) | copy-start | bytes 4718596
  0.6 42.4 %collective-permute-start.8 = (bf16[2048,256]{1,0:T(8,128)(2,1)}, bf16[2048,256]{1,0:T(8,128)(2,1)}, u32[]{:S(2)}, u32[]{:S(2)}) collective-permute-start(bf16[2048,256]{1,0:T(8,128)(2,1)} %bitcast.125), channel_id=1, source_target_pairs={{0,3},{1,0},{2,1},{3,2},{4,7},{5,4},{6,5},{7,6},{8,11},{9,8},{10,9... | collective-permute-start | bytes 3145736 | tf_op jit(solution)/shard_map/ppermute | solution.py:29
  3.7 82.8 %collective-permute-start.6 = (bf16[2048,256]{1,0:T(8,128)(2,1)}, bf16[2048,256]{1,0:T(8,128)(2,1)}, u32[]{:S(2)}, u32[]{:S(2)}) collective-permute-start(bf16[2048,256]{1,0:T(8,128)(2,1)} %bitcast.126), channel_id=1, source_target_pairs={{0,1},{1,2},{2,3},{3,0},{4,5},{5,6},{6,7},{7,4},{8,9},{9,10},{10,1... | collective-permute-start | bytes 3145736 | tf_op jit(solution)/shard_map/ppermute | solution.py:29
  3.7 48.6 %collective-permute-start.5 = (bf16[2048,256]{1,0:T(8,128)(2,1)}, bf16[2048,256]{1,0:T(8,128)(2,1)}, u32[]{:S(2)}, u32[]{:S(2)}) collective-permute-start(bf16[2048,256]{1,0:T(8,128)(2,1)} %bitcast.122), channel_id=1, source_target_pairs={{0,1},{1,2},{2,3},{3,0},{4,5},{5,6},{6,7},{7,4},{8,9},{9,10},{10,1... | collective-permute-start | bytes 3145736 | tf_op jit(solution)/shard_map/ppermute | solution.py:29
  4.3 83.6 %collective-permute-start.7 = (bf16[2048,256]{1,0:T(8,128)(2,1)}, bf16[2048,256]{1,0:T(8,128)(2,1)}, u32[]{:S(2)}, u32[]{:S(2)}) collective-permute-start(bf16[2048,256]{1,0:T(8,128)(2,1)} %bitcast.123), channel_id=1, source_target_pairs={{0,3},{1,0},{2,1},{3,2},{4,7},{5,4},{6,5},{7,6},{8,11},{9,8},{10,9... | collective-permute-start | bytes 3145736 | tf_op jit(solution)/shard_map/ppermute | solution.py:29
  12.1 14.7 %copy-start.28 = (bf16[2048,64]{0,1:T(8,128)(2,1)S(1)}, bf16[2048,64]{0,1:T(8,128)(2,1)}, u32[]{:S(2)}) copy-start(bf16[2048,64]{0,1:T(8,128)(2,1)} %param.22) | copy-start | bytes 786436
  12.1 80.5 %all-to-all-start = ((bf16[64,8,2048]{2,1,0:T(8,128)(2,1)}), bf16[64,8,2048]{2,1,0:T(8,128)(2,1)}, u32[]{:S(2)}, u32[]{:S(2)}) async-start(bf16[64,8,2048]{2,1,0:T(8,128)(2,1)} %bitcast.117), calls=%async_computation | async-start | bytes 4194304 | tf_op jit(solution)/shard_map/all_to_all | solution.py:38
  24.5 2.3 %copy-start.30 = (f32[2048]{0:T(1024)S(1)}, f32[2048]{0:T(1024)}, u32[]{:S(2)}) copy-start(f32[2048]{0:T(1024)} %param.19) | copy-start | bytes 24580
  24.5 2.3 %copy-start.10 = (bf16[512,2048]{1,0:T(8,128)(2,1)S(1)}, bf16[512,2048]{1,0:T(8,128)(2,1)}, u32[]{:S(2)}) copy-start(bf16[512,2048]{1,0:T(8,128)(2,1)} %param.17) | copy-start | bytes 6291460
  26.8 1.0 copy-start.29
  29.6 23.5 %collective-permute-start = (bf16[128,128]{0,1:T(8,128)(2,1)}, bf16[128,128]{0,1:T(8,128)(2,1)}, u32[]{:S(2)}, u32[]{:S(2)}) collective-permute-start(bf16[128,128]{0,1:T(8,128)(2,1)} %pad_maximum_fusion.3), channel_id=1, source_target_pairs={{0,4},{4,8},{8,12},{12,16},{16,20},{20,24},{24,28},{28,32},{32,36}... | collective-permute-start | bytes 98312 | tf_op jit(solution)/shard_map/ppermute | solution.py:24
  34.8 2.4 %copy-start.24 = (f32[2048]{0:T(1024)S(1)}, f32[2048]{0:T(1024)}, u32[]{:S(2)}) copy-start(f32[2048]{0:T(1024)} %param.20) | copy-start | bytes 24580
  34.9 2.3 %copy-start.1 = (bf16[512,2048]{1,0:T(8,128)(2,1)S(1)}, bf16[512,2048]{1,0:T(8,128)(2,1)}, u32[]{:S(2)}) copy-start(bf16[512,2048]{1,0:T(8,128)(2,1)} %rows_ref.1) | copy-start | bytes 6291460
  37.2 1.9 copy-start.27
  39.1 1.2 copy-start.13
  39.9 1.8 copy-start.7
  40.3 45.6 %copy-start.15 = (bf16[256,256]{1,0:T(8,128)(2,1)}, bf16[256,256]{1,0:T(8,128)(2,1)S(1)}, u32[]{:S(2)}) copy-start(bf16[256,256]{1,0:T(8,128)(2,1)S(1)} %get-tuple-element.9.refs_0_) | copy-start | bytes 393220
  40.3 46.2 %copy-start.14 = (bf16[256,256]{1,0:T(8,128)(2,1)}, bf16[256,256]{1,0:T(8,128)(2,1)S(1)}, u32[]{:S(2)}) copy-start(bf16[256,256]{1,0:T(8,128)(2,1)S(1)} %get-tuple-element.8.refs_4_) | copy-start | bytes 393220
  43.0 45.0 %collective-permute-start.10 = (bf16[2048,256]{1,0:T(8,128)(2,1)}, bf16[2048,256]{1,0:T(8,128)(2,1)}, u32[]{:S(2)}, u32[]{:S(2)}) collective-permute-start(bf16[2048,256]{1,0:T(8,128)(2,1)} %collective-permute-done.8.refs_5_), channel_id=1, source_target_pairs={{0,3},{1,0},{2,1},{3,2},{4,7},{5,4},{6,5},{7,6},{8,11},{9,8},{10,9... | collective-permute-start | bytes 3145736 | tf_op jit(solution)/shard_map/ppermute | solution.py:29
  45.1 56.8 %copy-start.12 = (bf16[256,768]{1,0:T(8,128)(2,1)}, bf16[256,768]{1,0:T(8,128)(2,1)S(1)}, u32[]{:S(2)}) copy-start(bf16[256,768]{1,0:T(8,128)(2,1)S(1)} %get-tuple-element.7.refs_0_) | copy-start | bytes 1179652
  45.2 60.2 %copy-start.11 = (bf16[256,768]{1,0:T(8,128)(2,1)}, bf16[256,768]{1,0:T(8,128)(2,1)S(1)}, u32[]{:S(2)}) copy-start(bf16[256,768]{1,0:T(8,128)(2,1)S(1)} %get-tuple-element.6.refs_4_) | copy-start | bytes 1179652
  52.4 40.3 %collective-permute-start.9 = (bf16[2048,256]{1,0:T(8,128)(2,1)}, bf16[2048,256]{1,0:T(8,128)(2,1)}, u32[]{:S(2)}, u32[]{:S(2)}) collective-permute-start(bf16[2048,256]{1,0:T(8,128)(2,1)} %collective-permute-done.5.refs_2_), channel_id=1, source_target_pairs={{0,1},{1,2},{2,3},{3,0},{4,5},{5,6},{6,7},{7,4},{8,9},{9,10},{10,1... | collective-permute-start | bytes 3145736 | tf_op jit(solution)/shard_map/ppermute | solution.py:29
  53.1 27.3 %collective-permute-start.11 = (bf16[256,256]{1,0:T(8,128)(2,1)S(1)}, bf16[256,256]{1,0:T(8,128)(2,1)S(1)}, u32[]{:S(2)}, u32[]{:S(2)}) collective-permute-start(bf16[256,256]{1,0:T(8,128)(2,1)S(1)} %get-tuple-element.9.refs_0_), channel_id=1, source_target_pairs={{0,1},{1,2},{2,3},{3,0},{4,5},{5,6},{6,7},{7,4},{8,9},{9,10},{10,1... | collective-permute-start | bytes 393224 | tf_op jit(solution)/shard_map/ppermute | solution.py:29
  80.3 21.6 %copy-start.17 = (bf16[256,256]{1,0:T(8,128)(2,1)}, bf16[256,256]{1,0:T(8,128)(2,1)S(1)}, u32[]{:S(2)}) copy-start(bf16[256,256]{1,0:T(8,128)(2,1)S(1)} %collective-permute-done.11.refs_1_) | copy-start | bytes 393220
  80.3 5.6 %collective-permute-start.15 = (bf16[256,256]{1,0:T(8,128)(2,1)S(1)}, bf16[256,256]{1,0:T(8,128)(2,1)S(1)}, u32[]{:S(2)}, u32[]{:S(2)}) collective-permute-start(bf16[256,256]{1,0:T(8,128)(2,1)S(1)} %get-tuple-element.8.refs_4_), channel_id=1, source_target_pairs={{0,3},{1,0},{2,1},{3,2},{4,7},{5,4},{6,5},{7,6},{8,11},{9,8},{10,9... | collective-permute-start | bytes 393224 | tf_op jit(solution)/shard_map/ppermute | solution.py:29
  85.9 16.0 %copy-start.18 = (bf16[256,256]{1,0:T(8,128)(2,1)}, bf16[256,256]{1,0:T(8,128)(2,1)S(1)}, u32[]{:S(2)}) copy-start(bf16[256,256]{1,0:T(8,128)(2,1)S(1)} %collective-permute-done.15.refs_6_) | copy-start | bytes 393220
  85.9 16.0 %collective-permute-start.12 = (bf16[256,256]{1,0:T(8,128)(2,1)S(1)}, bf16[256,256]{1,0:T(8,128)(2,1)S(1)}, u32[]{:S(2)}, u32[]{:S(2)}) collective-permute-start(bf16[256,256]{1,0:T(8,128)(2,1)S(1)} %get-tuple-element.9.refs_0_), channel_id=1, source_target_pairs={{0,3},{1,0},{2,1},{3,2},{4,7},{5,4},{6,5},{7,6},{8,11},{9,8},{10,9... | collective-permute-start | bytes 393224 | tf_op jit(solution)/shard_map/ppermute | solution.py:29
  86.5 18.7 %collective-permute-start.14 = (bf16[256,256]{1,0:T(8,128)(2,1)S(1)}, bf16[256,256]{1,0:T(8,128)(2,1)S(1)}, u32[]{:S(2)}, u32[]{:S(2)}) collective-permute-start(bf16[256,256]{1,0:T(8,128)(2,1)S(1)} %get-tuple-element.8.refs_4_), channel_id=1, source_target_pairs={{0,1},{1,2},{2,3},{3,0},{4,5},{5,6},{6,7},{7,4},{8,9},{9,10},{10,1... | collective-permute-start | bytes 393224 | tf_op jit(solution)/shard_map/ppermute | solution.py:29
  88.0 17.4 %collective-permute-start.13 = (bf16[256,256]{1,0:T(8,128)(2,1)S(1)}, bf16[256,256]{1,0:T(8,128)(2,1)}, u32[]{:S(2)}, u32[]{:S(2)}) collective-permute-start(bf16[256,256]{1,0:T(8,128)(2,1)S(1)} %collective-permute-done.11.refs_1_), channel_id=1, source_target_pairs={{0,1},{1,2},{2,3},{3,0},{4,5},{5,6},{6,7},{7,4},{8,9},{9,10},{10,1... | collective-permute-start | bytes 393224 | tf_op jit(solution)/shard_map/ppermute | solution.py:29
  88.1 19.3 %collective-permute-start.16 = (bf16[256,256]{1,0:T(8,128)(2,1)S(1)}, bf16[256,256]{1,0:T(8,128)(2,1)}, u32[]{:S(2)}, u32[]{:S(2)}) collective-permute-start(bf16[256,256]{1,0:T(8,128)(2,1)S(1)} %collective-permute-done.15.refs_6_), channel_id=1, source_target_pairs={{0,3},{1,0},{2,1},{3,2},{4,7},{5,4},{6,5},{7,6},{8,11},{9,8},{10,9... | collective-permute-start | bytes 393224 | tf_op jit(solution)/shard_map/ppermute | solution.py:29
  92.6 32.7 %collective-permute-start.17 = (bf16[256,768]{1,0:T(8,128)(2,1)S(1)}, bf16[256,768]{1,0:T(8,128)(2,1)}, u32[]{:S(2)}, u32[]{:S(2)}) collective-permute-start(bf16[256,768]{1,0:T(8,128)(2,1)S(1)} %get-tuple-element.7.refs_0_), channel_id=1, source_target_pairs={{0,1},{1,2},{2,3},{3,0},{4,5},{5,6},{6,7},{7,4},{8,9},{9,10},{10,1... | collective-permute-start | bytes 1179656 | tf_op jit(solution)/shard_map/ppermute | solution.py:29
  101.9 21.7 %copy-start.23 = (bf16[4,128,1,32]{1,3,0,2:T(8,128)(2,1)S(1)}, bf16[4,128,1,32]{1,3,0,2:T(8,128)(2,1)}, u32[]{:S(2)}) copy-start(bf16[4,128,1,32]{1,3,0,2:T(8,128)(2,1)} %get-tuple-element.32) | copy-start | bytes 98308
  101.9 6.7 %copy-start.19 = (bf16[256,256]{1,0:T(8,128)(2,1)}, bf16[256,256]{1,0:T(8,128)(2,1)S(1)}, u32[]{:S(2)}) copy-start(bf16[256,256]{1,0:T(8,128)(2,1)S(1)} %collective-permute-done.12.refs_2_) | copy-start | bytes 393220
  102.0 21.7 %copy-start.16 = (bf16[4,128,6,32]{1,3,2,0:T(8,128)(2,1)S(1)}, bf16[4,128,6,32]{1,3,2,0:T(8,128)(2,1)}, u32[]{:S(2)}) copy-start(bf16[4,128,6,32]{1,3,2,0:T(8,128)(2,1)} %get-tuple-element.28) | copy-start | bytes 589828
  102.0 27.4 %collective-permute-start.18 = (bf16[256,768]{1,0:T(8,128)(2,1)S(1)}, bf16[256,768]{1,0:T(8,128)(2,1)}, u32[]{:S(2)}, u32[]{:S(2)}) collective-permute-start(bf16[256,768]{1,0:T(8,128)(2,1)S(1)} %get-tuple-element.7.refs_0_), channel_id=1, source_target_pairs={{0,3},{1,0},{2,1},{3,2},{4,7},{5,4},{6,5},{7,6},{8,11},{9,8},{10,9... | collective-permute-start | bytes 1179656 | tf_op jit(solution)/shard_map/ppermute | solution.py:29
  105.3 3.4 %copy-start.20 = (bf16[256,256]{1,0:T(8,128)(2,1)}, bf16[256,256]{1,0:T(8,128)(2,1)S(1)}, u32[]{:S(2)}) copy-start(bf16[256,256]{1,0:T(8,128)(2,1)S(1)} %collective-permute-done.14.refs_5_) | copy-start | bytes 393220
  105.3 20.1 %collective-permute-start.21 = (bf16[256,768]{1,0:T(8,128)(2,1)S(1)}, bf16[256,768]{1,0:T(8,128)(2,1)}, u32[]{:S(2)}, u32[]{:S(2)}) collective-permute-start(bf16[256,768]{1,0:T(8,128)(2,1)S(1)} %get-tuple-element.6.refs_4_), channel_id=1, source_target_pairs={{0,3},{1,0},{2,1},{3,2},{4,7},{5,4},{6,5},{7,6},{8,11},{9,8},{10,9... | collective-permute-start | bytes 1179656 | tf_op jit(solution)/shard_map/ppermute | solution.py:29
  105.4 24.0 %collective-permute-start.20 = (bf16[256,768]{1,0:T(8,128)(2,1)S(1)}, bf16[256,768]{1,0:T(8,128)(2,1)}, u32[]{:S(2)}, u32[]{:S(2)}) collective-permute-start(bf16[256,768]{1,0:T(8,128)(2,1)S(1)} %get-tuple-element.6.refs_4_), channel_id=1, source_target_pairs={{0,1},{1,2},{2,3},{3,0},{4,5},{5,6},{6,7},{7,4},{8,9},{9,10},{10,1... | collective-permute-start | bytes 1179656 | tf_op jit(solution)/shard_map/ppermute | solution.py:29
  107.3 63.1 %collective-permute-start.3 = (bf16[256,2048]{1,0:T(8,128)(2,1)}, bf16[256,2048]{1,0:T(8,128)(2,1)}, u32[]{:S(2)}, u32[]{:S(2)}) collective-permute-start(bf16[256,2048]{1,0:T(8,128)(2,1)} %convolution_convert_fusion), channel_id=1, source_target_pairs={{0,3},{1,2},{2,1},{3,0},{4,7},{5,6},{6,5},{7,4},{8,11},{9,10},{10,... | collective-permute-start | bytes 3145736 | tf_op jit(solution)/shard_map/ppermute | solution.py:33
  111.6 41.3 %all-to-all-start.1 = ((bf16[64,8,512]{2,1,0:T(8,128)(2,1)}), bf16[64,8,512]{2,1,0:T(8,128)(2,1)S(1)}, u32[]{:S(2)}, u32[]{:S(2)}) async-start(bf16[64,8,512]{2,1,0:T(8,128)(2,1)} %bitcast.116), calls=%async_computation.1 | async-start | bytes 1048576 | tf_op jit(solution)/shard_map/all_to_all | solution.py:38
  123.6 1.6 copy-start.26
  125.2 3.4 %copy-start.6 = (f32[4,256,128,6]{2,1,3,0:T(8,128)}, f32[4,256,128,6]{2,1,3,0:T(8,128)S(1)}, u32[]{:S(2)}) copy-start(f32[4,256,128,6]{2,1,3,0:T(8,128)S(1)} %get-tuple-element.27) | copy-start | bytes 9437188
  125.3 17.8 %collective-permute-start.19 = (bf16[256,768]{1,0:T(8,128)(2,1)}, bf16[256,768]{1,0:T(8,128)(2,1)}, u32[]{:S(2)}, u32[]{:S(2)}) collective-permute-start(bf16[256,768]{1,0:T(8,128)(2,1)} %collective-permute-done.17.refs_1_), channel_id=1, source_target_pairs={{0,1},{1,2},{2,3},{3,0},{4,5},{5,6},{6,7},{7,4},{8,9},{9,10},{10,1... | collective-permute-start | bytes 1179656 | tf_op jit(solution)/shard_map/ppermute | solution.py:29
  125.4 22.6 %collective-permute-start.22 = (bf16[256,768]{1,0:T(8,128)(2,1)}, bf16[256,768]{1,0:T(8,128)(2,1)}, u32[]{:S(2)}, u32[]{:S(2)}) collective-permute-start(bf16[256,768]{1,0:T(8,128)(2,1)} %collective-permute-done.21.refs_6_), channel_id=1, source_target_pairs={{0,3},{1,0},{2,1},{3,2},{4,7},{5,4},{6,5},{7,6},{8,11},{9,8},{10,9... | collective-permute-start | bytes 1179656 | tf_op jit(solution)/shard_map/ppermute | solution.py:29
  152.9 12.9 %copy-start.21 = (bf16[4,128,1,64]{1,3,0,2:T(8,128)(2,1)S(1)}, bf16[4,128,1,64]{1,3,0,2:T(8,128)(2,1)}, u32[]{:S(2)}) copy-start(bf16[4,128,1,64]{1,3,0,2:T(8,128)(2,1)} %copy.28) | copy-start | bytes 196612
  152.9 12.9 %copy-start.22 = (bf16[1,8,4,8,128]{4,3,1,2,0:T(8,128)(2,1)S(1)}, bf16[1,8,4,8,128]{4,3,1,2,0:T(8,128)(2,1)}, u32[]{:S(2)}) copy-start(bf16[1,8,4,8,128]{4,3,1,2,0:T(8,128)(2,1)} %copy.57) | copy-start | bytes 196612
  152.9 0.9 copy-start.9
  153.8 61.6 %all-to-all-start.2 = ((bf16[64,8,1536]{2,1,0:T(8,128)(2,1)}), bf16[64,8,1536]{2,1,0:T(8,128)(2,1)S(1)}, u32[]{:S(2)}, u32[]{:S(2)}) async-start(bf16[64,8,1536]{2,1,0:T(8,128)(2,1)} %bitcast.114), calls=%async_computation.2 | async-start | bytes 3145728 | tf_op jit(solution)/shard_map/all_to_all | solution.py:38
  169.0 1.4 copy-start.8
  169.9 26.1 %collective-permute-start.1 = (bf16[256,2048]{1,0:T(8,128)(2,1)S(1)}, bf16[256,2048]{1,0:T(8,128)(2,1)S(1)}, u32[]{:S(2)}, u32[]{:S(2)}) collective-permute-start(bf16[256,2048]{1,0:T(8,128)(2,1)S(1)} %convolution_convert_fusion.2), channel_id=1, source_target_pairs={{0,1},{1,0},{2,3},{3,2},{4,5},{5,4},{6,7},{7,6},{8,9},{9,8},{10,11... | collective-permute-start | bytes 3145736 | tf_op jit(solution)/shard_map/ppermute | solution.py:33
  172.1 1.4 copy-start.2
  174.3 32.2 %collective-permute-start.4 = (bf16[128,2048]{1,0:T(8,128)(2,1)}, bf16[128,2048]{1,0:T(8,128)(2,1)}, u32[]{:S(2)}, u32[]{:S(2)}) collective-permute-start(bf16[128,2048]{1,0:T(8,128)(2,1)} %slice.132), channel_id=1, source_target_pairs={{0,1},{1,0},{2,3},{3,2},{4,5},{5,4},{6,7},{7,6},{8,9},{9,8},{10,11... | collective-permute-start | bytes 1572872 | tf_op jit(solution)/shard_map/ppermute | solution.py:33
  196.0 6.7 %copy-start.25 = (f32[512,2]{0,1:T(2,128)S(1)}, f32[512,2]{0,1:T(2,128)}, u32[]{:S(2)}) copy-start(f32[512,2]{0,1:T(2,128)} %param.27) | copy-start | bytes 12292
  196.7 1.4 copy-start.3
  199.0 14.5 %collective-permute-start.2 = (bf16[128,2048]{1,0:T(8,128)(2,1)}, bf16[128,2048]{1,0:T(8,128)(2,1)}, u32[]{:S(2)}, u32[]{:S(2)}) collective-permute-start(bf16[128,2048]{1,0:T(8,128)(2,1)} %slice.133), channel_id=1, source_target_pairs={{0,3},{1,2},{2,1},{3,0},{4,7},{5,6},{6,5},{7,4},{8,11},{9,10},{10,... | collective-permute-start | bytes 1572872 | tf_op jit(solution)/shard_map/ppermute | solution.py:33
  203.5 9.9 %copy-start.4 = (f32[256,2048]{1,0:T(8,128)S(1)}, f32[256,2048]{1,0:T(8,128)}, u32[]{:S(2)}) copy-start(f32[256,2048]{1,0:T(8,128)} %copy-done.3) | copy-start | bytes 6291460
  215.4 1.2 copy-start.5

commit v3 on v2

--- a/solution.py
+++ b/solution.py
@@ -11,7 +11,7 @@
 HEAD_DIM = 64
 WINDOW = 128
 SEQS = 1
-PIECES = ((256, 256), (768, 768))
+SPANS = (768, 1280)
 
 
 norm_eps = 1e-06
@@ -44,9 +44,8 @@
     ).reshape(slots, width)
 
 
-def halved_sum(rows, weight, own_rows, mask):
+def halved_products(rows, weight, own_rows, mask):
     rank = lax.axis_index("tp")
-    other = mask ^ 2
 
     def product(*masks):
         blocks = [
@@ -55,10 +54,14 @@
         joined = jnp.concatenate(blocks, axis=0)
         return jnp.dot(joined, weight, preferred_element_type=jnp.float32).astype(jnp.bfloat16)
 
-    got = crossed(product(mask, 2), mask)
-    kept = product(0, other)
+    return product(mask, 2), product(0, mask ^ 2)
+
+
+def halved_sum(sent, kept, mask):
+    own_rows = kept.shape[0] // 2
+    got = crossed(sent, mask)
     half = kept.astype(jnp.float32) + got.astype(jnp.float32)
-    last = crossed(half[own_rows:].astype(jnp.bfloat16), other)
+    last = crossed(half[own_rows:].astype(jnp.bfloat16), mask ^ 2)
     return half[:own_rows] + last.astype(jnp.float32)
 
 
@@ -130,30 +133,26 @@
         slots = experts * capacity
         scale = lax.rsqrt(jnp.mean(rows * rows, axis=-1, keepdims=True) + norm_eps)
         normed = (rows * scale * gain_ref[...]).astype(jnp.bfloat16)
-        first = choice_ref[:, 0:1]
-        second = choice_ref[:, 1:2]
-        expert = lax.broadcasted_iota(jnp.int32, (tokens, experts), 1)
+        first = choice_ref[0:1, :]
+        second = choice_ref[1:2, :]
+        expert = lax.broadcasted_iota(jnp.int32, (experts, tokens), 0)
         named = jnp.where((first == expert) | (second == expert), 1.0, 0.0).astype(jnp.bfloat16)
         row = lax.broadcasted_iota(jnp.int32, (tokens, tokens), 0)
         col = lax.broadcasted_iota(jnp.int32, (tokens, tokens), 1)
-        earlier = jnp.where(row > col, 1.0, 0.0).astype(jnp.bfloat16)
-        ranks = jnp.dot(earlier, named, preferred_element_type=jnp.float32)
-        spread_e = lax.broadcasted_iota(jnp.int32, (experts, slots), 0)
-        spread_s = lax.broadcasted_iota(jnp.int32, (experts, slots), 1)
-        spread = jnp.where(spread_s // capacity == spread_e, 1.0, 0.0).astype(jnp.bfloat16)
-        slot_rank = jnp.dot(ranks.astype(jnp.bfloat16), spread, preferred_element_type=jnp.float32)
-        slot = lax.broadcasted_iota(jnp.int32, (tokens, slots), 1)
-        fits = slot_rank.astype(jnp.int32) == slot % capacity
+        earlier = jnp.where(row < col, 1.0, 0.0).astype(jnp.bfloat16)
+        ranks = jnp.dot(named, earlier, preferred_element_type=jnp.float32)
+        slot_rank = jnp.broadcast_to(
+            ranks.astype(jnp.int32)[:, None, :], (experts, capacity, tokens)
+        ).reshape(slots, tokens)
+        slot = lax.broadcasted_iota(jnp.int32, (slots, tokens), 0)
+        fits = slot_rank == slot % capacity
         owner = slot // capacity
         pick_first = jnp.where((owner == first) & fits, 1.0, 0.0).astype(jnp.bfloat16)
         pick_second = jnp.where((owner == second) & fits, 1.0, 0.0).astype(jnp.bfloat16)
         pick_ref[0] = pick_first
         pick_ref[1] = pick_second
-        out_ref[...] = lax.dot_general(
-            pick_first + pick_second,
-            normed,
-            (((0,), (0,)), ((), ())),
-            preferred_element_type=jnp.float32,
+        out_ref[...] = jnp.dot(
+            pick_first + pick_second, normed, preferred_element_type=jnp.float32
         ).astype(jnp.bfloat16)
 
     return body
@@ -170,120 +169,94 @@
             in_specs=[
                 pl.BlockSpec((tokens, width), lambda i, r: (r[0], 0)),
                 pl.BlockSpec((1, width), lambda i, r: (0, 0)),
-                pl.BlockSpec((tokens, 2), lambda i, r: (r[0], 0)),
+                pl.BlockSpec((2, tokens), lambda i, r: (0, r[0])),
             ],
             out_specs=[
                 pl.BlockSpec((slots, width), lambda i, r: (0, 0)),
-                pl.BlockSpec((2, tokens, slots), lambda i, r: (0, 0, 0)),
+                pl.BlockSpec((2, slots, tokens), lambda i, r: (0, 0, 0)),
             ],
         ),
         out_shape=[
             jax.ShapeDtypeStruct((slots, width), jnp.bfloat16),
-            jax.ShapeDtypeStruct((2, tokens, slots), jnp.bfloat16),
+            jax.ShapeDtypeStruct((2, slots, tokens), jnp.bfloat16),
         ],
         name="dispatch",
     )(rank, rows, gain, choice)
 
 
 def hidden_body(rows_ref, *refs):
-    out_ref = refs[-1]
-    weights = refs[:-1]
-    at = 0
-    for gate_ref, up_ref in zip(weights[0::2], weights[1::2]):
-        units = gate_ref.shape[1]
-        gate = jnp.dot(rows_ref[...], gate_ref[...], preferred_element_type=jnp.float32)
-        up = jnp.dot(rows_ref[...], up_ref[...], preferred_element_type=jnp.float32)
-        out_ref[:, at : at + units] = (gate / (1.0 + jnp.exp(-gate)) * up).astype(jnp.bfloat16)
-        at += units
-
-
-def expert_hidden(rows, pairs, steps=2):
+    count = len(refs) - 4
+    sources, (out_ref, rows, held, sems) = refs[:count], refs[count:]
+    units = held.shape[2] // 2
+    copies = [pltpu.make_async_copy(rows_ref, rows, sems.at[count])]
+    for at, source in enumerate(sources):
+        place = held.at[at // 2, :, pl.ds(at % 2 * units, units)]
+        copies.append(pltpu.make_async_copy(source, place, sems.at[at]))
+    for copy in copies:
+        copy.start()
+    copies[0].wait()
+    for index in range(held.shape[0]):
+        copies[1 + 2 * index].wait()
+        copies[2 + 2 * index].wait()
+        both_values = jnp.dot(rows[...], held[index], preferred_element_type=jnp.float32)
+        gate = both_values[:, :units]
+        up = both_values[:, units:]
+        out_ref[:, index * units : (index + 1) * units] = (
+            gate / (1.0 + jnp.exp(-gate)) * up
+        ).astype(jnp.bfloat16)
+
+
+def expert_hidden(rows, pairs):
     slots, width = rows.shape
     units = pairs[0][0].shape[1]
-    block = slots // steps
     flat = [matrix for pair in pairs for matrix in pair]
     return pl.pallas_call(
         hidden_body,
-        grid=(steps,),
-        in_specs=[pl.BlockSpec((block, width), lambda i: (i, 0))]
-        + [pl.BlockSpec((width, units), lambda i: (0, 0))] * len(flat),
-        out_specs=pl.BlockSpec((block, len(pairs) * units), lambda i: (i, 0)),
+        grid=(1,),
+        in_specs=[pl.BlockSpec(memory_space=pl.ANY)] * (1 + len(flat)),
+        out_specs=pl.BlockSpec((slots, len(pairs) * units), lambda i: (0, 0)),
         out_shape=jax.ShapeDtypeStruct((slots, len(pairs) * units), jnp.bfloat16),
-        name="hidden",
+        scratch_shapes=[
+            pltpu.VMEM((slots, width), rows.dtype),
+            pltpu.VMEM((len(pairs), width, 2 * units), rows.dtype),
+            pltpu.SemaphoreType.DMA((len(flat) + 1,)),
+        ],
     )(rows, *flat)
 
 
-def down_body(hidden_ref, *refs):
+def down_body(near_ref, far_hidden_ref, *refs):
     out_ref = refs[-1]
-    weights = refs[:-1]
-    slices = 4
-    units = weights[0].shape[0]
+    whole = refs[:3]
+    far = refs[3:-1]
+    units = whole[0].shape[0]
     at = 0
-    for piece in range(len(weights) // slices):
-        group = weights[piece * slices : (piece + 1) * slices]
-        span = group[0].shape[1]
-        total = 0.0
-        for index, weight in enumerate(group):
+    for part in far:
+        span = part.shape[1]
+        total = jnp.dot(far_hidden_ref[...], part[...], preferred_element_type=jnp.float32)
+        for index in range(3):
             total = total + jnp.dot(
-                hidden_ref[:, index * units : (index + 1) * units],
-                weight[...],
+                near_ref[:, index * units : (index + 1) * units],
+                whole[index][:, at : at + span],
                 preferred_element_type=jnp.float32,
             )
         out_ref[:, at : at + span] = total.astype(jnp.bfloat16)
         at += span
 
 
-def expert_result(hidden, groups, steps=2):
-    slots, units_all = hidden.shape
+def expert_result(near, far, matrices, steps=2):
+    slots = near.shape[0]
     block = slots // steps
-    flat = [matrix for group in groups for matrix in group]
-    width = sum(group[0].shape[1] for group in groups)
+    width = matrices[0].shape[1]
+    by_rows = lambda columns: pl.BlockSpec((block, columns), lambda i: (i, 0))
     return pl.pallas_call(
         down_body,
         grid=(steps,),
-        in_specs=[pl.BlockSpec((block, units_all), lambda i: (i, 0))]
-        + [pl.BlockSpec(matrix.shape, lambda i: (0, 0)) for matrix in flat],
-        out_specs=pl.BlockSpec((block, width), lambda i: (i, 0)),
+        in_specs=[by_rows(near.shape[1]), by_rows(far.shape[1])]
+        + [pl.BlockSpec(matrix.shape, lambda i: (0, 0)) for matrix in matrices],
+        out_specs=by_rows(width),
         out_shape=jax.ShapeDtypeStruct((slots, width), jnp.bfloat16),
         name="down",
-    )(hidden, *flat)
-
-
-def combine_body(rank_ref, pick_ref, weight_ref, shared_ref, *rest):
-    parts = rest[:-1]
-    out_ref = rest[-1]
-    first = weight_ref[:, 0:1]
-    second = weight_ref[:, 1:2]
-    at = 0
-    for part in parts:
-        returned = part[...]
-        span = returned.shape[1]
-        total = first * jnp.dot(pick_ref[0], returned, preferred_element_type=jnp.float32)
-        total = total + second * jnp.dot(pick_ref[1], returned, preferred_element_type=jnp.float32)
-        total = total + shared_ref[:, at : at + span].astype(jnp.float32)
-        out_ref[:, at : at + span] = total.astype(jnp.bfloat16)
-        at += span
-
-
-def combined(rank, pick, weights, shared, parts):
-    tokens, width = shared.shape
-    whole = lambda shape: pl.BlockSpec(shape, lambda i, r: (0,) * len(shape))
-    return pl.pallas_call(
-        combine_body,
-        grid_spec=pltpu.PrefetchScalarGridSpec(
-            num_scalar_prefetch=1,
-            grid=(1,),
-            in_specs=[
-                whole(pick.shape),
-                pl.BlockSpec((tokens, 2), lambda i, r: (r[0], 0)),
-                whole(shared.shape),
-                *[whole(part.shape) for part in parts],
-            ],
-            out_specs=whole((tokens, width)),
-        ),
-        out_shape=jax.ShapeDtypeStruct((tokens, width), jnp.bfloat16),
-        name="combine",
-    )(rank, pick, weights, shared, *parts)
+    )(near, far, *matrices)
 
 
 def both(
@@ -320,23 +293,15 @@
     gate_left, gate_right = shifted(gate, 1), shifted(gate, -1)
     up_left, up_right = shifted(up, 1), shifted(up, -1)
     gate_far, up_far = shifted(gate_left, 1), shifted(up_right, -1)
-    chunks = []
+    near_down = []
     at = 0
-    for spans in PIECES:
-        groups = []
-        for index, span in enumerate(spans):
-            piece = down[:, at : at + span]
-            at += span
-            left, right = shifted(piece, 1), shifted(piece, -1)
-            if index == 0:
-                far = shifted(left, 1)
-            else:
-                far = shifted(right, -1)
-            groups.append((piece, left, right, far))
-        chunks.append(groups)
+    for span in SPANS:
+        piece = down[:, at : at + span]
+        at += span
+        near_down.append((piece, shifted(piece, 1), shifted(piece, -1)))
 
     outgoing, pick = dispatched(
-        rank, expert_input, gain_expert[None, :], expert_choice, own_tokens, capacity, experts_all
+        rank, expert_input, gain_expert[None, :], expert_choice.T, own_tokens, capacity, experts_all
     )
     arrived = exchanged(outgoing, experts_all)
 
@@ -357,6 +322,26 @@
         [rot_keys.reshape(group_rows, key_width)[tail_start:], value_rows[tail_start:]], axis=1
     )
     earlier_pair = from_behind(tail_pair, "ep", 1)
+    normed_rows = rms_scale(expert_input, gain_expert)
+    gate_values = jnp.dot(normed_rows, shared_gate, preferred_element_type=jnp.float32)
+    up_values = jnp.dot(normed_rows, shared_up, preferred_element_type=jnp.float32)
+    hidden = (jax.nn.silu(gate_values) * up_values).astype(jnp.bfloat16)
+    shared_parts = halved_products(hidden, shared_down, own_tokens, 3)
+    arrived, shared_parts = lax.optimization_barrier((arrived, shared_parts))
+    near = expert_hidden(arrived, [(gate, up), (gate_left, up_left), (gate_right, up_right)])
+    far = expert_hidden(arrived, [(gate_far, up_far)])
+    returned = []
+    for number, (piece, left, right) in enumerate(near_down):
+        if number > 0:
+            left, right, earlier_pair, _ = lax.optimization_barrier(
+                (left, right, earlier_pair, result)
+            )
+        middle = left.shape[1] // 2
+        far_left = shifted(left[:, :middle], 1)
+        far_right = shifted(right[:, middle:], -1)
+        result = expert_result(near, far, (piece, left, right, far_left, far_right))
+        returned.append(exchanged(result, experts_all))
+
     prior_keys = earlier_pair[:, :key_width].reshape(WINDOW, -1, HEAD_DIM)
     prior_values = earlier_pair[:, key_width:].reshape(WINDOW, -1, HEAD_DIM)
     attended = attend(
@@ -368,22 +353,23 @@
         first_position,
         sink_logits,
     )
-    mixer_output = halved_sum(attended, output_weight, own_tokens, 1).astype(jnp.bfloat16)
-
-    normed_rows = rms_scale(expert_input, gain_expert)
-    gate_values = jnp.dot(normed_rows, shared_gate, preferred_element_type=jnp.float32)
-    up_values = jnp.dot(normed_rows, shared_up, preferred_element_type=jnp.float32)
-    hidden = (jax.nn.silu(gate_values) * up_values).astype(jnp.bfloat16)
-    shared_part = halved_sum(hidden, shared_down, own_tokens, 3)
-
-    routed_hidden = expert_hidden(
-        arrived, [(gate, up), (gate_left, up_left), (gate_right, up_right), (gate_far, up_far)]
-    )
-    returned = []
-    for groups in chunks:
-        result = expert_result(routed_hidden, groups)
-        returned.append(exchanged(result, experts_all))
-    expert_output = combined(rank, pick, route_weights, shared_part, returned)
+    mixer_parts = halved_products(attended, output_weight, own_tokens, 1)
+    mixer_output = halved_sum(*mixer_parts, 1).astype(jnp.bfloat16)
+    shared_part = halved_sum(*shared_parts, 3)
+
+    own_weights = lax.dynamic_slice_in_dim(route_weights, tp_rank * own_tokens, own_tokens, 0)
+    mixing = jnp.sum(pick.astype(jnp.float32) * own_weights.T[:, None, :], axis=0)
+    mixing = mixing.astype(jnp.bfloat16)
+    done = []
+    at = 0
+    for part in returned:
+        span = part.shape[1]
+        routed = lax.dot_general(
+            mixing, part, (((0,), (0,)), ((), ())), preferred_element_type=jnp.float32
+        )
+        done.append((routed + shared_part[:, at : at + span]).astype(jnp.bfloat16))
+        at += span
+    expert_output = jnp.concatenate(done, axis=1)
     return (mixer_output, expert_output)
 
 

time: 221 us -> 199 us (0.900)
  waiting for transfers between devices: 85.4 us -> 74.3 us
  starting transfers between devices: 67.7 us -> 59.2 us
  local copies, waits for them, and re-layouts: 13.5 us -> 10.6 us
    all_to_all x3, waiting for transfers between devices: 0.01 us -> 14.8 us  [exchanged(): lax.all_to_all(rows.reshape(experts, slots // experts, width), 'ep', spli...]
    ppermute x4, waiting for transfers between devices: 27.6 us -> 13.8 us  [crossed(): lax.ppermute(value, 'tp', [(at, at ^ mask) for at in range(lax.axis_size(...]
    ppermute x18 -> x14, waiting for transfers between devices: 57.8 us -> 45.8 us  [shifted(): lax.ppermute(value, 'tp', [(at, (at + steps) % count) for at in range(cou...]
    ppermute x4, starting transfers between devices: 7.12 us -> 1.95 us  [crossed(): lax.ppermute(value, 'tp', [(at, at ^ mask) for at in range(lax.axis_size(...]
    unnamed x65 -> x69, local copies, waits for them, and re-layouts: 7.78 us -> 3.39 us
    add x1, other arithmetic: 2.43 us -> 0.11 us  [halved_sum(): return half[:own_rows] + last.astype(jnp.float32)]
    ppermute x18 -> x14, starting transfers between devices: 22.2 us -> 20.4 us  [shifted(): lax.ppermute(value, 'tp', [(at, (at + steps) % count) for at in range(cou...]
  transfers between devices with their start and end apart: 26 -> 22, of which waited for: 8 -> 8; matrix products, arithmetic and copies ran while one was open for 16% -> 17% of each run, Pallas kernels for 9% -> 12%
where the time goes in v3:
time: 199 us; the launch traced here: 198 us
  waiting for transfers between devices  74.3 us (37%)
  starting transfers between devices  59.2 us (30%)
  Pallas kernels  22.9 us (12%)
  matrix products  18.3 us (9%)
  other arithmetic  10.9 us (5%)
  local copies, waits for them, and re-layouts  10.6 us (5%)
    ppermute x14, waiting for transfers between devices, shifted(): lax.ppermute(value, 'tp', [(at, (at + steps) % count) for at in range(cou...  45.8 us
    all_to_all x3, starting transfers between devices, exchanged(): lax.all_to_all(rows.reshape(experts, slots // experts, width), 'ep', spli...  35 us
    ppermute x14, starting transfers between devices, shifted(): lax.ppermute(value, 'tp', [(at, (at + steps) % count) for at in range(cou...  20.4 us
    all_to_all x3, waiting for transfers between devices, exchanged(): lax.all_to_all(rows.reshape(experts, slots // experts, width), 'ep', spli...  14.8 us
    ppermute x4, waiting for transfers between devices, crossed(): lax.ppermute(value, 'tp', [(at, at ^ mask) for at in range(lax.axis_size(...  13.8 us
    pallas_call x2, Pallas kernels, expert_hidden(): pl.pallas_call(hidden_body, grid=(1,), in_specs=[pl.BlockSpec(memory_spac...  11.1 us
    pallas_call x2, Pallas kernels, expert_result(): pl.pallas_call(down_body, grid=(steps,), in_specs=[by_rows(near.shape[1])...  8.45 us
    dot_general x4, matrix products, product(): jnp.dot(joined, weight, preferred_element_type=jnp.float32)  6.48 us
  transfers between devices with their start and end apart: 22, of which 8 were waited for; matrix products, arithmetic and copies ran while one was open for 17% of the time, Pallas kernels for 12%

profile of v3, /device:TPU:2, one launch (start us, length us, event | category | flops | bytes accessed | tf_op | source)
XLA Modules:
  0.0 197.6 jit_solution(762682903672127622)
XLA Ops:
  0.6 3.1 %collective-permute-start.6 = (bf16[2048,256]{1,0:T(8,128)(2,1)}, bf16[2048,256]{1,0:T(8,128)(2,1)}, u32[]{:S(2)}, u32[]{:S(2)}) collective-permute-start(bf16[2048,256]{1,0:T(8,128)(2,1)} %bitcast.130), channel_id=1, source_target_pairs={{0,3},{1,0},{2,1},{3,2},{4,7},{5,4},{6,5},{7,6},{8,11},{9,8},{10,9... | collective-permute-start | bytes 3145736 | tf_op jit(solution)/shard_map/ppermute | solution.py:29
  3.7 0.6 collective-permute-start.3
  4.3 2.7 %collective-permute-start.5 = (bf16[2048,256]{1,0:T(8,128)(2,1)}, bf16[2048,256]{1,0:T(8,128)(2,1)}, u32[]{:S(2)}, u32[]{:S(2)}) collective-permute-start(bf16[2048,256]{1,0:T(8,128)(2,1)} %bitcast.128), channel_id=1, source_target_pairs={{0,3},{1,0},{2,1},{3,2},{4,7},{5,4},{6,5},{7,6},{8,11},{9,8},{10,9... | collective-permute-start | bytes 3145736 | tf_op jit(solution)/shard_map/ppermute | solution.py:29
  7.0 3.3 %dispatch.1 = (bf16[512,2048]{1,0:T(8,128)(2,1)}, bf16[2,512,128]{2,1,0:T(8,128)(2,1)}) custom-call(s32[1]{0:T(128)} %bitcast.4.rank_ref, bf16[512,2048]{1,0:T(8,128)(2,1)} %rows_ref.1, f32[1,2048]{1,0:T(1,128)} %bitcast.139, s32[2,512]{1,0:T(2,128)} %bitcast.140), custom_call_target="tpu_custom_call" | custom-call | tf_op jit(solution)/shard_map/dispatch/pallas_call | solution.py:164
  10.3 12.2 %all-to-all-start = ((bf16[64,8,2048]{2,1,0:T(8,128)(2,1)}), bf16[64,8,2048]{2,1,0:T(8,128)(2,1)}, u32[]{:S(2)}, u32[]{:S(2)}) async-start(bf16[64,8,2048]{2,1,0:T(8,128)(2,1)} %bitcast.124), calls=%async_computation | async-start | bytes 4194304 | tf_op jit(solution)/shard_map/all_to_all | solution.py:38
  22.5 1.0 slice.113.refs_0_
  23.7 2.1 %fusion.3 = f32[512]{0:T(512)S(1)} fusion(bf16[512,2048]{1,0:T(8,128)(2,1)} %rows_ref.1), kind=kLoop, calls=%fused_computation.7 | loop fusion | flops 3145216 | bytes 2099200 | tf_op jit(solution)/shard_map/reduce_sum | solution.py:70
  25.9 2.2 %fusion = f32[512]{0:T(512)S(1)} fusion(bf16[512,2048]{1,0:T(8,128)(2,1)} %param.17), kind=kLoop, calls=%fused_computation.4 | loop fusion | flops 3145216 | bytes 2099200 | tf_op jit(solution)/shard_map/reduce_sum | solution.py:70
  28.1 2.6 %convolution_convert_fusion.4 = bf16[512,384]{0,1:T(8,128)(2,1)S(1)} fusion(bf16[2048,384]{1,0:T(8,128)(2,1)} %param.21, bf16[512,2048]{1,0:T(8,128)(2,1)S(1)} %copy-done.7, f32[2048]{0:T(1024)S(1)} %copy-done.32, f32[512]{0:T(512)S(1)} %add_rsqrt_fusion.1), kind=kOutput, calls=%fused_computation.28 | convolution fusion | flops 809697280 | bytes 4073472 | tf_op jit(solution)/shard_map/dot_general | solution.py:309
  30.9 0.3 multiply_cosine_fusion
  31.3 0.8 copy_bitcast_fusion.1
  32.2 0.2 copy-done.1
  32.4 0.2 copy-done.28
  32.6 0.8 fusion.27
  33.3 0.3 copy-done.29
  33.6 0.8 fusion.21
  34.7 1.4 convolution_convert_fusion.2
  36.1 2.6 %fusion.23 = f32[512,1,64]{0,2,1:T(8,128)S(1)} fusion(bf16[2048,64]{0,1:T(8,128)(2,1)S(1)} %copy-done.30, bf16[512,2048]{1,0:T(8,128)(2,1)} %param.17, f32[2048]{0:T(1024)S(1)} %copy-done.32, f32[512]{0:T(512)S(1)} %add_rsqrt_fusion.1), kind=kOutput, calls=%fused_computation.38 | convolution fusion | flops 138477568 | bytes 2500608 | tf_op jit(solution)/shard_map/dot_general | solution.py:310
  38.8 15.0 %collective-permute-done.3.refs_2_ = bf16[2048,256]{1,0:T(8,128)(2,1)} collective-permute-done((bf16[2048,256]{1,0:T(8,128)(2,1)}, bf16[2048,256]{1,0:T(8,128)(2,1)}, u32[]{:S(2)}, u32[]{:S(2)}) %collective-permute-start.3) | collective-permute-done | bytes 1048608 | tf_op jit(solution)/shard_map/ppermute | solution.py:29
  53.8 3.2 %collective-permute-start.8 = (bf16[2048,256]{1,0:T(8,128)(2,1)}, bf16[2048,256]{1,0:T(8,128)(2,1)}, u32[]{:S(2)}, u32[]{:S(2)}) collective-permute-start(bf16[2048,256]{1,0:T(8,128)(2,1)} %collective-permute-done.6.refs_5_), channel_id=1, source_target_pairs={{0,3},{1,0},{2,1},{3,2},{4,7},{5,4},{6,5},{7,6},{8,11},{9,8},{10,9... | collective-permute-start | bytes 3145736 | tf_op jit(solution)/shard_map/ppermute | solution.py:29
  57.0 0.2 broadcast_and_fusion
  57.2 4.9 %collective-permute-done.9.refs_1_ = bf16[256,768]{1,0:T(8,128)(2,1)S(1)} collective-permute-done((bf16[256,768]{1,0:T(8,128)(2,1)S(1)}, bf16[256,768]{1,0:T(8,128)(2,1)S(1)}, u32[]{:S(2)}, u32[]{:S(2)}) %collective-permute-start.9) | collective-permute-done | bytes 393248 | tf_op jit(solution)/shard_map/ppermute | solution.py:29
  62.1 0.7 copy-done.11
  62.8 0.3 fusion.57
  63.3 0.8 convolution_convert_fusion.5
  64.1 21.1 %collective-permute-done.10.refs_2_ = bf16[256,768]{1,0:T(8,128)(2,1)S(1)} collective-permute-done((bf16[256,768]{1,0:T(8,128)(2,1)S(1)}, bf16[256,768]{1,0:T(8,128)(2,1)S(1)}, u32[]{:S(2)}, u32[]{:S(2)}) %collective-permute-start.10) | collective-permute-done | bytes 393248 | tf_op jit(solution)/shard_map/ppermute | solution.py:29
  85.2 3.8 %collective-permute-start.1 = (bf16[256,1280]{1,0:T(8,128)(2,1)S(1)}, bf16[256,1280]{1,0:T(8,128)(2,1)}, u32[]{:S(2)}, u32[]{:S(2)}) collective-permute-start(bf16[256,1280]{1,0:T(8,128)(2,1)S(1)} %slice.109.refs_0_), channel_id=1, source_target_pairs={{0,3},{1,0},{2,1},{3,2},{4,7},{5,4},{6,5},{7,6},{8,11},{9,8},{10,9... | collective-permute-start | bytes 1966088 | tf_op jit(solution)/shard_map/ppermute | solution.py:29
  89.0 0.6 pad_maximum_fusion.4
  89.6 1.4 convolution_convert_fusion.3
  91.1 1.9 collective-permute-start.2
  93.2 3.2 %collective-permute-start.12 = (bf16[256,384]{1,0:T(8,128)(2,1)S(1)}, bf16[256,384]{1,0:T(8,128)(2,1)S(1)}, u32[]{:S(2)}, u32[]{:S(2)}) collective-permute-start(bf16[256,384]{1,0:T(8,128)(2,1)S(1)} %slice.115), channel_id=1, source_target_pairs={{0,3},{1,0},{2,1},{3,2},{4,7},{5,4},{6,5},{7,6},{8,11},{9,8},{10,9... | collective-permute-start | bytes 589832 | tf_op jit(solution)/shard_map/ppermute | solution.py:29
  96.4 0.6 copy_bitcast_fusion.5
  97.0 0.6 copy.26
  97.7 6.9 %shard_map.176.near_ref = bf16[512,768]{1,0:T(8,128)(2,1)} custom-call(bf16[512,2048]{1,0:T(8,128)(2,1)} %bitcast.8.rows_ref, bf16[2048,256]{1,0:T(8,128)(2,1)} %bitcast.129, bf16[2048,256]{1,0:T(8,128)(2,1)} %bitcast.132, bf16[2048,256]{1,0:T(8,128)(2,1)} %collective-permute-done.3.refs_2_, bf16[2048,256]{1,0:T(8,128)(2,1)} %collective-permute-done.4.refs_3_, ...), custom_call_target="tpu_custom_call" | custom-call | tf_op jit(solution)/shard_map/pallas_call | solution.py:213
  104.6 4.2 %shard_map.177.far_hidden_ref = bf16[512,256]{1,0:T(8,128)(2,1)} custom-call(bf16[512,2048]{1,0:T(8,128)(2,1)} %bitcast.8.rows_ref, bf16[2048,256]{1,0:T(8,128)(2,1)} %collective-permute-done.7.refs_0_, bf16[2048,256]{1,0:T(8,128)(2,1)} %collective-permute-done.8.refs_1_), custom_call_target="tpu_custom_call" | custom-call | tf_op jit(solution)/shard_map/pallas_call | solution.py:213
  108.8 0.8 collective-permute-start.15
  109.7 0.7 copy-done.22
  110.3 3.7 %down.2 = bf16[512,768]{1,0:T(8,128)(2,1)} custom-call(bf16[512,768]{1,0:T(8,128)(2,1)} %shard_map.176.near_ref, bf16[512,256]{1,0:T(8,128)(2,1)} %shard_map.177.far_hidden_ref, bf16[256,768]{1,0:T(8,128)(2,1)} %copy-done.9, bf16[256,768]{1,0:T(8,128)(2,1)} %copy-done.11, bf16[256,768]{1,0:T(8,128)(2,1)} %copy-done.13, bf16[256,384]{1,0:T(8,128)(2,1)} %copy-done.21, ...), custom_call_target="tpu_custom_call" | custom-call | tf_op jit(solution)/shard_map/down/pallas_call | solution.py:251
  114.1 12.4 %all-to-all-start.1 = ((bf16[64,8,768]{2,1,0:T(8,128)(2,1)}), bf16[64,8,768]{2,1,0:T(8,128)(2,1)S(1)}, u32[]{:S(2)}, u32[]{:S(2)}) async-start(bf16[64,8,768]{2,1,0:T(8,128)(2,1)} %bitcast.123), calls=%async_computation.1 | async-start | bytes 1572864 | tf_op jit(solution)/shard_map/all_to_all | solution.py:38
  126.5 1.0 slice.106
  127.6 1.0 slice.107
  128.6 3.5 %collective-permute-start.18 = (bf16[256,640]{1,0:T(8,128)(2,1)S(1)}, bf16[256,640]{1,0:T(8,128)(2,1)}, u32[]{:S(2)}, u32[]{:S(2)}) collective-permute-start(bf16[256,640]{1,0:T(8,128)(2,1)S(1)} %slice.107), channel_id=1, source_target_pairs={{0,3},{1,0},{2,1},{3,2},{4,7},{5,4},{6,5},{7,6},{8,11},{9,8},{10,9... | collective-permute-start | bytes 983048 | tf_op jit(solution)/shard_map/ppermute | solution.py:29
  132.1 0.7 slice_bitcast_fusion.1
  133.0 1.7 fusion.9
  134.7 0.7 fusion.6
  135.5 1.0 fusion.17
  136.5 0.3 copy.33
  136.9 1.7 convolution_convert_fusion
  138.7 4.8 %collective-permute-done.17.refs_3_ = bf16[256,640]{1,0:T(8,128)(2,1)} collective-permute-done((bf16[256,640]{1,0:T(8,128)(2,1)S(1)}, bf16[256,640]{1,0:T(8,128)(2,1)}, u32[]{:S(2)}, u32[]{:S(2)}) %collective-permute-start.17) | collective-permute-done | bytes 327712 | tf_op jit(solution)/shard_map/ppermute | solution.py:29
  143.4 4.7 %down.3 = bf16[512,1280]{1,0:T(8,128)(2,1)} custom-call(bf16[512,768]{1,0:T(8,128)(2,1)} %shard_map.176.near_ref, bf16[512,256]{1,0:T(8,128)(2,1)} %shard_map.177.far_hidden_ref, bf16[256,1280]{1,0:T(8,128)(2,1)} %copy-done.5, bf16[256,1280]{1,0:T(8,128)(2,1)} %collective-permute-done.refs_1_, bf16[256,1280]{1,0:T(8,128)(2,1)} %collective-permute-done.1.refs_2_, ...), custom_call_target="tpu_custom_call" | custom-call | tf_op jit(solution)/shard_map/down/pallas_call | solution.py:251
  148.2 1.5 all-to-all-done.1
  149.6 0.9 copy-done.3
  150.5 10.4 %all-to-all-start.2 = ((bf16[64,8,1280]{2,1,0:T(8,128)(2,1)}), bf16[64,8,1280]{2,1,0:T(8,128)(2,1)S(1)}, u32[]{:S(2)}, u32[]{:S(2)}) async-start(bf16[64,8,1280]{2,1,0:T(8,128)(2,1)} %bitcast.122), calls=%async_computation.2 | async-start | bytes 2621440 | tf_op jit(solution)/shard_map/all_to_all | solution.py:38
  160.9 1.9 convert_add_fusion
  163.1 0.7 fusion.71
  163.8 2.0 convert_add_fusion.1
  165.8 1.0 collective-permute-start.14
  166.9 10.1 %collective-permute-done.16 = bf16[128,2048]{1,0:T(8,128)(2,1)S(1)} collective-permute-done((bf16[128,2048]{1,0:T(8,128)(2,1)S(1)}, bf16[128,2048]{1,0:T(8,128)(2,1)S(1)}, u32[]{:S(2)}, u32[]{:S(2)}) %collective-permute-start.16) | collective-permute-done | bytes 524320 | tf_op jit(solution)/shard_map/ppermute | solution.py:33
  177.1 0.3 fusion.20
  177.4 3.7 %collective-permute-done.14 = bf16[128,2048]{1,0:T(8,128)(2,1)S(1)} collective-permute-done((bf16[128,2048]{1,0:T(8,128)(2,1)S(1)}, bf16[128,2048]{1,0:T(8,128)(2,1)S(1)}, u32[]{:S(2)}, u32[]{:S(2)}) %collective-permute-start.14) | collective-permute-done | bytes 524320 | tf_op jit(solution)/shard_map/ppermute | solution.py:33
  181.1 0.9 fusion.24
  182.0 13.3 %all-to-all-done.2 = bf16[64,8,1280]{2,1,0:T(8,128)(2,1)S(1)} async-done(((bf16[64,8,1280]{2,1,0:T(8,128)(2,1)}), bf16[64,8,1280]{2,1,0:T(8,128)(2,1)S(1)}, u32[]{:S(2)}, u32[]{:S(2)}) %all-to-all-start.2) | async-done | bytes 1310752 | tf_op jit(solution)/shard_map/all_to_all | solution.py:38
  195.3 1.4 fusion.8
  196.8 0.8 pad_maximum_fusion
  (113 shorter events, 1.8 us)
Async XLA Ops:
  0.6 136.3 %copy-start = (bf16[384,2048]{1,0:T(8,128)(2,1)S(1)}, bf16[384,2048]{1,0:T(8,128)(2,1)}, u32[]{:S(2)}) copy-start(bf16[384,2048]{1,0:T(8,128)(2,1)} %param.25) | copy-start | bytes 4718596
  0.6 53.1 %collective-permute-start.6 = (bf16[2048,256]{1,0:T(8,128)(2,1)}, bf16[2048,256]{1,0:T(8,128)(2,1)}, u32[]{:S(2)}, u32[]{:S(2)}) collective-permute-start(bf16[2048,256]{1,0:T(8,128)(2,1)} %bitcast.130), channel_id=1, source_target_pairs={{0,3},{1,0},{2,1},{3,2},{4,7},{5,4},{6,5},{7,6},{8,11},{9,8},{10,9... | collective-permute-start | bytes 3145736 | tf_op jit(solution)/shard_map/ppermute | solution.py:29
  3.7 81.5 %collective-permute-start.4 = (bf16[2048,256]{1,0:T(8,128)(2,1)}, bf16[2048,256]{1,0:T(8,128)(2,1)}, u32[]{:S(2)}, u32[]{:S(2)}) collective-permute-start(bf16[2048,256]{1,0:T(8,128)(2,1)} %bitcast.131), channel_id=1, source_target_pairs={{0,1},{1,2},{2,3},{3,0},{4,5},{5,6},{6,7},{7,4},{8,9},{9,10},{10,1... | collective-permute-start | bytes 3145736 | tf_op jit(solution)/shard_map/ppermute | solution.py:29
  3.7 50.0 %collective-permute-start.3 = (bf16[2048,256]{1,0:T(8,128)(2,1)}, bf16[2048,256]{1,0:T(8,128)(2,1)}, u32[]{:S(2)}, u32[]{:S(2)}) collective-permute-start(bf16[2048,256]{1,0:T(8,128)(2,1)} %bitcast.127), channel_id=1, source_target_pairs={{0,1},{1,2},{2,3},{3,0},{4,5},{5,6},{6,7},{7,4},{8,9},{9,10},{10,1... | collective-permute-start | bytes 3145736 | tf_op jit(solution)/shard_map/ppermute | solution.py:29
  4.3 86.8 %collective-permute-start.5 = (bf16[2048,256]{1,0:T(8,128)(2,1)}, bf16[2048,256]{1,0:T(8,128)(2,1)}, u32[]{:S(2)}, u32[]{:S(2)}) collective-permute-start(bf16[2048,256]{1,0:T(8,128)(2,1)} %bitcast.128), channel_id=1, source_target_pairs={{0,3},{1,0},{2,1},{3,2},{4,7},{5,4},{6,5},{7,6},{8,11},{9,8},{10,9... | collective-permute-start | bytes 3145736 | tf_op jit(solution)/shard_map/ppermute | solution.py:29
  10.3 87.3 %all-to-all-start = ((bf16[64,8,2048]{2,1,0:T(8,128)(2,1)}), bf16[64,8,2048]{2,1,0:T(8,128)(2,1)}, u32[]{:S(2)}, u32[]{:S(2)}) async-start(bf16[64,8,2048]{2,1,0:T(8,128)(2,1)} %bitcast.124), calls=%async_computation | async-start | bytes 4194304 | tf_op jit(solution)/shard_map/all_to_all | solution.py:38
  23.6 38.5 %copy-start.9 = (bf16[256,768]{1,0:T(8,128)(2,1)}, bf16[256,768]{1,0:T(8,128)(2,1)S(1)}, u32[]{:S(2)}) copy-start(bf16[256,768]{1,0:T(8,128)(2,1)S(1)} %slice.113.refs_0_) | copy-start | bytes 1179652
  23.6 4.5 %copy-start.32 = (f32[2048]{0:T(1024)S(1)}, f32[2048]{0:T(1024)}, u32[]{:S(2)}) copy-start(f32[2048]{0:T(1024)} %param.19) | copy-start | bytes 24580
  23.6 38.5 %collective-permute-start.9 = (bf16[256,768]{1,0:T(8,128)(2,1)S(1)}, bf16[256,768]{1,0:T(8,128)(2,1)S(1)}, u32[]{:S(2)}, u32[]{:S(2)}) collective-permute-start(bf16[256,768]{1,0:T(8,128)(2,1)S(1)} %slice.113.refs_0_), channel_id=1, source_target_pairs={{0,1},{1,2},{2,3},{3,0},{4,5},{5,6},{6,7},{7,4},{8,9},{9,10},{10,1... | collective-permute-start | bytes 1179656 | tf_op jit(solution)/shard_map/ppermute | solution.py:29
  25.9 2.3 %copy-start.7 = (bf16[512,2048]{1,0:T(8,128)(2,1)S(1)}, bf16[512,2048]{1,0:T(8,128)(2,1)}, u32[]{:S(2)}) copy-start(bf16[512,2048]{1,0:T(8,128)(2,1)} %param.17) | copy-start | bytes 6291460
  30.8 1.6 copy-start.1
  30.8 1.6 copy-start.26
  30.8 1.8 copy-start.28
  32.6 1.0 copy-start.29
  33.6 1.0 copy-start.6
  33.6 2.5 %copy-start.30 = (bf16[2048,64]{0,1:T(8,128)(2,1)S(1)}, bf16[2048,64]{0,1:T(8,128)(2,1)}, u32[]{:S(2)}) copy-start(bf16[2048,64]{0,1:T(8,128)(2,1)} %param.22) | copy-start | bytes 786436
  36.1 27.1 %copy-start.10 = (bf16[1,256,2048]{2,1,0:T(8,128)(2,1)S(1)}, bf16[1,256,2048]{2,1,0:T(8,128)(2,1)}, u32[]{:S(2)}) copy-start(bf16[1,256,2048]{2,1,0:T(8,128)(2,1)} %param.30) | copy-start | bytes 3145732
  36.1 27.2 %copy-start.8 = (bf16[512,2048]{1,0:T(8,128)(2,1)S(1)}, bf16[512,2048]{1,0:T(8,128)(2,1)}, u32[]{:S(2)}) copy-start(bf16[512,2048]{1,0:T(8,128)(2,1)} %param.17) | copy-start | bytes 6291460
  36.1 27.2 %copy-start.31 = (bf16[2048,64]{0,1:T(8,128)(2,1)S(1)}, bf16[2048,64]{0,1:T(8,128)(2,1)}, u32[]{:S(2)}) copy-start(bf16[2048,64]{0,1:T(8,128)(2,1)} %param.23) | copy-start | bytes 786436
  36.1 27.2 %copy-start.33 = (f32[2048]{0:T(1024)S(1)}, f32[2048]{0:T(1024)}, u32[]{:S(2)}) copy-start(f32[2048]{0:T(1024)} %param.19) | copy-start | bytes 24580
  53.8 39.3 %collective-permute-start.7 = (bf16[2048,256]{1,0:T(8,128)(2,1)}, bf16[2048,256]{1,0:T(8,128)(2,1)}, u32[]{:S(2)}, u32[]{:S(2)}) collective-permute-start(bf16[2048,256]{1,0:T(8,128)(2,1)} %collective-permute-done.3.refs_2_), channel_id=1, source_target_pairs={{0,1},{1,2},{2,3},{3,0},{4,5},{5,6},{6,7},{7,4},{8,9},{9,10},{10,1... | collective-permute-start | bytes 3145736 | tf_op jit(solution)/shard_map/ppermute | solution.py:29
  53.8 39.4 %collective-permute-start.8 = (bf16[2048,256]{1,0:T(8,128)(2,1)}, bf16[2048,256]{1,0:T(8,128)(2,1)}, u32[]{:S(2)}, u32[]{:S(2)}) collective-permute-start(bf16[2048,256]{1,0:T(8,128)(2,1)} %collective-permute-done.6.refs_5_), channel_id=1, source_target_pairs={{0,3},{1,0},{2,1},{3,2},{4,7},{5,4},{6,5},{7,6},{8,11},{9,8},{10,9... | collective-permute-start | bytes 3145736 | tf_op jit(solution)/shard_map/ppermute | solution.py:29
  62.1 0.7 copy-start.11
  62.1 23.1 %collective-permute-start.10 = (bf16[256,768]{1,0:T(8,128)(2,1)S(1)}, bf16[256,768]{1,0:T(8,128)(2,1)S(1)}, u32[]{:S(2)}, u32[]{:S(2)}) collective-permute-start(bf16[256,768]{1,0:T(8,128)(2,1)S(1)} %slice.113.refs_0_), channel_id=1, source_target_pairs={{0,3},{1,0},{2,1},{3,2},{4,7},{5,4},{6,5},{7,6},{8,11},{9,8},{10,9... | collective-permute-start | bytes 1179656 | tf_op jit(solution)/shard_map/ppermute | solution.py:29
  63.2 33.2 %copy-start.14 = (bf16[512,1,32]{0,2,1:T(8,128)(2,1)}, bf16[512,1,32]{0,2,1:T(8,128)(2,1)S(1)}, u32[]{:S(2)}) copy-start(bf16[512,1,32]{0,2,1:T(8,128)(2,1)S(1)} %get-tuple-element.24) | copy-start | bytes 98308
  63.2 33.2 %copy-start.16 = (bf16[512,1,32]{0,2,1:T(8,128)(2,1)}, bf16[512,1,32]{0,2,1:T(8,128)(2,1)S(1)}, u32[]{:S(2)}) copy-start(bf16[512,1,32]{0,2,1:T(8,128)(2,1)S(1)} %get-tuple-element.25) | copy-start | bytes 98308
  63.3 25.7 %copy-start.5 = (bf16[256,1280]{1,0:T(8,128)(2,1)}, bf16[256,1280]{1,0:T(8,128)(2,1)S(1)}, u32[]{:S(2)}) copy-start(bf16[256,1280]{1,0:T(8,128)(2,1)S(1)} %slice.109.refs_0_) | copy-start | bytes 1966084
  63.3 27.8 %copy-start.12 = (bf16[256,768]{1,0:T(8,128)(2,1)S(1)}, bf16[256,768]{1,0:T(8,128)(2,1)}, u32[]{:S(2)}) copy-start(bf16[256,768]{1,0:T(8,128)(2,1)} %copy-done.11) | copy-start | bytes 1179652
  64.1 40.5 %copy-start.18 = (bf16[512,64]{0,1:T(8,128)(2,1)}, bf16[512,64]{0,1:T(8,128)(2,1)S(1)}, u32[]{:S(2)}) copy-start(bf16[512,64]{0,1:T(8,128)(2,1)S(1)} %convolution_convert_fusion.5) | copy-start | bytes 196612
  85.2 5.8 %copy-start.13 = (bf16[256,768]{1,0:T(8,128)(2,1)}, bf16[256,768]{1,0:T(8,128)(2,1)S(1)}, u32[]{:S(2)}) copy-start(bf16[256,768]{1,0:T(8,128)(2,1)S(1)} %collective-permute-done.10.refs_2_) | copy-start | bytes 1179652
  85.2 41.2 %collective-permute-start = (bf16[256,1280]{1,0:T(8,128)(2,1)S(1)}, bf16[256,1280]{1,0:T(8,128)(2,1)}, u32[]{:S(2)}, u32[]{:S(2)}) collective-permute-start(bf16[256,1280]{1,0:T(8,128)(2,1)S(1)} %slice.109.refs_0_), channel_id=1, source_target_pairs={{0,1},{1,2},{2,3},{3,0},{4,5},{5,6},{6,7},{7,4},{8,9},{9,10},{10,1... | collective-permute-start | bytes 1966088 | tf_op jit(solution)/shard_map/ppermute | solution.py:29
  85.2 41.2 %collective-permute-start.1 = (bf16[256,1280]{1,0:T(8,128)(2,1)S(1)}, bf16[256,1280]{1,0:T(8,128)(2,1)}, u32[]{:S(2)}, u32[]{:S(2)}) collective-permute-start(bf16[256,1280]{1,0:T(8,128)(2,1)S(1)} %slice.109.refs_0_), channel_id=1, source_target_pairs={{0,3},{1,0},{2,1},{3,2},{4,7},{5,4},{6,5},{7,6},{8,11},{9,8},{10,9... | collective-permute-start | bytes 1966088 | tf_op jit(solution)/shard_map/ppermute | solution.py:29
  91.1 35.4 %collective-permute-start.2 = (bf16[128,128]{0,1:T(8,128)(2,1)}, bf16[128,128]{0,1:T(8,128)(2,1)}, u32[]{:S(2)}, u32[]{:S(2)}) collective-permute-start(bf16[128,128]{0,1:T(8,128)(2,1)} %pad_maximum_fusion.4), channel_id=1, source_target_pairs={{0,4},{4,8},{8,12},{12,16},{16,20},{20,24},{24,28},{28,32},{32,36}... | collective-permute-start | bytes 98312 | tf_op jit(solution)/shard_map/ppermute | solution.py:24
  93.1 15.8 %collective-permute-start.11 = (bf16[256,384]{1,0:T(8,128)(2,1)S(1)}, bf16[256,384]{1,0:T(8,128)(2,1)S(1)}, u32[]{:S(2)}, u32[]{:S(2)}) collective-permute-start(bf16[256,384]{1,0:T(8,128)(2,1)S(1)} %slice.114), channel_id=1, source_target_pairs={{0,1},{1,2},{2,3},{3,0},{4,5},{5,6},{6,7},{7,4},{8,9},{9,10},{10,1... | collective-permute-start | bytes 589832 | tf_op jit(solution)/shard_map/ppermute | solution.py:29
  93.2 16.5 %collective-permute-start.12 = (bf16[256,384]{1,0:T(8,128)(2,1)S(1)}, bf16[256,384]{1,0:T(8,128)(2,1)S(1)}, u32[]{:S(2)}, u32[]{:S(2)}) collective-permute-start(bf16[256,384]{1,0:T(8,128)(2,1)S(1)} %slice.115), channel_id=1, source_target_pairs={{0,3},{1,0},{2,1},{3,2},{4,7},{5,4},{6,5},{7,6},{8,11},{9,8},{10,9... | collective-permute-start | bytes 589832 | tf_op jit(solution)/shard_map/ppermute | solution.py:29
  108.8 0.8 copy-start.21
  108.8 52.1 %collective-permute-start.15 = (bf16[256,2048]{1,0:T(8,128)(2,1)}, bf16[256,2048]{1,0:T(8,128)(2,1)}, u32[]{:S(2)}, u32[]{:S(2)}) collective-permute-start(bf16[256,2048]{1,0:T(8,128)(2,1)} %convolution_convert_fusion.3), channel_id=1, source_target_pairs={{0,3},{1,2},{2,1},{3,0},{4,7},{5,6},{6,5},{7,4},{8,11},{9,10},{10,... | collective-permute-start | bytes 3145736 | tf_op jit(solution)/shard_map/ppermute | solution.py:33
  109.7 0.7 copy-start.22
  114.1 18.8 %copy-start.15 = (bf16[512,1,32]{0,2,1:T(8,128)(2,1)S(1)}, bf16[512,1,32]{0,2,1:T(8,128)(2,1)}, u32[]{:S(2)}) copy-start(bf16[512,1,32]{0,2,1:T(8,128)(2,1)} %copy-done.14) | copy-start | bytes 98308
  114.1 18.8 %copy-start.17 = (bf16[512,1,32]{0,2,1:T(8,128)(2,1)S(1)}, bf16[512,1,32]{0,2,1:T(8,128)(2,1)}, u32[]{:S(2)}) copy-start(bf16[512,1,32]{0,2,1:T(8,128)(2,1)} %copy-done.16) | copy-start | bytes 98308
  114.1 18.8 %copy-start.19 = (bf16[512,64]{0,1:T(8,128)(2,1)S(1)}, bf16[512,64]{0,1:T(8,128)(2,1)}, u32[]{:S(2)}) copy-start(bf16[512,64]{0,1:T(8,128)(2,1)} %copy-done.18) | copy-start | bytes 196612
  114.1 18.9 %copy-start.24 = (bf16[4,128,1,32]{1,3,0,2:T(8,128)(2,1)S(1)}, bf16[4,128,1,32]{1,3,0,2:T(8,128)(2,1)}, u32[]{:S(2)}) copy-start(bf16[4,128,1,32]{1,3,0,2:T(8,128)(2,1)} %get-tuple-element.40) | copy-start | bytes 98308
  114.1 18.9 %copy-start.25 = (bf16[4,128,1,32]{1,3,0,2:T(8,128)(2,1)S(1)}, bf16[4,128,1,32]{1,3,0,2:T(8,128)(2,1)}, u32[]{:S(2)}) copy-start(bf16[4,128,1,32]{1,3,0,2:T(8,128)(2,1)} %get-tuple-element.41) | copy-start | bytes 98308
  114.1 35.5 %all-to-all-start.1 = ((bf16[64,8,768]{2,1,0:T(8,128)(2,1)}), bf16[64,8,768]{2,1,0:T(8,128)(2,1)S(1)}, u32[]{:S(2)}, u32[]{:S(2)}) async-start(bf16[64,8,768]{2,1,0:T(8,128)(2,1)} %bitcast.123), calls=%async_computation.1 | async-start | bytes 1572864 | tf_op jit(solution)/shard_map/all_to_all | solution.py:38
  127.5 15.9 %collective-permute-start.17 = (bf16[256,640]{1,0:T(8,128)(2,1)S(1)}, bf16[256,640]{1,0:T(8,128)(2,1)}, u32[]{:S(2)}, u32[]{:S(2)}) collective-permute-start(bf16[256,640]{1,0:T(8,128)(2,1)S(1)} %slice.106), channel_id=1, source_target_pairs={{0,1},{1,2},{2,3},{3,0},{4,5},{5,6},{6,7},{7,4},{8,9},{9,10},{10,1... | collective-permute-start | bytes 983048 | tf_op jit(solution)/shard_map/ppermute | solution.py:29
  128.6 14.8 %collective-permute-start.18 = (bf16[256,640]{1,0:T(8,128)(2,1)S(1)}, bf16[256,640]{1,0:T(8,128)(2,1)}, u32[]{:S(2)}, u32[]{:S(2)}) collective-permute-start(bf16[256,640]{1,0:T(8,128)(2,1)S(1)} %slice.107), channel_id=1, source_target_pairs={{0,3},{1,0},{2,1},{3,2},{4,7},{5,4},{6,5},{7,6},{8,11},{9,8},{10,9... | collective-permute-start | bytes 983048 | tf_op jit(solution)/shard_map/ppermute | solution.py:29
  132.9 1.7 copy-start.27
  134.6 0.9 copy-start.23
  138.7 25.1 %collective-permute-start.13 = (bf16[256,2048]{1,0:T(8,128)(2,1)}, bf16[256,2048]{1,0:T(8,128)(2,1)}, u32[]{:S(2)}, u32[]{:S(2)}) collective-permute-start(bf16[256,2048]{1,0:T(8,128)(2,1)} %convolution_convert_fusion), channel_id=1, source_target_pairs={{0,1},{1,0},{2,3},{3,2},{4,5},{5,4},{6,7},{7,6},{8,9},{9,8},{10,11... | collective-permute-start | bytes 3145736 | tf_op jit(solution)/shard_map/ppermute | solution.py:33
  149.6 0.9 copy-start.3
  150.5 44.8 %all-to-all-start.2 = ((bf16[64,8,1280]{2,1,0:T(8,128)(2,1)}), bf16[64,8,1280]{2,1,0:T(8,128)(2,1)S(1)}, u32[]{:S(2)}, u32[]{:S(2)}) async-start(bf16[64,8,1280]{2,1,0:T(8,128)(2,1)} %bitcast.122), calls=%async_computation.2 | async-start | bytes 2621440 | tf_op jit(solution)/shard_map/all_to_all | solution.py:38
  160.9 2.8 %copy-start.20 = (bf16[2,512,128]{2,1,0:T(8,128)(2,1)S(1)}, bf16[2,512,128]{2,1,0:T(8,128)(2,1)}, u32[]{:S(2)}) copy-start(bf16[2,512,128]{2,1,0:T(8,128)(2,1)} %get-tuple-element.13) | copy-start | bytes 786436
  163.0 14.0 %collective-permute-start.16 = (bf16[128,2048]{1,0:T(8,128)(2,1)S(1)}, bf16[128,2048]{1,0:T(8,128)(2,1)S(1)}, u32[]{:S(2)}, u32[]{:S(2)}) collective-permute-start(bf16[128,2048]{1,0:T(8,128)(2,1)S(1)} %slice.150), channel_id=1, source_target_pairs={{0,1},{1,0},{2,3},{3,2},{4,5},{5,4},{6,7},{7,6},{8,9},{9,8},{10,11... | collective-permute-start | bytes 1572872 | tf_op jit(solution)/shard_map/ppermute | solution.py:33
  165.8 11.3 %copy-start.4 = (bf16[64,8,768]{2,1,0:T(8,128)(2,1)S(1)}, bf16[64,8,768]{2,1,0:T(8,128)(2,1)}, u32[]{:S(2)}) copy-start(bf16[64,8,768]{2,1,0:T(8,128)(2,1)} %copy-done.3) | copy-start | bytes 2359300
  165.8 15.2 %collective-permute-start.14 = (bf16[128,2048]{1,0:T(8,128)(2,1)S(1)}, bf16[128,2048]{1,0:T(8,128)(2,1)S(1)}, u32[]{:S(2)}, u32[]{:S(2)}) collective-permute-start(bf16[128,2048]{1,0:T(8,128)(2,1)S(1)} %slice.151), channel_id=1, source_target_pairs={{0,3},{1,2},{2,1},{3,0},{4,7},{5,6},{6,5},{7,4},{8,11},{9,10},{10,... | collective-permute-start | bytes 1572872 | tf_op jit(solution)/shard_map/ppermute | solution.py:33
  177.1 4.0 %copy-start.2 = (f32[128,2048]{1,0:T(8,128)}, f32[128,2048]{1,0:T(8,128)S(1)}, u32[]{:S(2)}) copy-start(f32[128,2048]{1,0:T(8,128)S(1)} %slice_add_fusion) | copy-start | bytes 3145732

commit v4 on v3

--- a/solution.py
+++ b/solution.py
@@ -224,39 +224,46 @@
     )(rows, *flat)
 
 
-def down_body(near_ref, far_hidden_ref, *refs):
-    out_ref = refs[-1]
-    whole = refs[:3]
-    far = refs[3:-1]
-    units = whole[0].shape[0]
-    at = 0
-    for part in far:
-        span = part.shape[1]
-        total = jnp.dot(far_hidden_ref[...], part[...], preferred_element_type=jnp.float32)
-        for index in range(3):
-            total = total + jnp.dot(
-                near_ref[:, index * units : (index + 1) * units],
-                whole[index][:, at : at + span],
-                preferred_element_type=jnp.float32,
-            )
-        out_ref[:, at : at + span] = total.astype(jnp.bfloat16)
-        at += span
+def down_kernel(counts):
+    def body(near_ref, far_ref, *refs):
+        out_ref = refs[-1]
+        units = refs[0].shape[0]
+        halves = max(counts)
+        span = out_ref.shape[1] // halves
+        for half in range(halves):
+            total = 0.0
+            first = 0
+            for index, count in enumerate(counts):
+                if index < 3:
+                    hidden = near_ref[:, index * units : (index + 1) * units]
+                else:
+                    hidden = far_ref[...]
+                if count == halves:
+                    piece = refs[first + half][...]
+                else:
+                    piece = refs[first][:, half * span : (half + 1) * span]
+                total = total + jnp.dot(hidden, piece, preferred_element_type=jnp.float32)
+                first += count
+            out_ref[:, half * span : (half + 1) * span] = total.astype(jnp.bfloat16)
+
+    return body
 
 
 def expert_result(near, far, matrices, steps=2):
     slots = near.shape[0]
     block = slots // steps
-    width = matrices[0].shape[1]
+    width = sum(piece.shape[1] for piece in matrices[0])
+    flat = [piece for pieces in matrices for piece in pieces]
     by_rows = lambda columns: pl.BlockSpec((block, columns), lambda i: (i, 0))
     return pl.pallas_call(
-        down_body,
+        down_kernel([len(pieces) for pieces in matrices]),
         grid=(steps,),
         in_specs=[by_rows(near.shape[1]), by_rows(far.shape[1])]
-        + [pl.BlockSpec(matrix.shape, lambda i: (0, 0)) for matrix in matrices],
+        + [pl.BlockSpec(piece.shape, lambda i: (0, 0)) for piece in flat],
         out_specs=by_rows(width),
         out_shape=jax.ShapeDtypeStruct((slots, width), jnp.bfloat16),
         name="down",
-    )(near, far, *matrices)
+    )(near, far, *flat)
 
 
 def both(
@@ -293,12 +300,18 @@
     gate_left, gate_right = shifted(gate, 1), shifted(gate, -1)
     up_left, up_right = shifted(up, 1), shifted(up, -1)
     gate_far, up_far = shifted(gate_left, 1), shifted(up_right, -1)
-    near_down = []
-    at = 0
-    for span in SPANS:
-        piece = down[:, at : at + span]
-        at += span
-        near_down.append((piece, shifted(piece, 1), shifted(piece, -1)))
+    first, second = SPANS
+    half = first // 2
+    piece = down[:, :first]
+    left, right = shifted(piece, 1), shifted(piece, -1)
+    far_pieces = (shifted(left[:, :half], 1), shifted(right[:, half:], -1))
+    first_down = ((piece,), (left,), (right,), far_pieces)
+    half = first + second // 2
+    pieces = (down[:, first:half], down[:, half:])
+    lefts = [shifted(piece, 1) for piece in pieces]
+    rights = [shifted(piece, -1) for piece in pieces]
+    far_pieces = (shifted(lefts[0], 1), shifted(rights[1], -1))
+    second_down = (pieces, lefts, rights, far_pieces)
 
     outgoing, pick = dispatched(
         rank, expert_input, gain_expert[None, :], expert_choice.T, own_tokens, capacity, experts_all
@@ -330,17 +343,22 @@
     arrived, shared_parts = lax.optimization_barrier((arrived, shared_parts))
     near = expert_hidden(arrived, [(gate, up), (gate_left, up_left), (gate_right, up_right)])
     far = expert_hidden(arrived, [(gate_far, up_far)])
-    returned = []
-    for number, (piece, left, right) in enumerate(near_down):
-        if number > 0:
-            left, right, earlier_pair, _ = lax.optimization_barrier(
-                (left, right, earlier_pair, result)
-            )
-        middle = left.shape[1] // 2
-        far_left = shifted(left[:, :middle], 1)
-        far_right = shifted(right[:, middle:], -1)
-        result = expert_result(near, far, (piece, left, right, far_left, far_right))
-        returned.append(exchanged(result, experts_all))
+    own_weights = lax.dynamic_slice_in_dim(route_weights, tp_rank * own_tokens, own_tokens, 0)
+    mixing = jnp.sum(pick.astype(jnp.float32) * own_weights.T[:, None, :], axis=0)
+    mixing = mixing.astype(jnp.bfloat16)
+
+    def weighted(part):
+        return lax.dot_general(
+            mixing, part, (((0,), (0,)), ((), ())), preferred_element_type=jnp.float32
+        )
+
+    result = expert_result(near, far, first_down)
+    earlier_pair, _ = lax.optimization_barrier((earlier_pair, result))
+    returned = [exchanged(result, experts_all)]
+    result = expert_result(near, far, second_down)
+    routed = [weighted(returned[0])]
+    result, routed[0] = lax.optimization_barrier((result, routed[0]))
+    returned.append(exchanged(result, experts_all))
 
     prior_keys = earlier_pair[:, :key_width].reshape(WINDOW, -1, HEAD_DIM)
     prior_values = earlier_pair[:, key_width:].reshape(WINDOW, -1, HEAD_DIM)
@@ -355,21 +373,17 @@
     )
     mixer_parts = halved_products(attended, output_weight, own_tokens, 1)
     mixer_output = halved_sum(*mixer_parts, 1).astype(jnp.bfloat16)
+
+    routed.append(weighted(returned[1]))
     shared_part = halved_sum(*shared_parts, 3)
-
-    own_weights = lax.dynamic_slice_in_dim(route_weights, tp_rank * own_tokens, own_tokens, 0)
-    mixing = jnp.sum(pick.astype(jnp.float32) * own_weights.T[:, None, :], axis=0)
-    mixing = mixing.astype(jnp.bfloat16)
-    done = []
-    at = 0
-    for part in returned:
-        span = part.shape[1]
-        routed = lax.dot_general(
-            mixing, part, (((0,), (0,)), ((), ())), preferred_element_type=jnp.float32
-        )
-        done.append((routed + shared_part[:, at : at + span]).astype(jnp.bfloat16))
-        at += span
-    expert_output = jnp.concatenate(done, axis=1)
+    first = routed[0].shape[1]
+    expert_output = jnp.concatenate(
+        [
+            (routed[0] + shared_part[:, :first]).astype(jnp.bfloat16),
+            (routed[1] + shared_part[:, first:]).astype(jnp.bfloat16),
+        ],
+        axis=1,
+    )
     return (mixer_output, expert_output)
 
 

time: 199 us -> 197 us (0.990)
  local copies, waits for them, and re-layouts: 10.6 us -> 8.02 us
    all_to_all x3, waiting for transfers between devices: 14.8 us -> 25.7 us  [exchanged(): lax.all_to_all(rows.reshape(experts, slots // experts, width), 'ep', spli...]
    ppermute x14 -> x16, waiting for transfers between devices: 45.8 us -> 37.1 us  [shifted(): lax.ppermute(value, 'tp', [(at, (at + steps) % count) for at in range(cou...]
    all_to_all x3, starting transfers between devices: 35 us -> 30 us  [exchanged(): lax.all_to_all(rows.reshape(experts, slots // experts, width), 'ep', spli...]
    ppermute x14 -> x16, starting transfers between devices: 20.4 us -> 24.6 us  [shifted(): lax.ppermute(value, 'tp', [(at, (at + steps) % count) for at in range(cou...]
    ppermute x4, waiting for transfers between devices: 13.8 us -> 10.6 us  [crossed(): lax.ppermute(value, 'tp', [(at, at ^ mask) for at in range(lax.axis_size(...]
    unnamed x69 -> x65, local copies, waits for them, and re-layouts: 3.39 us -> 0.55 us
    ppermute x4, starting transfers between devices: 1.95 us -> 4.05 us  [crossed(): lax.ppermute(value, 'tp', [(at, at ^ mask) for at in range(lax.axis_size(...]
  transfers between devices with their start and end apart: 22 -> 24, of which waited for: 8 -> 8; matrix products, arithmetic and copies ran while one was open for 17% -> 18% of each run, Pallas kernels for 12% -> 12%
where the time goes in v4:
time: 197 us; the launch traced here: 196 us
  waiting for transfers between devices  73.4 us (37%)
  starting transfers between devices  60.6 us (31%)
  Pallas kernels  22.9 us (12%)
  matrix products  18.4 us (9%)
  other arithmetic  11.7 us (6%)
  local copies, waits for them, and re-layouts  8.02 us (4%)
    ppermute x16, waiting for transfers between devices, shifted(): lax.ppermute(value, 'tp', [(at, (at + steps) % count) for at in range(cou...  37.1 us
    all_to_all x3, starting transfers between devices, exchanged(): lax.all_to_all(rows.reshape(experts, slots // experts, width), 'ep', spli...  30 us
    all_to_all x3, waiting for transfers between devices, exchanged(): lax.all_to_all(rows.reshape(experts, slots // experts, width), 'ep', spli...  25.7 us
    ppermute x16, starting transfers between devices, shifted(): lax.ppermute(value, 'tp', [(at, (at + steps) % count) for at in range(cou...  24.6 us
    pallas_call x2, Pallas kernels, expert_hidden(): pl.pallas_call(hidden_body, grid=(1,), in_specs=[pl.BlockSpec(memory_spac...  11.1 us
    ppermute x4, waiting for transfers between devices, crossed(): lax.ppermute(value, 'tp', [(at, at ^ mask) for at in range(lax.axis_size(...  10.6 us
    pallas_call x2, Pallas kernels, expert_result(): pl.pallas_call(down_kernel([len(pieces) for pieces in matrices]), grid=(s...  8.46 us
    dot_general x4, matrix products, product(): jnp.dot(joined, weight, preferred_element_type=jnp.float32)  6.48 us
  transfers between devices with their start and end apart: 24, of which 8 were waited for; matrix products, arithmetic and copies ran while one was open for 18% of the time, Pallas kernels for 12%

profile of v4, /device:TPU:2, one launch (start us, length us, event | category | flops | bytes accessed | tf_op | source)
XLA Modules:
  0.0 196.4 jit_solution(3517279896716223231)
XLA Ops:
  0.6 3.1 %collective-permute-start.4 = (bf16[2048,256]{1,0:T(8,128)(2,1)}, bf16[2048,256]{1,0:T(8,128)(2,1)}, u32[]{:S(2)}, u32[]{:S(2)}) collective-permute-start(bf16[2048,256]{1,0:T(8,128)(2,1)} %bitcast.132), channel_id=1, source_target_pairs={{0,3},{1,0},{2,1},{3,2},{4,7},{5,4},{6,5},{7,6},{8,11},{9,8},{10,9... | collective-permute-start | bytes 3145736 | tf_op jit(solution)/shard_map/ppermute | solution.py:29
  3.7 0.6 collective-permute-start.1
  4.3 2.7 %collective-permute-start.3 = (bf16[2048,256]{1,0:T(8,128)(2,1)}, bf16[2048,256]{1,0:T(8,128)(2,1)}, u32[]{:S(2)}, u32[]{:S(2)}) collective-permute-start(bf16[2048,256]{1,0:T(8,128)(2,1)} %bitcast.130), channel_id=1, source_target_pairs={{0,3},{1,0},{2,1},{3,2},{4,7},{5,4},{6,5},{7,6},{8,11},{9,8},{10,9... | collective-permute-start | bytes 3145736 | tf_op jit(solution)/shard_map/ppermute | solution.py:29
  7.0 3.3 %dispatch.1 = (bf16[512,2048]{1,0:T(8,128)(2,1)}, bf16[2,512,128]{2,1,0:T(8,128)(2,1)}) custom-call(s32[1]{0:T(128)} %bitcast.3.rank_ref, bf16[512,2048]{1,0:T(8,128)(2,1)} %rows_ref.1, f32[1,2048]{1,0:T(1,128)} %bitcast.141, s32[2,512]{1,0:T(2,128)} %bitcast.142), custom_call_target="tpu_custom_call" | custom-call | tf_op jit(solution)/shard_map/dispatch/pallas_call | solution.py:164
  10.3 12.2 %all-to-all-start = ((bf16[64,8,2048]{2,1,0:T(8,128)(2,1)}), bf16[64,8,2048]{2,1,0:T(8,128)(2,1)}, u32[]{:S(2)}, u32[]{:S(2)}) async-start(bf16[64,8,2048]{2,1,0:T(8,128)(2,1)} %bitcast.126), calls=%async_computation | async-start | bytes 4194304 | tf_op jit(solution)/shard_map/all_to_all | solution.py:38
  22.5 1.0 slice.108.refs_0_
  23.6 2.1 %collective-permute-start.8 = (bf16[256,768]{1,0:T(8,128)(2,1)S(1)}, bf16[256,768]{1,0:T(8,128)(2,1)}, u32[]{:S(2)}, u32[]{:S(2)}) collective-permute-start(bf16[256,768]{1,0:T(8,128)(2,1)S(1)} %slice.108.refs_0_), channel_id=1, source_target_pairs={{0,3},{1,0},{2,1},{3,2},{4,7},{5,4},{6,5},{7,6},{8,11},{9,8},{10,9... | collective-permute-start | bytes 1179656 | tf_op jit(solution)/shard_map/ppermute | solution.py:29
  25.7 2.1 %fusion.3 = f32[512]{0:T(512)S(1)} fusion(bf16[512,2048]{1,0:T(8,128)(2,1)} %rows_ref.1), kind=kLoop, calls=%fused_computation.7 | loop fusion | flops 3145216 | bytes 2099200 | tf_op jit(solution)/shard_map/reduce_sum | solution.py:70
  27.8 2.2 %fusion = f32[512]{0:T(512)S(1)} fusion(bf16[512,2048]{1,0:T(8,128)(2,1)} %param.17), kind=kLoop, calls=%fused_computation.4 | loop fusion | flops 3145216 | bytes 2099200 | tf_op jit(solution)/shard_map/reduce_sum | solution.py:70
  30.1 2.7 %convolution_convert_fusion.4 = bf16[512,384]{0,1:T(8,128)(2,1)S(1)} fusion(bf16[2048,384]{1,0:T(8,128)(2,1)} %param.21, bf16[512,2048]{1,0:T(8,128)(2,1)S(1)} %copy-done.4, f32[2048]{0:T(1024)S(1)} %copy-done.31, f32[512]{0:T(512)S(1)} %add_rsqrt_fusion.1), kind=kOutput, calls=%fused_computation.27 | convolution fusion | flops 809697280 | bytes 4073472 | tf_op jit(solution)/shard_map/dot_general | solution.py:322
  32.9 2.5 %fusion.28 = f32[512,128]{1,0:T(8,128)S(1)} fusion(bf16[2048,128]{1,0:T(8,128)(2,1)S(1)} %copy-done.27, bf16[512,2048]{1,0:T(8,128)(2,1)} %rows_ref.1, f32[2048]{0:T(1024)S(1)} %copy-done.25, f32[512]{0:T(512)S(1)} %add_rsqrt_fusion), kind=kOutput, calls=%fused_computation.45 | convolution fusion | flops 272629760 | bytes 2893824 | tf_op jit(solution)/shard_map/dot_general | solution.py:339
  35.5 0.8 fusion.20
  36.4 0.3 multiply_cosine_fusion
  36.8 0.8 copy_bitcast_fusion.1
  37.6 1.4 convolution_convert_fusion.2
  39.2 0.8 convolution_convert_fusion.5
  40.1 0.3 copy-done.30
  40.4 0.8 fusion.22
  41.2 11.1 %collective-permute-done.1.refs_2_ = bf16[2048,256]{1,0:T(8,128)(2,1)} collective-permute-done((bf16[2048,256]{1,0:T(8,128)(2,1)}, bf16[2048,256]{1,0:T(8,128)(2,1)}, u32[]{:S(2)}, u32[]{:S(2)}) %collective-permute-start.1) | collective-permute-done | bytes 1048608 | tf_op jit(solution)/shard_map/ppermute | solution.py:29
  52.4 0.9 broadcast_and_fusion
  53.2 3.2 %collective-permute-start.6 = (bf16[2048,256]{1,0:T(8,128)(2,1)}, bf16[2048,256]{1,0:T(8,128)(2,1)S(1)}, u32[]{:S(2)}, u32[]{:S(2)}) collective-permute-start(bf16[2048,256]{1,0:T(8,128)(2,1)} %collective-permute-done.4.refs_5_), channel_id=1, source_target_pairs={{0,3},{1,0},{2,1},{3,2},{4,7},{5,4},{6,5},{7,6},{8,11},{9,8},{10,9... | collective-permute-start | bytes 3145736 | tf_op jit(solution)/shard_map/ppermute | solution.py:29
  56.5 0.3 fusion.59
  56.8 1.6 collective-permute-done.8.refs_2_
  58.4 1.1 collective-permute-start.7
  59.5 0.6 copy_bitcast_fusion.5
  60.2 1.4 convolution_convert_fusion.3
  61.6 24.4 %collective-permute-done.7.refs_1_ = bf16[256,768]{1,0:T(8,128)(2,1)S(1)} collective-permute-done((bf16[256,768]{1,0:T(8,128)(2,1)S(1)}, bf16[256,768]{1,0:T(8,128)(2,1)S(1)}, u32[]{:S(2)}, u32[]{:S(2)}) %collective-permute-start.7) | collective-permute-done | bytes 393248 | tf_op jit(solution)/shard_map/ppermute | solution.py:29
  86.0 3.2 %collective-permute-start.16 = (bf16[256,640]{1,0:T(8,128)(2,1)S(1)}, bf16[256,640]{1,0:T(8,128)(2,1)}, u32[]{:S(2)}, u32[]{:S(2)}) collective-permute-start(bf16[256,640]{1,0:T(8,128)(2,1)S(1)} %get-tuple-element.18.refs_1_), channel_id=1, source_target_pairs={{0,3},{1,0},{2,1},{3,2},{4,7},{5,4},{6,5},{7,6},{8,11},{9,8},{10,9... | collective-permute-start | bytes 983048 | tf_op jit(solution)/shard_map/ppermute | solution.py:29
  89.2 1.6 slice.110
  90.8 0.7 slice.109
  91.6 2.0 %collective-permute-start.9 = (bf16[256,384]{1,0:T(8,128)(2,1)}, bf16[256,384]{1,0:T(8,128)(2,1)}, u32[]{:S(2)}, u32[]{:S(2)}) collective-permute-start(bf16[256,384]{1,0:T(8,128)(2,1)} %slice.109), channel_id=1, source_target_pairs={{0,1},{1,2},{2,3},{3,0},{4,5},{5,6},{6,7},{7,4},{8,9},{9,10},{10,1... | collective-permute-start | bytes 589832 | tf_op jit(solution)/shard_map/ppermute | solution.py:29
  93.6 0.7 fusion.77
  94.3 1.9 collective-permute-start
  96.3 0.6 copy.26
  97.0 6.9 %shard_map.176.near_ref = bf16[512,768]{1,0:T(8,128)(2,1)} custom-call(bf16[512,2048]{1,0:T(8,128)(2,1)} %bitcast.7.rows_ref, bf16[2048,256]{1,0:T(8,128)(2,1)} %bitcast.131, bf16[2048,256]{1,0:T(8,128)(2,1)} %bitcast.134, bf16[2048,256]{1,0:T(8,128)(2,1)} %collective-permute-done.1.refs_2_, bf16[2048,256]{1,0:T(8,128)(2,1)} %collective-permute-done.2.refs_3_, ...), custom_call_target="tpu_custom_call" | custom-call | tf_op jit(solution)/shard_map/pallas_call | solution.py:213
  103.9 4.2 %shard_map.177.far_ref = bf16[512,256]{1,0:T(8,128)(2,1)} custom-call(bf16[512,2048]{1,0:T(8,128)(2,1)} %bitcast.7.rows_ref, bf16[2048,256]{1,0:T(8,128)(2,1)} %copy-done.9, bf16[2048,256]{1,0:T(8,128)(2,1)} %copy-done.10), custom_call_target="tpu_custom_call" | custom-call | tf_op jit(solution)/shard_map/pallas_call | solution.py:213
  108.2 0.1 collective-permute-start.14
  108.3 3.2 %collective-permute-start.15 = (bf16[256,640]{1,0:T(8,128)(2,1)S(1)}, bf16[256,640]{1,0:T(8,128)(2,1)}, u32[]{:S(2)}, u32[]{:S(2)}) collective-permute-start(bf16[256,640]{1,0:T(8,128)(2,1)S(1)} %get-tuple-element.19.refs_0_), channel_id=1, source_target_pairs={{0,3},{1,0},{2,1},{3,2},{4,7},{5,4},{6,5},{7,6},{8,11},{9,8},{10,9... | collective-permute-start | bytes 983048 | tf_op jit(solution)/shard_map/ppermute | solution.py:29
  111.5 3.2 %collective-permute-start.18 = (bf16[256,640]{1,0:T(8,128)(2,1)}, bf16[256,640]{1,0:T(8,128)(2,1)}, u32[]{:S(2)}, u32[]{:S(2)}) collective-permute-start(bf16[256,640]{1,0:T(8,128)(2,1)} %collective-permute-done.16.refs_5_), channel_id=1, source_target_pairs={{0,3},{1,0},{2,1},{3,2},{4,7},{5,4},{6,5},{7,6},{8,11},{9,8},{10,9... | collective-permute-start | bytes 983048 | tf_op jit(solution)/shard_map/ppermute | solution.py:29
  114.7 3.7 %down.2 = bf16[512,768]{1,0:T(8,128)(2,1)} custom-call(bf16[512,768]{1,0:T(8,128)(2,1)} %shard_map.176.near_ref, bf16[512,256]{1,0:T(8,128)(2,1)} %shard_map.177.far_ref, bf16[256,768]{1,0:T(8,128)(2,1)} %copy-done.6, bf16[256,768]{1,0:T(8,128)(2,1)} %copy-done.12, bf16[256,768]{1,0:T(8,128)(2,1)} %collective-permute-done.8.refs_2_, ...), custom_call_target="tpu_custom_call" | custom-call | tf_op jit(solution)/shard_map/down/pallas_call | solution.py:258
  118.5 12.0 %all-to-all-start.1 = ((bf16[64,8,768]{2,1,0:T(8,128)(2,1)}), bf16[64,8,768]{2,1,0:T(8,128)(2,1)S(1)}, u32[]{:S(2)}, u32[]{:S(2)}) async-start(bf16[64,8,768]{2,1,0:T(8,128)(2,1)} %bitcast.125), calls=%async_computation.1 | async-start | bytes 1572864 | tf_op jit(solution)/shard_map/all_to_all | solution.py:38
  130.5 0.2 collective-permute-start.19
  130.8 1.7 fusion.8
  132.6 0.7 fusion.6
  133.4 1.0 fusion.17
  134.3 0.3 copy.33
  134.7 0.8 constant_dynamic-slice_fusion.4
  135.4 1.7 convolution_convert_fusion
  137.2 4.7 %down.3 = bf16[512,1280]{1,0:T(8,128)(2,1)} custom-call(bf16[512,768]{1,0:T(8,128)(2,1)} %shard_map.176.near_ref, bf16[512,256]{1,0:T(8,128)(2,1)} %shard_map.177.far_ref, bf16[256,640]{1,0:T(8,128)(2,1)} %copy-done.8, bf16[256,640]{1,0:T(8,128)(2,1)} %copy-done.7, bf16[256,640]{1,0:T(8,128)(2,1)} %collective-permute-done.13.refs_2_, ...), custom_call_target="tpu_custom_call" | custom-call | tf_op jit(solution)/shard_map/down/pallas_call | solution.py:258
  141.9 11.7 %all-to-all-done.1 = bf16[64,8,768]{2,1,0:T(8,128)(2,1)S(1)} async-done(((bf16[64,8,768]{2,1,0:T(8,128)(2,1)}), bf16[64,8,768]{2,1,0:T(8,128)(2,1)S(1)}, u32[]{:S(2)}, u32[]{:S(2)}) %all-to-all-start.1) | async-done | bytes 786464 | tf_op jit(solution)/shard_map/all_to_all | solution.py:38
  153.6 0.3 fusion.24
  153.9 5.8 %all-to-all-start.2 = ((bf16[64,8,1280]{2,1,0:T(8,128)(2,1)}), bf16[64,8,1280]{2,1,0:T(8,128)(2,1)S(1)}, u32[]{:S(2)}, u32[]{:S(2)}) async-start(bf16[64,8,1280]{2,1,0:T(8,128)(2,1)} %bitcast.124), calls=%async_computation.2 | async-start | bytes 2621440 | tf_op jit(solution)/shard_map/all_to_all | solution.py:38
  159.8 1.9 convert_add_fusion
  161.9 0.7 collective-permute-done.11
  162.6 2.0 convert_add_fusion.1
  164.6 3.8 %collective-permute-start.12 = (bf16[128,2048]{1,0:T(8,128)(2,1)S(1)}, bf16[128,2048]{1,0:T(8,128)(2,1)S(1)}, u32[]{:S(2)}, u32[]{:S(2)}) collective-permute-start(bf16[128,2048]{1,0:T(8,128)(2,1)S(1)} %slice.152), channel_id=1, source_target_pairs={{0,3},{1,2},{2,1},{3,0},{4,7},{5,6},{6,5},{7,4},{8,11},{9,10},{10,... | collective-permute-start | bytes 1572872 | tf_op jit(solution)/shard_map/ppermute | solution.py:33
  168.4 7.4 %collective-permute-done.20 = bf16[128,2048]{1,0:T(8,128)(2,1)S(1)} collective-permute-done((bf16[128,2048]{1,0:T(8,128)(2,1)S(1)}, bf16[128,2048]{1,0:T(8,128)(2,1)S(1)}, u32[]{:S(2)}, u32[]{:S(2)}) %collective-permute-start.20) | collective-permute-done | bytes 524320 | tf_op jit(solution)/shard_map/ppermute | solution.py:33
  175.8 0.1 slice_add_fusion
  175.9 0.8 fusion.30
  176.7 2.4 %collective-permute-done.12 = bf16[128,2048]{1,0:T(8,128)(2,1)S(1)} collective-permute-done((bf16[128,2048]{1,0:T(8,128)(2,1)S(1)}, bf16[128,2048]{1,0:T(8,128)(2,1)S(1)}, u32[]{:S(2)}, u32[]{:S(2)}) %collective-permute-start.12) | collective-permute-done | bytes 524320 | tf_op jit(solution)/shard_map/ppermute | solution.py:33
  179.2 0.9 fusion.23
  180.1 14.0 %all-to-all-done.2 = bf16[64,8,1280]{2,1,0:T(8,128)(2,1)S(1)} async-done(((bf16[64,8,1280]{2,1,0:T(8,128)(2,1)}), bf16[64,8,1280]{2,1,0:T(8,128)(2,1)S(1)}, u32[]{:S(2)}, u32[]{:S(2)}) %all-to-all-start.2) | async-done | bytes 1310752 | tf_op jit(solution)/shard_map/all_to_all | solution.py:38
  194.1 1.5 fusion.26
  195.6 0.8 pad_maximum_fusion
  (112 shorter events, 1.2 us)
Async XLA Ops:
  0.6 134.8 %copy-start = (bf16[384,2048]{1,0:T(8,128)(2,1)S(1)}, bf16[384,2048]{1,0:T(8,128)(2,1)}, u32[]{:S(2)}) copy-start(bf16[384,2048]{1,0:T(8,128)(2,1)} %param.25) | copy-start | bytes 4718596
  0.6 52.6 %collective-permute-start.4 = (bf16[2048,256]{1,0:T(8,128)(2,1)}, bf16[2048,256]{1,0:T(8,128)(2,1)}, u32[]{:S(2)}, u32[]{:S(2)}) collective-permute-start(bf16[2048,256]{1,0:T(8,128)(2,1)} %bitcast.132), channel_id=1, source_target_pairs={{0,3},{1,0},{2,1},{3,2},{4,7},{5,4},{6,5},{7,6},{8,11},{9,8},{10,9... | collective-permute-start | bytes 3145736 | tf_op jit(solution)/shard_map/ppermute | solution.py:29
  3.7 82.2 %collective-permute-start.2 = (bf16[2048,256]{1,0:T(8,128)(2,1)}, bf16[2048,256]{1,0:T(8,128)(2,1)}, u32[]{:S(2)}, u32[]{:S(2)}) collective-permute-start(bf16[2048,256]{1,0:T(8,128)(2,1)} %bitcast.133), channel_id=1, source_target_pairs={{0,1},{1,2},{2,3},{3,0},{4,5},{5,6},{6,7},{7,4},{8,9},{9,10},{10,1... | collective-permute-start | bytes 3145736 | tf_op jit(solution)/shard_map/ppermute | solution.py:29
  3.7 48.6 %collective-permute-start.1 = (bf16[2048,256]{1,0:T(8,128)(2,1)}, bf16[2048,256]{1,0:T(8,128)(2,1)}, u32[]{:S(2)}, u32[]{:S(2)}) collective-permute-start(bf16[2048,256]{1,0:T(8,128)(2,1)} %bitcast.129), channel_id=1, source_target_pairs={{0,1},{1,2},{2,3},{3,0},{4,5},{5,6},{6,7},{7,4},{8,9},{9,10},{10,1... | collective-permute-start | bytes 3145736 | tf_op jit(solution)/shard_map/ppermute | solution.py:29
  4.3 87.2 %collective-permute-start.3 = (bf16[2048,256]{1,0:T(8,128)(2,1)}, bf16[2048,256]{1,0:T(8,128)(2,1)}, u32[]{:S(2)}, u32[]{:S(2)}) collective-permute-start(bf16[2048,256]{1,0:T(8,128)(2,1)} %bitcast.130), channel_id=1, source_target_pairs={{0,3},{1,0},{2,1},{3,2},{4,7},{5,4},{6,5},{7,6},{8,11},{9,8},{10,9... | collective-permute-start | bytes 3145736 | tf_op jit(solution)/shard_map/ppermute | solution.py:29
  10.3 86.6 %all-to-all-start = ((bf16[64,8,2048]{2,1,0:T(8,128)(2,1)}), bf16[64,8,2048]{2,1,0:T(8,128)(2,1)}, u32[]{:S(2)}, u32[]{:S(2)}) async-start(bf16[64,8,2048]{2,1,0:T(8,128)(2,1)} %bitcast.126), calls=%async_computation | async-start | bytes 4194304 | tf_op jit(solution)/shard_map/all_to_all | solution.py:38
  23.6 34.8 %copy-start.6 = (bf16[256,768]{1,0:T(8,128)(2,1)}, bf16[256,768]{1,0:T(8,128)(2,1)S(1)}, u32[]{:S(2)}) copy-start(bf16[256,768]{1,0:T(8,128)(2,1)S(1)} %slice.108.refs_0_) | copy-start | bytes 1179652
  23.6 34.8 %collective-permute-start.8 = (bf16[256,768]{1,0:T(8,128)(2,1)S(1)}, bf16[256,768]{1,0:T(8,128)(2,1)}, u32[]{:S(2)}, u32[]{:S(2)}) collective-permute-start(bf16[256,768]{1,0:T(8,128)(2,1)S(1)} %slice.108.refs_0_), channel_id=1, source_target_pairs={{0,3},{1,0},{2,1},{3,2},{4,7},{5,4},{6,5},{7,6},{8,11},{9,8},{10,9... | collective-permute-start | bytes 1179656 | tf_op jit(solution)/shard_map/ppermute | solution.py:29
  25.7 4.4 %copy-start.31 = (f32[2048]{0:T(1024)S(1)}, f32[2048]{0:T(1024)}, u32[]{:S(2)}) copy-start(f32[2048]{0:T(1024)} %param.19) | copy-start | bytes 24580
  27.8 2.3 %copy-start.4 = (bf16[512,2048]{1,0:T(8,128)(2,1)S(1)}, bf16[512,2048]{1,0:T(8,128)(2,1)}, u32[]{:S(2)}) copy-start(bf16[512,2048]{1,0:T(8,128)(2,1)} %param.17) | copy-start | bytes 6291460
  30.1 2.8 %copy-start.25 = (f32[2048]{0:T(1024)S(1)}, f32[2048]{0:T(1024)}, u32[]{:S(2)}) copy-start(f32[2048]{0:T(1024)} %param.20) | copy-start | bytes 24580
  30.1 2.8 %copy-start.27 = (bf16[2048,128]{1,0:T(8,128)(2,1)S(1)}, bf16[2048,128]{1,0:T(8,128)(2,1)}, u32[]{:S(2)}) copy-start(bf16[2048,128]{1,0:T(8,128)(2,1)} %param.31) | copy-start | bytes 1572868
  32.9 2.5 %copy-start.1 = (bf16[512,2048]{1,0:T(8,128)(2,1)S(1)}, bf16[512,2048]{1,0:T(8,128)(2,1)}, u32[]{:S(2)}) copy-start(bf16[512,2048]{1,0:T(8,128)(2,1)} %rows_ref.1) | copy-start | bytes 6291460
  32.9 2.5 %copy-start.28 = (bf16[2048,128]{1,0:T(8,128)(2,1)S(1)}, bf16[2048,128]{1,0:T(8,128)(2,1)}, u32[]{:S(2)}) copy-start(bf16[2048,128]{1,0:T(8,128)(2,1)} %param.32) | copy-start | bytes 1572868
  36.2 1.4 copy-start.3
  36.2 2.9 %copy-start.11 = (bf16[1,256,2048]{2,1,0:T(8,128)(2,1)S(1)}, bf16[1,256,2048]{2,1,0:T(8,128)(2,1)}, u32[]{:S(2)}) copy-start(bf16[1,256,2048]{2,1,0:T(8,128)(2,1)} %param.30) | copy-start | bytes 3145732
  36.8 2.4 %copy-start.5 = (bf16[512,2048]{1,0:T(8,128)(2,1)S(1)}, bf16[512,2048]{1,0:T(8,128)(2,1)}, u32[]{:S(2)}) copy-start(bf16[512,2048]{1,0:T(8,128)(2,1)} %param.17) | copy-start | bytes 6291460
  36.8 2.4 %copy-start.29 = (bf16[2048,64]{0,1:T(8,128)(2,1)S(1)}, bf16[2048,64]{0,1:T(8,128)(2,1)}, u32[]{:S(2)}) copy-start(bf16[2048,64]{0,1:T(8,128)(2,1)} %param.23) | copy-start | bytes 786436
  39.2 69.0 %copy-start.7 = (bf16[256,640]{1,0:T(8,128)(2,1)}, bf16[256,640]{1,0:T(8,128)(2,1)S(1)}, u32[]{:S(2)}) copy-start(bf16[256,640]{1,0:T(8,128)(2,1)S(1)} %get-tuple-element.18.refs_1_) | copy-start | bytes 983044
  39.2 69.1 %copy-start.8 = (bf16[256,640]{1,0:T(8,128)(2,1)}, bf16[256,640]{1,0:T(8,128)(2,1)S(1)}, u32[]{:S(2)}) copy-start(bf16[256,640]{1,0:T(8,128)(2,1)S(1)} %get-tuple-element.19.refs_0_) | copy-start | bytes 983044
  39.2 1.2 copy-start.30
  40.4 55.9 %copy-start.21 = (bf16[512,64]{0,1:T(8,128)(2,1)}, bf16[512,64]{0,1:T(8,128)(2,1)S(1)}, u32[]{:S(2)}) copy-start(bf16[512,64]{0,1:T(8,128)(2,1)S(1)} %convolution_convert_fusion.5) | copy-start | bytes 196612
  41.2 55.0 %copy-start.23 = (bf16[2,512,128]{2,1,0:T(8,128)(2,1)S(1)}, bf16[2,512,128]{2,1,0:T(8,128)(2,1)}, u32[]{:S(2)}) copy-start(bf16[2,512,128]{2,1,0:T(8,128)(2,1)} %get-tuple-element.13) | copy-start | bytes 786436
  52.4 39.2 %collective-permute-start.5 = (bf16[2048,256]{1,0:T(8,128)(2,1)}, bf16[2048,256]{1,0:T(8,128)(2,1)S(1)}, u32[]{:S(2)}, u32[]{:S(2)}) collective-permute-start(bf16[2048,256]{1,0:T(8,128)(2,1)} %collective-permute-done.1.refs_2_), channel_id=1, source_target_pairs={{0,1},{1,2},{2,3},{3,0},{4,5},{5,6},{6,7},{7,4},{8,9},{9,10},{10,1... | collective-permute-start | bytes 3145736 | tf_op jit(solution)/shard_map/ppermute | solution.py:29
  53.2 41.0 %collective-permute-start.6 = (bf16[2048,256]{1,0:T(8,128)(2,1)}, bf16[2048,256]{1,0:T(8,128)(2,1)S(1)}, u32[]{:S(2)}, u32[]{:S(2)}) collective-permute-start(bf16[2048,256]{1,0:T(8,128)(2,1)} %collective-permute-done.4.refs_5_), channel_id=1, source_target_pairs={{0,3},{1,0},{2,1},{3,2},{4,7},{5,4},{6,5},{7,6},{8,11},{9,8},{10,9... | collective-permute-start | bytes 3145736 | tf_op jit(solution)/shard_map/ppermute | solution.py:29
  56.8 47.1 %copy-start.15 = (bf16[512,1,32]{0,2,1:T(8,128)(2,1)}, bf16[512,1,32]{0,2,1:T(8,128)(2,1)S(1)}, u32[]{:S(2)}) copy-start(bf16[512,1,32]{0,2,1:T(8,128)(2,1)S(1)} %get-tuple-element.26) | copy-start | bytes 98308
  56.8 47.1 %copy-start.17 = (bf16[512,1,32]{0,2,1:T(8,128)(2,1)}, bf16[512,1,32]{0,2,1:T(8,128)(2,1)S(1)}, u32[]{:S(2)}) copy-start(bf16[512,1,32]{0,2,1:T(8,128)(2,1)S(1)} %get-tuple-element.27) | copy-start | bytes 98308
  58.4 27.6 %collective-permute-start.7 = (bf16[256,768]{1,0:T(8,128)(2,1)S(1)}, bf16[256,768]{1,0:T(8,128)(2,1)S(1)}, u32[]{:S(2)}, u32[]{:S(2)}) collective-permute-start(bf16[256,768]{1,0:T(8,128)(2,1)S(1)} %slice.108.refs_0_), channel_id=1, source_target_pairs={{0,1},{1,2},{2,3},{3,0},{4,5},{5,6},{6,7},{7,4},{8,9},{9,10},{10,1... | collective-permute-start | bytes 1179656 | tf_op jit(solution)/shard_map/ppermute | solution.py:29
  86.0 18.0 %copy-start.12 = (bf16[256,768]{1,0:T(8,128)(2,1)}, bf16[256,768]{1,0:T(8,128)(2,1)S(1)}, u32[]{:S(2)}) copy-start(bf16[256,768]{1,0:T(8,128)(2,1)S(1)} %collective-permute-done.7.refs_1_) | copy-start | bytes 1179652
  86.0 22.2 %collective-permute-start.13 = (bf16[256,640]{1,0:T(8,128)(2,1)S(1)}, bf16[256,640]{1,0:T(8,128)(2,1)}, u32[]{:S(2)}, u32[]{:S(2)}) collective-permute-start(bf16[256,640]{1,0:T(8,128)(2,1)S(1)} %get-tuple-element.19.refs_0_), channel_id=1, source_target_pairs={{0,1},{1,2},{2,3},{3,0},{4,5},{5,6},{6,7},{7,4},{8,9},{9,10},{10,1... | collective-permute-start | bytes 983048 | tf_op jit(solution)/shard_map/ppermute | solution.py:29
  86.0 22.3 %collective-permute-start.16 = (bf16[256,640]{1,0:T(8,128)(2,1)S(1)}, bf16[256,640]{1,0:T(8,128)(2,1)}, u32[]{:S(2)}, u32[]{:S(2)}) collective-permute-start(bf16[256,640]{1,0:T(8,128)(2,1)S(1)} %get-tuple-element.18.refs_1_), channel_id=1, source_target_pairs={{0,3},{1,0},{2,1},{3,2},{4,7},{5,4},{6,5},{7,6},{8,11},{9,8},{10,9... | collective-permute-start | bytes 983048 | tf_op jit(solution)/shard_map/ppermute | solution.py:29
  91.6 19.9 %collective-permute-start.10 = (bf16[256,384]{1,0:T(8,128)(2,1)}, bf16[256,384]{1,0:T(8,128)(2,1)}, u32[]{:S(2)}, u32[]{:S(2)}) collective-permute-start(bf16[256,384]{1,0:T(8,128)(2,1)} %slice.110), channel_id=1, source_target_pairs={{0,3},{1,0},{2,1},{3,2},{4,7},{5,4},{6,5},{7,6},{8,11},{9,8},{10,9... | collective-permute-start | bytes 589832 | tf_op jit(solution)/shard_map/ppermute | solution.py:29
  91.6 4.6 %copy-start.9 = (bf16[2048,256]{1,0:T(8,128)(2,1)}, bf16[2048,256]{1,0:T(8,128)(2,1)S(1)}, u32[]{:S(2)}) copy-start(bf16[2048,256]{1,0:T(8,128)(2,1)S(1)} %collective-permute-done.5.refs_0_) | copy-start | bytes 3145732
  91.6 19.9 %collective-permute-start.9 = (bf16[256,384]{1,0:T(8,128)(2,1)}, bf16[256,384]{1,0:T(8,128)(2,1)}, u32[]{:S(2)}, u32[]{:S(2)}) collective-permute-start(bf16[256,384]{1,0:T(8,128)(2,1)} %slice.109), channel_id=1, source_target_pairs={{0,1},{1,2},{2,3},{3,0},{4,5},{5,6},{6,7},{7,4},{8,9},{9,10},{10,1... | collective-permute-start | bytes 589832 | tf_op jit(solution)/shard_map/ppermute | solution.py:29
  94.3 1.9 copy-start.10
  94.3 36.2 %collective-permute-start = (bf16[128,128]{0,1:T(8,128)(2,1)S(1)}, bf16[128,128]{0,1:T(8,128)(2,1)S(1)}, u32[]{:S(2)}, u32[]{:S(2)}) collective-permute-start(bf16[128,128]{0,1:T(8,128)(2,1)S(1)} %pad_maximum_fusion.4), channel_id=1, source_target_pairs={{0,4},{4,8},{8,12},{12,16},{16,20},{20,24},{24,28},{28,32},{32,36}... | collective-permute-start | bytes 98312 | tf_op jit(solution)/shard_map/ppermute | solution.py:24
  108.1 22.6 %copy-start.16 = (bf16[512,1,32]{0,2,1:T(8,128)(2,1)S(1)}, bf16[512,1,32]{0,2,1:T(8,128)(2,1)}, u32[]{:S(2)}) copy-start(bf16[512,1,32]{0,2,1:T(8,128)(2,1)} %copy-done.15) | copy-start | bytes 98308
  108.1 22.6 %copy-start.18 = (bf16[512,1,32]{0,2,1:T(8,128)(2,1)S(1)}, bf16[512,1,32]{0,2,1:T(8,128)(2,1)}, u32[]{:S(2)}) copy-start(bf16[512,1,32]{0,2,1:T(8,128)(2,1)} %copy-done.17) | copy-start | bytes 98308
  108.1 22.6 %copy-start.22 = (bf16[512,64]{0,1:T(8,128)(2,1)S(1)}, bf16[512,64]{0,1:T(8,128)(2,1)}, u32[]{:S(2)}) copy-start(bf16[512,64]{0,1:T(8,128)(2,1)} %copy-done.21) | copy-start | bytes 196612
  108.1 22.6 %copy-start.14 = (pred[4,128,256]{1,2,0:T(8,128)(4,1)S(1)}, pred[4,128,256]{1,2,0:T(8,128)(4,1)}, u32[]{:S(2)}) copy-start(pred[4,128,256]{1,2,0:T(8,128)(4,1)} %broadcast_and_fusion) | copy-start | bytes 393220
  108.2 29.0 %collective-permute-start.14 = (bf16[256,640]{1,0:T(8,128)(2,1)S(1)}, bf16[256,640]{1,0:T(8,128)(2,1)}, u32[]{:S(2)}, u32[]{:S(2)}) collective-permute-start(bf16[256,640]{1,0:T(8,128)(2,1)S(1)} %get-tuple-element.18.refs_1_), channel_id=1, source_target_pairs={{0,1},{1,2},{2,3},{3,0},{4,5},{5,6},{6,7},{7,4},{8,9},{9,10},{10,1... | collective-permute-start | bytes 983048 | tf_op jit(solution)/shard_map/ppermute | solution.py:29
  108.3 28.9 %collective-permute-start.15 = (bf16[256,640]{1,0:T(8,128)(2,1)S(1)}, bf16[256,640]{1,0:T(8,128)(2,1)}, u32[]{:S(2)}, u32[]{:S(2)}) collective-permute-start(bf16[256,640]{1,0:T(8,128)(2,1)S(1)} %get-tuple-element.19.refs_0_), channel_id=1, source_target_pairs={{0,3},{1,0},{2,1},{3,2},{4,7},{5,4},{6,5},{7,6},{8,11},{9,8},{10,9... | collective-permute-start | bytes 983048 | tf_op jit(solution)/shard_map/ppermute | solution.py:29
  111.5 25.7 %collective-permute-start.17 = (bf16[256,640]{1,0:T(8,128)(2,1)}, bf16[256,640]{1,0:T(8,128)(2,1)}, u32[]{:S(2)}, u32[]{:S(2)}) collective-permute-start(bf16[256,640]{1,0:T(8,128)(2,1)} %collective-permute-done.13.refs_2_), channel_id=1, source_target_pairs={{0,1},{1,2},{2,3},{3,0},{4,5},{5,6},{6,7},{7,4},{8,9},{9,10},{10,1... | collective-permute-start | bytes 983048 | tf_op jit(solution)/shard_map/ppermute | solution.py:29
  111.5 25.7 %collective-permute-start.18 = (bf16[256,640]{1,0:T(8,128)(2,1)}, bf16[256,640]{1,0:T(8,128)(2,1)}, u32[]{:S(2)}, u32[]{:S(2)}) collective-permute-start(bf16[256,640]{1,0:T(8,128)(2,1)} %collective-permute-done.16.refs_5_), channel_id=1, source_target_pairs={{0,3},{1,0},{2,1},{3,2},{4,7},{5,4},{6,5},{7,6},{8,11},{9,8},{10,9... | collective-permute-start | bytes 983048 | tf_op jit(solution)/shard_map/ppermute | solution.py:29
  118.5 35.2 %all-to-all-start.1 = ((bf16[64,8,768]{2,1,0:T(8,128)(2,1)}), bf16[64,8,768]{2,1,0:T(8,128)(2,1)S(1)}, u32[]{:S(2)}, u32[]{:S(2)}) async-start(bf16[64,8,768]{2,1,0:T(8,128)(2,1)} %bitcast.125), calls=%async_computation.1 | async-start | bytes 1572864 | tf_op jit(solution)/shard_map/all_to_all | solution.py:38
  130.5 29.2 %collective-permute-start.19 = (bf16[256,2048]{1,0:T(8,128)(2,1)}, bf16[256,2048]{1,0:T(8,128)(2,1)}, u32[]{:S(2)}, u32[]{:S(2)}) collective-permute-start(bf16[256,2048]{1,0:T(8,128)(2,1)} %convolution_convert_fusion.3), channel_id=1, source_target_pairs={{0,3},{1,2},{2,1},{3,0},{4,7},{5,6},{6,5},{7,4},{8,11},{9,10},{10,... | collective-permute-start | bytes 3145736 | tf_op jit(solution)/shard_map/ppermute | solution.py:33
  130.7 1.7 copy-start.26
  132.5 0.9 copy-start.24
  137.2 25.4 %collective-permute-start.11 = (bf16[256,2048]{1,0:T(8,128)(2,1)}, bf16[256,2048]{1,0:T(8,128)(2,1)}, u32[]{:S(2)}, u32[]{:S(2)}) collective-permute-start(bf16[256,2048]{1,0:T(8,128)(2,1)} %convolution_convert_fusion), channel_id=1, source_target_pairs={{0,1},{1,0},{2,3},{3,2},{4,5},{5,4},{6,7},{7,6},{8,9},{9,8},{10,11... | collective-permute-start | bytes 3145736 | tf_op jit(solution)/shard_map/ppermute | solution.py:33
  153.9 40.2 %all-to-all-start.2 = ((bf16[64,8,1280]{2,1,0:T(8,128)(2,1)}), bf16[64,8,1280]{2,1,0:T(8,128)(2,1)S(1)}, u32[]{:S(2)}, u32[]{:S(2)}) async-start(bf16[64,8,1280]{2,1,0:T(8,128)(2,1)} %bitcast.124), calls=%async_computation.2 | async-start | bytes 2621440 | tf_op jit(solution)/shard_map/all_to_all | solution.py:38
  159.7 2.9 %copy-start.19 = (bf16[128,384]{0,1:T(8,128)(2,1)S(1)}, bf16[128,384]{0,1:T(8,128)(2,1)}, u32[]{:S(2)}) copy-start(bf16[128,384]{0,1:T(8,128)(2,1)} %get-tuple-element.22) | copy-start | bytes 294916
  159.7 2.9 %copy-start.20 = (bf16[128,384]{0,1:T(8,128)(2,1)S(1)}, bf16[128,384]{0,1:T(8,128)(2,1)}, u32[]{:S(2)}) copy-start(bf16[128,384]{0,1:T(8,128)(2,1)} %get-tuple-element.25) | copy-start | bytes 294916
  161.8 14.0 %collective-permute-start.20 = (bf16[128,2048]{1,0:T(8,128)(2,1)S(1)}, bf16[128,2048]{1,0:T(8,128)(2,1)S(1)}, u32[]{:S(2)}, u32[]{:S(2)}) collective-permute-start(bf16[128,2048]{1,0:T(8,128)(2,1)S(1)} %slice.151), channel_id=1, source_target_pairs={{0,1},{1,0},{2,3},{3,2},{4,5},{5,4},{6,7},{7,6},{8,9},{9,8},{10,11... | collective-permute-start | bytes 1572872 | tf_op jit(solution)/shard_map/ppermute | solution.py:33
  164.6 14.5 %collective-permute-start.12 = (bf16[128,2048]{1,0:T(8,128)(2,1)S(1)}, bf16[128,2048]{1,0:T(8,128)(2,1)S(1)}, u32[]{:S(2)}, u32[]{:S(2)}) collective-permute-start(bf16[128,2048]{1,0:T(8,128)(2,1)S(1)} %slice.152), channel_id=1, source_target_pairs={{0,3},{1,2},{2,1},{3,0},{4,7},{5,6},{6,5},{7,4},{8,11},{9,10},{10,... | collective-permute-start | bytes 1572872 | tf_op jit(solution)/shard_map/ppermute | solution.py:33
  175.9 3.2 %copy-start.2 = (f32[128,2048]{1,0:T(8,128)}, f32[128,2048]{1,0:T(8,128)S(1)}, u32[]{:S(2)}) copy-start(f32[128,2048]{1,0:T(8,128)S(1)} %slice_add_fusion) | copy-start | bytes 3145732
  176.7 18.8 %copy-start.13 = (bf16[128,768]{1,0:T(8,128)(2,1)S(1)}, bf16[128,768]{1,0:T(8,128)(2,1)}, u32[]{:S(2)}) copy-start(bf16[128,768]{1,0:T(8,128)(2,1)} %fusion.30) | copy-start | bytes 589828

commit v5 on v4

--- a/solution.py
+++ b/solution.py
@@ -289,7 +289,7 @@
     ep_count = lax.axis_size("ep")
     tp_rank = lax.axis_index("tp")
     rank = tp_rank.astype(jnp.int32).reshape(1)
-    group_rows, _ = mixer_input.shape
+    group_rows, model_width = mixer_input.shape
     group_tokens = expert_input.shape[0]
     own_tokens = group_tokens // tp_count
     top_count = expert_choice.shape[1]
@@ -377,13 +377,10 @@
     routed.append(weighted(returned[1]))
     shared_part = halved_sum(*shared_parts, 3)
     first = routed[0].shape[1]
-    expert_output = jnp.concatenate(
-        [
-            (routed[0] + shared_part[:, :first]).astype(jnp.bfloat16),
-            (routed[1] + shared_part[:, first:]).astype(jnp.bfloat16),
-        ],
-        axis=1,
-    )
+    head = (routed[0] + shared_part[:, :first]).astype(jnp.bfloat16)
+    head = lax.optimization_barrier(jnp.pad(head, ((0, 0), (0, model_width - first))))
+    tail = (routed[1] + shared_part[:, first:]).astype(jnp.bfloat16)
+    expert_output = lax.dynamic_update_slice(head, tail, (0, first))
     return (mixer_output, expert_output)
 
 

time: 197 us -> 197 us (level)
  no operation moved by 1% of the time
where the time goes in v5:
time: 197 us; the launch traced here: 196 us
  waiting for transfers between devices  74.1 us (38%)
  starting transfers between devices  60.6 us (31%)
  Pallas kernels  22.9 us (12%)
  matrix products  18.4 us (9%)
  other arithmetic  10.1 us (5%)
  local copies, waits for them, and re-layouts  8.85 us (4%)
    ppermute x16, waiting for transfers between devices, shifted(): lax.ppermute(value, 'tp', [(at, (at + steps) % count) for at in range(cou...  37.1 us
    all_to_all x3, starting transfers between devices, exchanged(): lax.all_to_all(rows.reshape(experts, slots // experts, width), 'ep', spli...  30 us
    all_to_all x3, waiting for transfers between devices, exchanged(): lax.all_to_all(rows.reshape(experts, slots // experts, width), 'ep', spli...  25.7 us
    ppermute x16, starting transfers between devices, shifted(): lax.ppermute(value, 'tp', [(at, (at + steps) % count) for at in range(cou...  24.6 us
    ppermute x4, waiting for transfers between devices, crossed(): lax.ppermute(value, 'tp', [(at, at ^ mask) for at in range(lax.axis_size(...  11.3 us
    pallas_call x2, Pallas kernels, expert_hidden(): pl.pallas_call(hidden_body, grid=(1,), in_specs=[pl.BlockSpec(memory_spac...  11.1 us
    pallas_call x2, Pallas kernels, expert_result(): pl.pallas_call(down_kernel([len(pieces) for pieces in matrices]), grid=(s...  8.46 us
    dot_general x4, matrix products, product(): jnp.dot(joined, weight, preferred_element_type=jnp.float32)  6.48 us
  transfers between devices with their start and end apart: 24, of which 8 were waited for; matrix products, arithmetic and copies ran while one was open for 18% of the time, Pallas kernels for 12%

profile of v5, /device:TPU:2, one launch (start us, length us, event | category | flops | bytes accessed | tf_op | source)
XLA Modules:
  0.0 196.4 jit_solution(9851631710320317817)
XLA Ops:
  0.6 3.1 %collective-permute-start.4 = (bf16[2048,256]{1,0:T(8,128)(2,1)}, bf16[2048,256]{1,0:T(8,128)(2,1)}, u32[]{:S(2)}, u32[]{:S(2)}) collective-permute-start(bf16[2048,256]{1,0:T(8,128)(2,1)} %bitcast.132), channel_id=1, source_target_pairs={{0,3},{1,0},{2,1},{3,2},{4,7},{5,4},{6,5},{7,6},{8,11},{9,8},{10,9... | collective-permute-start | bytes 3145736 | tf_op jit(solution)/shard_map/ppermute | solution.py:29
  3.7 0.6 collective-permute-start.1
  4.3 2.7 %collective-permute-start.3 = (bf16[2048,256]{1,0:T(8,128)(2,1)}, bf16[2048,256]{1,0:T(8,128)(2,1)}, u32[]{:S(2)}, u32[]{:S(2)}) collective-permute-start(bf16[2048,256]{1,0:T(8,128)(2,1)} %bitcast.130), channel_id=1, source_target_pairs={{0,3},{1,0},{2,1},{3,2},{4,7},{5,4},{6,5},{7,6},{8,11},{9,8},{10,9... | collective-permute-start | bytes 3145736 | tf_op jit(solution)/shard_map/ppermute | solution.py:29
  7.0 3.3 %dispatch.1 = (bf16[512,2048]{1,0:T(8,128)(2,1)}, bf16[2,512,128]{2,1,0:T(8,128)(2,1)}) custom-call(s32[1]{0:T(128)} %bitcast.3.rank_ref, bf16[512,2048]{1,0:T(8,128)(2,1)} %rows_ref.1, f32[1,2048]{1,0:T(1,128)} %bitcast.141, s32[2,512]{1,0:T(2,128)} %bitcast.142), custom_call_target="tpu_custom_call" | custom-call | tf_op jit(solution)/shard_map/dispatch/pallas_call | solution.py:164
  10.3 12.2 %all-to-all-start = ((bf16[64,8,2048]{2,1,0:T(8,128)(2,1)}), bf16[64,8,2048]{2,1,0:T(8,128)(2,1)}, u32[]{:S(2)}, u32[]{:S(2)}) async-start(bf16[64,8,2048]{2,1,0:T(8,128)(2,1)} %bitcast.126), calls=%async_computation | async-start | bytes 4194304 | tf_op jit(solution)/shard_map/all_to_all | solution.py:38
  22.5 1.0 slice.108.refs_0_
  23.6 2.1 %collective-permute-start.8 = (bf16[256,768]{1,0:T(8,128)(2,1)S(1)}, bf16[256,768]{1,0:T(8,128)(2,1)}, u32[]{:S(2)}, u32[]{:S(2)}) collective-permute-start(bf16[256,768]{1,0:T(8,128)(2,1)S(1)} %slice.108.refs_0_), channel_id=1, source_target_pairs={{0,3},{1,0},{2,1},{3,2},{4,7},{5,4},{6,5},{7,6},{8,11},{9,8},{10,9... | collective-permute-start | bytes 1179656 | tf_op jit(solution)/shard_map/ppermute | solution.py:29
  25.7 2.1 %fusion.3 = f32[512]{0:T(512)S(1)} fusion(bf16[512,2048]{1,0:T(8,128)(2,1)} %rows_ref.1), kind=kLoop, calls=%fused_computation.7 | loop fusion | flops 3145216 | bytes 2099200 | tf_op jit(solution)/shard_map/reduce_sum | solution.py:70
  27.8 2.2 %fusion = f32[512]{0:T(512)S(1)} fusion(bf16[512,2048]{1,0:T(8,128)(2,1)} %param.17), kind=kLoop, calls=%fused_computation.4 | loop fusion | flops 3145216 | bytes 2099200 | tf_op jit(solution)/shard_map/reduce_sum | solution.py:70
  30.1 2.7 %convolution_convert_fusion.4 = bf16[512,384]{0,1:T(8,128)(2,1)S(1)} fusion(bf16[2048,384]{1,0:T(8,128)(2,1)} %param.21, bf16[512,2048]{1,0:T(8,128)(2,1)S(1)} %copy-done.4, f32[2048]{0:T(1024)S(1)} %copy-done.31, f32[512]{0:T(512)S(1)} %add_rsqrt_fusion.1), kind=kOutput, calls=%fused_computation.27 | convolution fusion | flops 809697280 | bytes 4073472 | tf_op jit(solution)/shard_map/dot_general | solution.py:322
  32.9 2.5 %fusion.28 = f32[512,128]{1,0:T(8,128)S(1)} fusion(bf16[2048,128]{1,0:T(8,128)(2,1)S(1)} %copy-done.27, bf16[512,2048]{1,0:T(8,128)(2,1)} %rows_ref.1, f32[2048]{0:T(1024)S(1)} %copy-done.25, f32[512]{0:T(512)S(1)} %add_rsqrt_fusion), kind=kOutput, calls=%fused_computation.45 | convolution fusion | flops 272629760 | bytes 2893824 | tf_op jit(solution)/shard_map/dot_general | solution.py:339
  35.5 0.8 fusion.20
  36.4 0.3 multiply_cosine_fusion
  36.7 0.1 fusion.36
  36.8 0.8 copy_bitcast_fusion.1
  37.6 1.4 convolution_convert_fusion.2
  39.2 0.8 convolution_convert_fusion.5
  40.1 0.3 copy-done.30
  40.4 0.8 fusion.22
  41.2 11.1 %collective-permute-done.1.refs_2_ = bf16[2048,256]{1,0:T(8,128)(2,1)} collective-permute-done((bf16[2048,256]{1,0:T(8,128)(2,1)}, bf16[2048,256]{1,0:T(8,128)(2,1)}, u32[]{:S(2)}, u32[]{:S(2)}) %collective-permute-start.1) | collective-permute-done | bytes 1048608 | tf_op jit(solution)/shard_map/ppermute | solution.py:29
  52.4 0.9 broadcast_and_fusion
  53.2 3.2 %collective-permute-start.6 = (bf16[2048,256]{1,0:T(8,128)(2,1)}, bf16[2048,256]{1,0:T(8,128)(2,1)S(1)}, u32[]{:S(2)}, u32[]{:S(2)}) collective-permute-start(bf16[2048,256]{1,0:T(8,128)(2,1)} %collective-permute-done.4.refs_5_), channel_id=1, source_target_pairs={{0,3},{1,0},{2,1},{3,2},{4,7},{5,4},{6,5},{7,6},{8,11},{9,8},{10,9... | collective-permute-start | bytes 3145736 | tf_op jit(solution)/shard_map/ppermute | solution.py:29
  56.5 0.3 fusion.60
  56.8 1.6 collective-permute-done.8.refs_2_
  58.4 1.1 collective-permute-start.7
  59.5 0.6 copy_bitcast_fusion.5
  60.2 1.4 convolution_convert_fusion.3
  61.6 24.4 %collective-permute-done.7.refs_1_ = bf16[256,768]{1,0:T(8,128)(2,1)S(1)} collective-permute-done((bf16[256,768]{1,0:T(8,128)(2,1)S(1)}, bf16[256,768]{1,0:T(8,128)(2,1)S(1)}, u32[]{:S(2)}, u32[]{:S(2)}) %collective-permute-start.7) | collective-permute-done | bytes 393248 | tf_op jit(solution)/shard_map/ppermute | solution.py:29
  86.0 3.2 %collective-permute-start.16 = (bf16[256,640]{1,0:T(8,128)(2,1)S(1)}, bf16[256,640]{1,0:T(8,128)(2,1)}, u32[]{:S(2)}, u32[]{:S(2)}) collective-permute-start(bf16[256,640]{1,0:T(8,128)(2,1)S(1)} %get-tuple-element.18.refs_1_), channel_id=1, source_target_pairs={{0,3},{1,0},{2,1},{3,2},{4,7},{5,4},{6,5},{7,6},{8,11},{9,8},{10,9... | collective-permute-start | bytes 983048 | tf_op jit(solution)/shard_map/ppermute | solution.py:29
  89.2 1.6 slice.110
  90.8 0.7 slice.109
  91.6 2.0 %collective-permute-start.9 = (bf16[256,384]{1,0:T(8,128)(2,1)}, bf16[256,384]{1,0:T(8,128)(2,1)}, u32[]{:S(2)}, u32[]{:S(2)}) collective-permute-start(bf16[256,384]{1,0:T(8,128)(2,1)} %slice.109), channel_id=1, source_target_pairs={{0,1},{1,2},{2,3},{3,0},{4,5},{5,6},{6,7},{7,4},{8,9},{9,10},{10,1... | collective-permute-start | bytes 589832 | tf_op jit(solution)/shard_map/ppermute | solution.py:29
  93.6 0.7 fusion.78
  94.3 1.9 collective-permute-start
  96.3 0.6 copy.26
  97.0 6.9 %shard_map.176.near_ref = bf16[512,768]{1,0:T(8,128)(2,1)} custom-call(bf16[512,2048]{1,0:T(8,128)(2,1)} %bitcast.7.rows_ref, bf16[2048,256]{1,0:T(8,128)(2,1)} %bitcast.131, bf16[2048,256]{1,0:T(8,128)(2,1)} %bitcast.134, bf16[2048,256]{1,0:T(8,128)(2,1)} %collective-permute-done.1.refs_2_, bf16[2048,256]{1,0:T(8,128)(2,1)} %collective-permute-done.2.refs_3_, ...), custom_call_target="tpu_custom_call" | custom-call | tf_op jit(solution)/shard_map/pallas_call | solution.py:213
  103.9 4.2 %shard_map.177.far_ref = bf16[512,256]{1,0:T(8,128)(2,1)} custom-call(bf16[512,2048]{1,0:T(8,128)(2,1)} %bitcast.7.rows_ref, bf16[2048,256]{1,0:T(8,128)(2,1)} %copy-done.9, bf16[2048,256]{1,0:T(8,128)(2,1)} %copy-done.10), custom_call_target="tpu_custom_call" | custom-call | tf_op jit(solution)/shard_map/pallas_call | solution.py:213
  108.2 0.1 collective-permute-start.14
  108.3 3.2 %collective-permute-start.15 = (bf16[256,640]{1,0:T(8,128)(2,1)S(1)}, bf16[256,640]{1,0:T(8,128)(2,1)}, u32[]{:S(2)}, u32[]{:S(2)}) collective-permute-start(bf16[256,640]{1,0:T(8,128)(2,1)S(1)} %get-tuple-element.19.refs_0_), channel_id=1, source_target_pairs={{0,3},{1,0},{2,1},{3,2},{4,7},{5,4},{6,5},{7,6},{8,11},{9,8},{10,9... | collective-permute-start | bytes 983048 | tf_op jit(solution)/shard_map/ppermute | solution.py:29
  111.5 3.2 %collective-permute-start.18 = (bf16[256,640]{1,0:T(8,128)(2,1)}, bf16[256,640]{1,0:T(8,128)(2,1)}, u32[]{:S(2)}, u32[]{:S(2)}) collective-permute-start(bf16[256,640]{1,0:T(8,128)(2,1)} %collective-permute-done.16.refs_5_), channel_id=1, source_target_pairs={{0,3},{1,0},{2,1},{3,2},{4,7},{5,4},{6,5},{7,6},{8,11},{9,8},{10,9... | collective-permute-start | bytes 983048 | tf_op jit(solution)/shard_map/ppermute | solution.py:29
  114.7 3.7 %down.2 = bf16[512,768]{1,0:T(8,128)(2,1)} custom-call(bf16[512,768]{1,0:T(8,128)(2,1)} %shard_map.176.near_ref, bf16[512,256]{1,0:T(8,128)(2,1)} %shard_map.177.far_ref, bf16[256,768]{1,0:T(8,128)(2,1)} %copy-done.6, bf16[256,768]{1,0:T(8,128)(2,1)} %copy-done.12, bf16[256,768]{1,0:T(8,128)(2,1)} %collective-permute-done.8.refs_2_, ...), custom_call_target="tpu_custom_call" | custom-call | tf_op jit(solution)/shard_map/down/pallas_call | solution.py:258
  118.5 12.0 %all-to-all-start.1 = ((bf16[64,8,768]{2,1,0:T(8,128)(2,1)}), bf16[64,8,768]{2,1,0:T(8,128)(2,1)S(1)}, u32[]{:S(2)}, u32[]{:S(2)}) async-start(bf16[64,8,768]{2,1,0:T(8,128)(2,1)} %bitcast.125), calls=%async_computation.1 | async-start | bytes 1572864 | tf_op jit(solution)/shard_map/all_to_all | solution.py:38
  130.5 0.2 collective-permute-start.19
  130.8 1.7 fusion.8
  132.6 0.7 fusion.6
  133.4 1.0 fusion.17
  134.3 0.3 copy.33
  134.7 0.8 constant_dynamic-slice_fusion.4
  135.4 1.7 convolution_convert_fusion
  137.2 4.7 %down.3 = bf16[512,1280]{1,0:T(8,128)(2,1)} custom-call(bf16[512,768]{1,0:T(8,128)(2,1)} %shard_map.176.near_ref, bf16[512,256]{1,0:T(8,128)(2,1)} %shard_map.177.far_ref, bf16[256,640]{1,0:T(8,128)(2,1)} %copy-done.8, bf16[256,640]{1,0:T(8,128)(2,1)} %copy-done.7, bf16[256,640]{1,0:T(8,128)(2,1)} %collective-permute-done.13.refs_2_, ...), custom_call_target="tpu_custom_call" | custom-call | tf_op jit(solution)/shard_map/down/pallas_call | solution.py:258
  141.9 11.7 %all-to-all-done.1 = bf16[64,8,768]{2,1,0:T(8,128)(2,1)S(1)} async-done(((bf16[64,8,768]{2,1,0:T(8,128)(2,1)}), bf16[64,8,768]{2,1,0:T(8,128)(2,1)S(1)}, u32[]{:S(2)}, u32[]{:S(2)}) %all-to-all-start.1) | async-done | bytes 786464 | tf_op jit(solution)/shard_map/all_to_all | solution.py:38
  153.6 0.3 fusion.24
  153.9 5.8 %all-to-all-start.2 = ((bf16[64,8,1280]{2,1,0:T(8,128)(2,1)}), bf16[64,8,1280]{2,1,0:T(8,128)(2,1)S(1)}, u32[]{:S(2)}, u32[]{:S(2)}) async-start(bf16[64,8,1280]{2,1,0:T(8,128)(2,1)} %bitcast.124), calls=%async_computation.2 | async-start | bytes 2621440 | tf_op jit(solution)/shard_map/all_to_all | solution.py:38
  159.8 1.9 convert_add_fusion
  161.9 0.7 collective-permute-done.11
  162.6 2.0 convert_add_fusion.1
  164.6 3.8 %collective-permute-start.12 = (bf16[128,2048]{1,0:T(8,128)(2,1)S(1)}, bf16[128,2048]{1,0:T(8,128)(2,1)S(1)}, u32[]{:S(2)}, u32[]{:S(2)}) collective-permute-start(bf16[128,2048]{1,0:T(8,128)(2,1)S(1)} %slice.154), channel_id=1, source_target_pairs={{0,3},{1,2},{2,1},{3,0},{4,7},{5,6},{6,5},{7,4},{8,11},{9,10},{10,... | collective-permute-start | bytes 1572872 | tf_op jit(solution)/shard_map/ppermute | solution.py:33
  168.4 7.4 %collective-permute-done.20 = bf16[128,2048]{1,0:T(8,128)(2,1)S(1)} collective-permute-done((bf16[128,2048]{1,0:T(8,128)(2,1)S(1)}, bf16[128,2048]{1,0:T(8,128)(2,1)S(1)}, u32[]{:S(2)}, u32[]{:S(2)}) %collective-permute-start.20) | collective-permute-done | bytes 524320 | tf_op jit(solution)/shard_map/ppermute | solution.py:33
  175.8 0.1 slice_add_fusion
  176.0 3.1 %collective-permute-done.12 = bf16[128,2048]{1,0:T(8,128)(2,1)S(1)} collective-permute-done((bf16[128,2048]{1,0:T(8,128)(2,1)S(1)}, bf16[128,2048]{1,0:T(8,128)(2,1)S(1)}, u32[]{:S(2)}, u32[]{:S(2)}) %collective-permute-start.12) | collective-permute-done | bytes 524320 | tf_op jit(solution)/shard_map/ppermute | solution.py:33
  179.2 0.9 fusion.23
  180.1 14.0 %all-to-all-done.2 = bf16[64,8,1280]{2,1,0:T(8,128)(2,1)S(1)} async-done(((bf16[64,8,1280]{2,1,0:T(8,128)(2,1)}), bf16[64,8,1280]{2,1,0:T(8,128)(2,1)S(1)}, u32[]{:S(2)}, u32[]{:S(2)}) %all-to-all-start.2) | async-done | bytes 1310752 | tf_op jit(solution)/shard_map/all_to_all | solution.py:38
  194.1 1.5 fusion.35
  195.6 0.8 copy-done.14
  (112 shorter events, 1.2 us)
Async XLA Ops:
  0.6 134.8 %copy-start = (bf16[384,2048]{1,0:T(8,128)(2,1)S(1)}, bf16[384,2048]{1,0:T(8,128)(2,1)}, u32[]{:S(2)}) copy-start(bf16[384,2048]{1,0:T(8,128)(2,1)} %param.25) | copy-start | bytes 4718596
  0.6 52.6 %collective-permute-start.4 = (bf16[2048,256]{1,0:T(8,128)(2,1)}, bf16[2048,256]{1,0:T(8,128)(2,1)}, u32[]{:S(2)}, u32[]{:S(2)}) collective-permute-start(bf16[2048,256]{1,0:T(8,128)(2,1)} %bitcast.132), channel_id=1, source_target_pairs={{0,3},{1,0},{2,1},{3,2},{4,7},{5,4},{6,5},{7,6},{8,11},{9,8},{10,9... | collective-permute-start | bytes 3145736 | tf_op jit(solution)/shard_map/ppermute | solution.py:29
  3.7 82.2 %collective-permute-start.2 = (bf16[2048,256]{1,0:T(8,128)(2,1)}, bf16[2048,256]{1,0:T(8,128)(2,1)}, u32[]{:S(2)}, u32[]{:S(2)}) collective-permute-start(bf16[2048,256]{1,0:T(8,128)(2,1)} %bitcast.133), channel_id=1, source_target_pairs={{0,1},{1,2},{2,3},{3,0},{4,5},{5,6},{6,7},{7,4},{8,9},{9,10},{10,1... | collective-permute-start | bytes 3145736 | tf_op jit(solution)/shard_map/ppermute | solution.py:29
  3.7 48.6 %collective-permute-start.1 = (bf16[2048,256]{1,0:T(8,128)(2,1)}, bf16[2048,256]{1,0:T(8,128)(2,1)}, u32[]{:S(2)}, u32[]{:S(2)}) collective-permute-start(bf16[2048,256]{1,0:T(8,128)(2,1)} %bitcast.129), channel_id=1, source_target_pairs={{0,1},{1,2},{2,3},{3,0},{4,5},{5,6},{6,7},{7,4},{8,9},{9,10},{10,1... | collective-permute-start | bytes 3145736 | tf_op jit(solution)/shard_map/ppermute | solution.py:29
  4.3 87.2 %collective-permute-start.3 = (bf16[2048,256]{1,0:T(8,128)(2,1)}, bf16[2048,256]{1,0:T(8,128)(2,1)}, u32[]{:S(2)}, u32[]{:S(2)}) collective-permute-start(bf16[2048,256]{1,0:T(8,128)(2,1)} %bitcast.130), channel_id=1, source_target_pairs={{0,3},{1,0},{2,1},{3,2},{4,7},{5,4},{6,5},{7,6},{8,11},{9,8},{10,9... | collective-permute-start | bytes 3145736 | tf_op jit(solution)/shard_map/ppermute | solution.py:29
  10.3 86.6 %all-to-all-start = ((bf16[64,8,2048]{2,1,0:T(8,128)(2,1)}), bf16[64,8,2048]{2,1,0:T(8,128)(2,1)}, u32[]{:S(2)}, u32[]{:S(2)}) async-start(bf16[64,8,2048]{2,1,0:T(8,128)(2,1)} %bitcast.126), calls=%async_computation | async-start | bytes 4194304 | tf_op jit(solution)/shard_map/all_to_all | solution.py:38
  23.6 34.8 %copy-start.6 = (bf16[256,768]{1,0:T(8,128)(2,1)}, bf16[256,768]{1,0:T(8,128)(2,1)S(1)}, u32[]{:S(2)}) copy-start(bf16[256,768]{1,0:T(8,128)(2,1)S(1)} %slice.108.refs_0_) | copy-start | bytes 1179652
  23.6 34.8 %collective-permute-start.8 = (bf16[256,768]{1,0:T(8,128)(2,1)S(1)}, bf16[256,768]{1,0:T(8,128)(2,1)}, u32[]{:S(2)}, u32[]{:S(2)}) collective-permute-start(bf16[256,768]{1,0:T(8,128)(2,1)S(1)} %slice.108.refs_0_), channel_id=1, source_target_pairs={{0,3},{1,0},{2,1},{3,2},{4,7},{5,4},{6,5},{7,6},{8,11},{9,8},{10,9... | collective-permute-start | bytes 1179656 | tf_op jit(solution)/shard_map/ppermute | solution.py:29
  25.7 4.4 %copy-start.31 = (f32[2048]{0:T(1024)S(1)}, f32[2048]{0:T(1024)}, u32[]{:S(2)}) copy-start(f32[2048]{0:T(1024)} %param.19) | copy-start | bytes 24580
  27.8 2.3 %copy-start.4 = (bf16[512,2048]{1,0:T(8,128)(2,1)S(1)}, bf16[512,2048]{1,0:T(8,128)(2,1)}, u32[]{:S(2)}) copy-start(bf16[512,2048]{1,0:T(8,128)(2,1)} %param.17) | copy-start | bytes 6291460
  30.1 2.8 %copy-start.25 = (f32[2048]{0:T(1024)S(1)}, f32[2048]{0:T(1024)}, u32[]{:S(2)}) copy-start(f32[2048]{0:T(1024)} %param.20) | copy-start | bytes 24580
  30.1 2.8 %copy-start.27 = (bf16[2048,128]{1,0:T(8,128)(2,1)S(1)}, bf16[2048,128]{1,0:T(8,128)(2,1)}, u32[]{:S(2)}) copy-start(bf16[2048,128]{1,0:T(8,128)(2,1)} %param.31) | copy-start | bytes 1572868
  32.9 2.5 %copy-start.1 = (bf16[512,2048]{1,0:T(8,128)(2,1)S(1)}, bf16[512,2048]{1,0:T(8,128)(2,1)}, u32[]{:S(2)}) copy-start(bf16[512,2048]{1,0:T(8,128)(2,1)} %rows_ref.1) | copy-start | bytes 6291460
  32.9 2.5 %copy-start.28 = (bf16[2048,128]{1,0:T(8,128)(2,1)S(1)}, bf16[2048,128]{1,0:T(8,128)(2,1)}, u32[]{:S(2)}) copy-start(bf16[2048,128]{1,0:T(8,128)(2,1)} %param.32) | copy-start | bytes 1572868
  36.2 1.4 copy-start.3
  36.2 2.9 %copy-start.11 = (bf16[1,256,2048]{2,1,0:T(8,128)(2,1)S(1)}, bf16[1,256,2048]{2,1,0:T(8,128)(2,1)}, u32[]{:S(2)}) copy-start(bf16[1,256,2048]{2,1,0:T(8,128)(2,1)} %param.30) | copy-start | bytes 3145732
  36.8 2.4 %copy-start.5 = (bf16[512,2048]{1,0:T(8,128)(2,1)S(1)}, bf16[512,2048]{1,0:T(8,128)(2,1)}, u32[]{:S(2)}) copy-start(bf16[512,2048]{1,0:T(8,128)(2,1)} %param.17) | copy-start | bytes 6291460
  36.8 2.4 %copy-start.29 = (bf16[2048,64]{0,1:T(8,128)(2,1)S(1)}, bf16[2048,64]{0,1:T(8,128)(2,1)}, u32[]{:S(2)}) copy-start(bf16[2048,64]{0,1:T(8,128)(2,1)} %param.23) | copy-start | bytes 786436
  39.2 69.0 %copy-start.7 = (bf16[256,640]{1,0:T(8,128)(2,1)}, bf16[256,640]{1,0:T(8,128)(2,1)S(1)}, u32[]{:S(2)}) copy-start(bf16[256,640]{1,0:T(8,128)(2,1)S(1)} %get-tuple-element.18.refs_1_) | copy-start | bytes 983044
  39.2 69.1 %copy-start.8 = (bf16[256,640]{1,0:T(8,128)(2,1)}, bf16[256,640]{1,0:T(8,128)(2,1)S(1)}, u32[]{:S(2)}) copy-start(bf16[256,640]{1,0:T(8,128)(2,1)S(1)} %get-tuple-element.19.refs_0_) | copy-start | bytes 983044
  39.2 1.2 copy-start.30
  40.4 55.9 %copy-start.21 = (bf16[512,64]{0,1:T(8,128)(2,1)}, bf16[512,64]{0,1:T(8,128)(2,1)S(1)}, u32[]{:S(2)}) copy-start(bf16[512,64]{0,1:T(8,128)(2,1)S(1)} %convolution_convert_fusion.5) | copy-start | bytes 196612
  41.2 55.0 %copy-start.23 = (bf16[2,512,128]{2,1,0:T(8,128)(2,1)S(1)}, bf16[2,512,128]{2,1,0:T(8,128)(2,1)}, u32[]{:S(2)}) copy-start(bf16[2,512,128]{2,1,0:T(8,128)(2,1)} %get-tuple-element.13) | copy-start | bytes 786436
  52.4 39.2 %collective-permute-start.5 = (bf16[2048,256]{1,0:T(8,128)(2,1)}, bf16[2048,256]{1,0:T(8,128)(2,1)S(1)}, u32[]{:S(2)}, u32[]{:S(2)}) collective-permute-start(bf16[2048,256]{1,0:T(8,128)(2,1)} %collective-permute-done.1.refs_2_), channel_id=1, source_target_pairs={{0,1},{1,2},{2,3},{3,0},{4,5},{5,6},{6,7},{7,4},{8,9},{9,10},{10,1... | collective-permute-start | bytes 3145736 | tf_op jit(solution)/shard_map/ppermute | solution.py:29
  53.2 41.0 %collective-permute-start.6 = (bf16[2048,256]{1,0:T(8,128)(2,1)}, bf16[2048,256]{1,0:T(8,128)(2,1)S(1)}, u32[]{:S(2)}, u32[]{:S(2)}) collective-permute-start(bf16[2048,256]{1,0:T(8,128)(2,1)} %collective-permute-done.4.refs_5_), channel_id=1, source_target_pairs={{0,3},{1,0},{2,1},{3,2},{4,7},{5,4},{6,5},{7,6},{8,11},{9,8},{10,9... | collective-permute-start | bytes 3145736 | tf_op jit(solution)/shard_map/ppermute | solution.py:29
  56.8 47.1 %copy-start.15 = (bf16[512,1,32]{0,2,1:T(8,128)(2,1)}, bf16[512,1,32]{0,2,1:T(8,128)(2,1)S(1)}, u32[]{:S(2)}) copy-start(bf16[512,1,32]{0,2,1:T(8,128)(2,1)S(1)} %get-tuple-element.26) | copy-start | bytes 98308
  56.8 47.1 %copy-start.17 = (bf16[512,1,32]{0,2,1:T(8,128)(2,1)}, bf16[512,1,32]{0,2,1:T(8,128)(2,1)S(1)}, u32[]{:S(2)}) copy-start(bf16[512,1,32]{0,2,1:T(8,128)(2,1)S(1)} %get-tuple-element.27) | copy-start | bytes 98308
  58.4 27.6 %collective-permute-start.7 = (bf16[256,768]{1,0:T(8,128)(2,1)S(1)}, bf16[256,768]{1,0:T(8,128)(2,1)S(1)}, u32[]{:S(2)}, u32[]{:S(2)}) collective-permute-start(bf16[256,768]{1,0:T(8,128)(2,1)S(1)} %slice.108.refs_0_), channel_id=1, source_target_pairs={{0,1},{1,2},{2,3},{3,0},{4,5},{5,6},{6,7},{7,4},{8,9},{9,10},{10,1... | collective-permute-start | bytes 1179656 | tf_op jit(solution)/shard_map/ppermute | solution.py:29
  86.0 18.0 %copy-start.12 = (bf16[256,768]{1,0:T(8,128)(2,1)}, bf16[256,768]{1,0:T(8,128)(2,1)S(1)}, u32[]{:S(2)}) copy-start(bf16[256,768]{1,0:T(8,128)(2,1)S(1)} %collective-permute-done.7.refs_1_) | copy-start | bytes 1179652
  86.0 22.2 %collective-permute-start.13 = (bf16[256,640]{1,0:T(8,128)(2,1)S(1)}, bf16[256,640]{1,0:T(8,128)(2,1)}, u32[]{:S(2)}, u32[]{:S(2)}) collective-permute-start(bf16[256,640]{1,0:T(8,128)(2,1)S(1)} %get-tuple-element.19.refs_0_), channel_id=1, source_target_pairs={{0,1},{1,2},{2,3},{3,0},{4,5},{5,6},{6,7},{7,4},{8,9},{9,10},{10,1... | collective-permute-start | bytes 983048 | tf_op jit(solution)/shard_map/ppermute | solution.py:29
  86.0 22.3 %collective-permute-start.16 = (bf16[256,640]{1,0:T(8,128)(2,1)S(1)}, bf16[256,640]{1,0:T(8,128)(2,1)}, u32[]{:S(2)}, u32[]{:S(2)}) collective-permute-start(bf16[256,640]{1,0:T(8,128)(2,1)S(1)} %get-tuple-element.18.refs_1_), channel_id=1, source_target_pairs={{0,3},{1,0},{2,1},{3,2},{4,7},{5,4},{6,5},{7,6},{8,11},{9,8},{10,9... | collective-permute-start | bytes 983048 | tf_op jit(solution)/shard_map/ppermute | solution.py:29
  91.6 19.9 %collective-permute-start.10 = (bf16[256,384]{1,0:T(8,128)(2,1)}, bf16[256,384]{1,0:T(8,128)(2,1)}, u32[]{:S(2)}, u32[]{:S(2)}) collective-permute-start(bf16[256,384]{1,0:T(8,128)(2,1)} %slice.110), channel_id=1, source_target_pairs={{0,3},{1,0},{2,1},{3,2},{4,7},{5,4},{6,5},{7,6},{8,11},{9,8},{10,9... | collective-permute-start | bytes 589832 | tf_op jit(solution)/shard_map/ppermute | solution.py:29
  91.6 4.6 %copy-start.9 = (bf16[2048,256]{1,0:T(8,128)(2,1)}, bf16[2048,256]{1,0:T(8,128)(2,1)S(1)}, u32[]{:S(2)}) copy-start(bf16[2048,256]{1,0:T(8,128)(2,1)S(1)} %collective-permute-done.5.refs_0_) | copy-start | bytes 3145732
  91.6 19.9 %collective-permute-start.9 = (bf16[256,384]{1,0:T(8,128)(2,1)}, bf16[256,384]{1,0:T(8,128)(2,1)}, u32[]{:S(2)}, u32[]{:S(2)}) collective-permute-start(bf16[256,384]{1,0:T(8,128)(2,1)} %slice.109), channel_id=1, source_target_pairs={{0,1},{1,2},{2,3},{3,0},{4,5},{5,6},{6,7},{7,4},{8,9},{9,10},{10,1... | collective-permute-start | bytes 589832 | tf_op jit(solution)/shard_map/ppermute | solution.py:29
  94.3 1.9 copy-start.10
  94.3 36.2 %collective-permute-start = (bf16[128,128]{0,1:T(8,128)(2,1)S(1)}, bf16[128,128]{0,1:T(8,128)(2,1)S(1)}, u32[]{:S(2)}, u32[]{:S(2)}) collective-permute-start(bf16[128,128]{0,1:T(8,128)(2,1)S(1)} %pad_maximum_fusion.3), channel_id=1, source_target_pairs={{0,4},{4,8},{8,12},{12,16},{16,20},{20,24},{24,28},{28,32},{32,36}... | collective-permute-start | bytes 98312 | tf_op jit(solution)/shard_map/ppermute | solution.py:24
  108.1 22.6 %copy-start.16 = (bf16[512,1,32]{0,2,1:T(8,128)(2,1)S(1)}, bf16[512,1,32]{0,2,1:T(8,128)(2,1)}, u32[]{:S(2)}) copy-start(bf16[512,1,32]{0,2,1:T(8,128)(2,1)} %copy-done.15) | copy-start | bytes 98308
  108.1 22.6 %copy-start.18 = (bf16[512,1,32]{0,2,1:T(8,128)(2,1)S(1)}, bf16[512,1,32]{0,2,1:T(8,128)(2,1)}, u32[]{:S(2)}) copy-start(bf16[512,1,32]{0,2,1:T(8,128)(2,1)} %copy-done.17) | copy-start | bytes 98308
  108.1 22.6 %copy-start.22 = (bf16[512,64]{0,1:T(8,128)(2,1)S(1)}, bf16[512,64]{0,1:T(8,128)(2,1)}, u32[]{:S(2)}) copy-start(bf16[512,64]{0,1:T(8,128)(2,1)} %copy-done.21) | copy-start | bytes 196612
  108.1 22.6 %copy-start.13 = (pred[4,128,256]{1,2,0:T(8,128)(4,1)S(1)}, pred[4,128,256]{1,2,0:T(8,128)(4,1)}, u32[]{:S(2)}) copy-start(pred[4,128,256]{1,2,0:T(8,128)(4,1)} %broadcast_and_fusion) | copy-start | bytes 393220
  108.2 29.0 %collective-permute-start.14 = (bf16[256,640]{1,0:T(8,128)(2,1)S(1)}, bf16[256,640]{1,0:T(8,128)(2,1)}, u32[]{:S(2)}, u32[]{:S(2)}) collective-permute-start(bf16[256,640]{1,0:T(8,128)(2,1)S(1)} %get-tuple-element.18.refs_1_), channel_id=1, source_target_pairs={{0,1},{1,2},{2,3},{3,0},{4,5},{5,6},{6,7},{7,4},{8,9},{9,10},{10,1... | collective-permute-start | bytes 983048 | tf_op jit(solution)/shard_map/ppermute | solution.py:29
  108.3 28.9 %collective-permute-start.15 = (bf16[256,640]{1,0:T(8,128)(2,1)S(1)}, bf16[256,640]{1,0:T(8,128)(2,1)}, u32[]{:S(2)}, u32[]{:S(2)}) collective-permute-start(bf16[256,640]{1,0:T(8,128)(2,1)S(1)} %get-tuple-element.19.refs_0_), channel_id=1, source_target_pairs={{0,3},{1,0},{2,1},{3,2},{4,7},{5,4},{6,5},{7,6},{8,11},{9,8},{10,9... | collective-permute-start | bytes 983048 | tf_op jit(solution)/shard_map/ppermute | solution.py:29
  111.5 25.7 %collective-permute-start.17 = (bf16[256,640]{1,0:T(8,128)(2,1)}, bf16[256,640]{1,0:T(8,128)(2,1)}, u32[]{:S(2)}, u32[]{:S(2)}) collective-permute-start(bf16[256,640]{1,0:T(8,128)(2,1)} %collective-permute-done.13.refs_2_), channel_id=1, source_target_pairs={{0,1},{1,2},{2,3},{3,0},{4,5},{5,6},{6,7},{7,4},{8,9},{9,10},{10,1... | collective-permute-start | bytes 983048 | tf_op jit(solution)/shard_map/ppermute | solution.py:29
  111.5 25.7 %collective-permute-start.18 = (bf16[256,640]{1,0:T(8,128)(2,1)}, bf16[256,640]{1,0:T(8,128)(2,1)}, u32[]{:S(2)}, u32[]{:S(2)}) collective-permute-start(bf16[256,640]{1,0:T(8,128)(2,1)} %collective-permute-done.16.refs_5_), channel_id=1, source_target_pairs={{0,3},{1,0},{2,1},{3,2},{4,7},{5,4},{6,5},{7,6},{8,11},{9,8},{10,9... | collective-permute-start | bytes 983048 | tf_op jit(solution)/shard_map/ppermute | solution.py:29
  118.5 35.2 %all-to-all-start.1 = ((bf16[64,8,768]{2,1,0:T(8,128)(2,1)}), bf16[64,8,768]{2,1,0:T(8,128)(2,1)S(1)}, u32[]{:S(2)}, u32[]{:S(2)}) async-start(bf16[64,8,768]{2,1,0:T(8,128)(2,1)} %bitcast.125), calls=%async_computation.1 | async-start | bytes 1572864 | tf_op jit(solution)/shard_map/all_to_all | solution.py:38
  130.5 29.2 %collective-permute-start.19 = (bf16[256,2048]{1,0:T(8,128)(2,1)}, bf16[256,2048]{1,0:T(8,128)(2,1)}, u32[]{:S(2)}, u32[]{:S(2)}) collective-permute-start(bf16[256,2048]{1,0:T(8,128)(2,1)} %convolution_convert_fusion.3), channel_id=1, source_target_pairs={{0,3},{1,2},{2,1},{3,0},{4,7},{5,6},{6,5},{7,4},{8,11},{9,10},{10,... | collective-permute-start | bytes 3145736 | tf_op jit(solution)/shard_map/ppermute | solution.py:33
  130.7 1.7 copy-start.26
  132.5 0.9 copy-start.24
  137.2 25.4 %collective-permute-start.11 = (bf16[256,2048]{1,0:T(8,128)(2,1)}, bf16[256,2048]{1,0:T(8,128)(2,1)}, u32[]{:S(2)}, u32[]{:S(2)}) collective-permute-start(bf16[256,2048]{1,0:T(8,128)(2,1)} %convolution_convert_fusion), channel_id=1, source_target_pairs={{0,1},{1,0},{2,3},{3,2},{4,5},{5,4},{6,7},{7,6},{8,9},{9,8},{10,11... | collective-permute-start | bytes 3145736 | tf_op jit(solution)/shard_map/ppermute | solution.py:33
  153.9 40.2 %all-to-all-start.2 = ((bf16[64,8,1280]{2,1,0:T(8,128)(2,1)}), bf16[64,8,1280]{2,1,0:T(8,128)(2,1)S(1)}, u32[]{:S(2)}, u32[]{:S(2)}) async-start(bf16[64,8,1280]{2,1,0:T(8,128)(2,1)} %bitcast.124), calls=%async_computation.2 | async-start | bytes 2621440 | tf_op jit(solution)/shard_map/all_to_all | solution.py:38
  159.7 2.9 %copy-start.19 = (bf16[128,384]{0,1:T(8,128)(2,1)S(1)}, bf16[128,384]{0,1:T(8,128)(2,1)}, u32[]{:S(2)}) copy-start(bf16[128,384]{0,1:T(8,128)(2,1)} %get-tuple-element.22) | copy-start | bytes 294916
  159.7 2.9 %copy-start.20 = (bf16[128,384]{0,1:T(8,128)(2,1)S(1)}, bf16[128,384]{0,1:T(8,128)(2,1)}, u32[]{:S(2)}) copy-start(bf16[128,384]{0,1:T(8,128)(2,1)} %get-tuple-element.25) | copy-start | bytes 294916
  161.8 14.0 %collective-permute-start.20 = (bf16[128,2048]{1,0:T(8,128)(2,1)S(1)}, bf16[128,2048]{1,0:T(8,128)(2,1)S(1)}, u32[]{:S(2)}, u32[]{:S(2)}) collective-permute-start(bf16[128,2048]{1,0:T(8,128)(2,1)S(1)} %slice.153), channel_id=1, source_target_pairs={{0,1},{1,0},{2,3},{3,2},{4,5},{5,4},{6,7},{7,6},{8,9},{9,8},{10,11... | collective-permute-start | bytes 1572872 | tf_op jit(solution)/shard_map/ppermute | solution.py:33
  164.6 14.5 %collective-permute-start.12 = (bf16[128,2048]{1,0:T(8,128)(2,1)S(1)}, bf16[128,2048]{1,0:T(8,128)(2,1)S(1)}, u32[]{:S(2)}, u32[]{:S(2)}) collective-permute-start(bf16[128,2048]{1,0:T(8,128)(2,1)S(1)} %slice.154), channel_id=1, source_target_pairs={{0,3},{1,2},{2,1},{3,0},{4,7},{5,6},{6,5},{7,4},{8,11},{9,10},{10,... | collective-permute-start | bytes 1572872 | tf_op jit(solution)/shard_map/ppermute | solution.py:33
  175.9 3.2 %copy-start.2 = (f32[128,2048]{1,0:T(8,128)}, f32[128,2048]{1,0:T(8,128)S(1)}, u32[]{:S(2)}) copy-start(f32[128,2048]{1,0:T(8,128)S(1)} %slice_add_fusion) | copy-start | bytes 3145732
  195.6 0.8 copy-start.14

commit v6 on v5

--- a/solution.py
+++ b/solution.py
@@ -188,6 +188,7 @@
     count = len(refs) - 4
     sources, (out_ref, rows, held, sems) = refs[:count], refs[count:]
     units = held.shape[2] // 2
+    row_block = rows.shape[0] // (2 if held.shape[0] > 1 else 1)
     copies = [pltpu.make_async_copy(rows_ref, rows, sems.at[count])]
     for at, source in enumerate(sources):
         place = held.at[at // 2, :, pl.ds(at % 2 * units, units)]
@@ -198,12 +199,18 @@
     for index in range(held.shape[0]):
         copies[1 + 2 * index].wait()
         copies[2 + 2 * index].wait()
-        both_values = jnp.dot(rows[...], held[index], preferred_element_type=jnp.float32)
-        gate = both_values[:, :units]
-        up = both_values[:, units:]
-        out_ref[:, index * units : (index + 1) * units] = (
-            gate / (1.0 + jnp.exp(-gate)) * up
-        ).astype(jnp.bfloat16)
+
+        def block(step, carry, index=index):
+            part = pl.ds(step * row_block, row_block)
+            both_values = jnp.dot(rows[part, :], held[index], preferred_element_type=jnp.float32)
+            gate = both_values[:, :units]
+            up = both_values[:, units:]
+            out_ref[part, index * units : (index + 1) * units] = (
+                gate / (1.0 + jnp.exp(-gate)) * up
+            ).astype(jnp.bfloat16)
+            return carry
+
+        lax.fori_loop(0, rows.shape[0] // row_block, block, 0)
 
 
 def expert_hidden(rows, pairs):

time: 197 us -> 198 us (level)
  no operation moved by 1% of the time
where the time goes in v6:
time: 198 us; the launch traced here: 197 us
  waiting for transfers between devices  74.1 us (37%)
  starting transfers between devices  60.8 us (31%)
  Pallas kernels  23.5 us (12%)
  matrix products  18.4 us (9%)
  other arithmetic  10.1 us (5%)
  local copies, waits for them, and re-layouts  8.85 us (4%)
    ppermute x16, waiting for transfers between devices, shifted(): lax.ppermute(value, 'tp', [(at, (at + steps) % count) for at in range(cou...  37.1 us
    all_to_all x3, starting transfers between devices, exchanged(): lax.all_to_all(rows.reshape(experts, slots // experts, width), 'ep', spli...  30.2 us
    all_to_all x3, waiting for transfers between devices, exchanged(): lax.all_to_all(rows.reshape(experts, slots // experts, width), 'ep', spli...  25.7 us
    ppermute x16, starting transfers between devices, shifted(): lax.ppermute(value, 'tp', [(at, (at + steps) % count) for at in range(cou...  24.6 us
    pallas_call x2, Pallas kernels, expert_hidden(): pl.pallas_call(hidden_body, grid=(1,), in_specs=[pl.BlockSpec(memory_spac...  11.7 us
    ppermute x4, waiting for transfers between devices, crossed(): lax.ppermute(value, 'tp', [(at, at ^ mask) for at in range(lax.axis_size(...  11.2 us
    pallas_call x2, Pallas kernels, expert_result(): pl.pallas_call(down_kernel([len(pieces) for pieces in matrices]), grid=(s...  8.46 us
    dot_general x4, matrix products, product(): jnp.dot(joined, weight, preferred_element_type=jnp.float32)  6.48 us
  transfers between devices with their start and end apart: 24, of which 8 were waited for; matrix products, arithmetic and copies ran while one was open for 18% of the time, Pallas kernels for 12%

profile of v6, /device:TPU:2, one launch (start us, length us, event | category | flops | bytes accessed | tf_op | source)
XLA Modules:
  0.0 197.1 jit_solution(11116755630745983991)
XLA Ops:
  0.6 3.1 %collective-permute-start.4 = (bf16[2048,256]{1,0:T(8,128)(2,1)}, bf16[2048,256]{1,0:T(8,128)(2,1)}, u32[]{:S(2)}, u32[]{:S(2)}) collective-permute-start(bf16[2048,256]{1,0:T(8,128)(2,1)} %bitcast.132), channel_id=1, source_target_pairs={{0,3},{1,0},{2,1},{3,2},{4,7},{5,4},{6,5},{7,6},{8,11},{9,8},{10,9... | collective-permute-start | bytes 3145736 | tf_op jit(solution)/shard_map/ppermute | solution.py:29
  3.7 0.6 collective-permute-start.1
  4.3 2.7 %collective-permute-start.3 = (bf16[2048,256]{1,0:T(8,128)(2,1)}, bf16[2048,256]{1,0:T(8,128)(2,1)}, u32[]{:S(2)}, u32[]{:S(2)}) collective-permute-start(bf16[2048,256]{1,0:T(8,128)(2,1)} %bitcast.130), channel_id=1, source_target_pairs={{0,3},{1,0},{2,1},{3,2},{4,7},{5,4},{6,5},{7,6},{8,11},{9,8},{10,9... | collective-permute-start | bytes 3145736 | tf_op jit(solution)/shard_map/ppermute | solution.py:29
  7.0 3.3 %dispatch.1 = (bf16[512,2048]{1,0:T(8,128)(2,1)}, bf16[2,512,128]{2,1,0:T(8,128)(2,1)}) custom-call(s32[1]{0:T(128)} %bitcast.3.rank_ref, bf16[512,2048]{1,0:T(8,128)(2,1)} %rows_ref.1, f32[1,2048]{1,0:T(1,128)} %bitcast.141, s32[2,512]{1,0:T(2,128)} %bitcast.142), custom_call_target="tpu_custom_call" | custom-call | tf_op jit(solution)/shard_map/dispatch/pallas_call | solution.py:164
  10.3 12.2 %all-to-all-start = ((bf16[64,8,2048]{2,1,0:T(8,128)(2,1)}), bf16[64,8,2048]{2,1,0:T(8,128)(2,1)}, u32[]{:S(2)}, u32[]{:S(2)}) async-start(bf16[64,8,2048]{2,1,0:T(8,128)(2,1)} %bitcast.126), calls=%async_computation | async-start | bytes 4194304 | tf_op jit(solution)/shard_map/all_to_all | solution.py:38
  22.5 1.0 slice.108.refs_0_
  23.6 2.1 %collective-permute-start.8 = (bf16[256,768]{1,0:T(8,128)(2,1)S(1)}, bf16[256,768]{1,0:T(8,128)(2,1)}, u32[]{:S(2)}, u32[]{:S(2)}) collective-permute-start(bf16[256,768]{1,0:T(8,128)(2,1)S(1)} %slice.108.refs_0_), channel_id=1, source_target_pairs={{0,3},{1,0},{2,1},{3,2},{4,7},{5,4},{6,5},{7,6},{8,11},{9,8},{10,9... | collective-permute-start | bytes 1179656 | tf_op jit(solution)/shard_map/ppermute | solution.py:29
  25.7 2.1 %fusion.3 = f32[512]{0:T(512)S(1)} fusion(bf16[512,2048]{1,0:T(8,128)(2,1)} %rows_ref.1), kind=kLoop, calls=%fused_computation.7 | loop fusion | flops 3145216 | bytes 2099200 | tf_op jit(solution)/shard_map/reduce_sum | solution.py:70
  27.8 2.2 %fusion = f32[512]{0:T(512)S(1)} fusion(bf16[512,2048]{1,0:T(8,128)(2,1)} %param.17), kind=kLoop, calls=%fused_computation.4 | loop fusion | flops 3145216 | bytes 2099200 | tf_op jit(solution)/shard_map/reduce_sum | solution.py:70
  30.1 2.7 %convolution_convert_fusion.4 = bf16[512,384]{0,1:T(8,128)(2,1)S(1)} fusion(bf16[2048,384]{1,0:T(8,128)(2,1)} %param.21, bf16[512,2048]{1,0:T(8,128)(2,1)S(1)} %copy-done.4, f32[2048]{0:T(1024)S(1)} %copy-done.31, f32[512]{0:T(512)S(1)} %add_rsqrt_fusion.1), kind=kOutput, calls=%fused_computation.27 | convolution fusion | flops 809697280 | bytes 4073472 | tf_op jit(solution)/shard_map/dot_general | solution.py:329
  32.9 2.5 %fusion.28 = f32[512,128]{1,0:T(8,128)S(1)} fusion(bf16[2048,128]{1,0:T(8,128)(2,1)S(1)} %copy-done.27, bf16[512,2048]{1,0:T(8,128)(2,1)} %rows_ref.1, f32[2048]{0:T(1024)S(1)} %copy-done.25, f32[512]{0:T(512)S(1)} %add_rsqrt_fusion), kind=kOutput, calls=%fused_computation.45 | convolution fusion | flops 272629760 | bytes 2893824 | tf_op jit(solution)/shard_map/dot_general | solution.py:346
  35.5 0.8 fusion.20
  36.4 0.3 multiply_cosine_fusion
  36.7 0.1 fusion.36
  36.8 0.8 copy_bitcast_fusion.1
  37.6 1.4 convolution_convert_fusion.2
  39.2 0.8 convolution_convert_fusion.5
  40.1 0.3 copy-done.30
  40.4 0.8 fusion.22
  41.2 11.1 %collective-permute-done.1.refs_2_ = bf16[2048,256]{1,0:T(8,128)(2,1)} collective-permute-done((bf16[2048,256]{1,0:T(8,128)(2,1)}, bf16[2048,256]{1,0:T(8,128)(2,1)}, u32[]{:S(2)}, u32[]{:S(2)}) %collective-permute-start.1) | collective-permute-done | bytes 1048608 | tf_op jit(solution)/shard_map/ppermute | solution.py:29
  52.4 0.9 broadcast_and_fusion
  53.2 3.2 %collective-permute-start.6 = (bf16[2048,256]{1,0:T(8,128)(2,1)}, bf16[2048,256]{1,0:T(8,128)(2,1)S(1)}, u32[]{:S(2)}, u32[]{:S(2)}) collective-permute-start(bf16[2048,256]{1,0:T(8,128)(2,1)} %collective-permute-done.4.refs_5_), channel_id=1, source_target_pairs={{0,3},{1,0},{2,1},{3,2},{4,7},{5,4},{6,5},{7,6},{8,11},{9,8},{10,9... | collective-permute-start | bytes 3145736 | tf_op jit(solution)/shard_map/ppermute | solution.py:29
  56.5 0.3 fusion.60
  56.8 1.6 collective-permute-done.8.refs_2_
  58.4 1.1 collective-permute-start.7
  59.5 0.6 copy_bitcast_fusion.5
  60.2 1.4 convolution_convert_fusion.3
  61.6 24.4 %collective-permute-done.7.refs_1_ = bf16[256,768]{1,0:T(8,128)(2,1)S(1)} collective-permute-done((bf16[256,768]{1,0:T(8,128)(2,1)S(1)}, bf16[256,768]{1,0:T(8,128)(2,1)S(1)}, u32[]{:S(2)}, u32[]{:S(2)}) %collective-permute-start.7) | collective-permute-done | bytes 393248 | tf_op jit(solution)/shard_map/ppermute | solution.py:29
  86.0 3.2 %collective-permute-start.16 = (bf16[256,640]{1,0:T(8,128)(2,1)S(1)}, bf16[256,640]{1,0:T(8,128)(2,1)}, u32[]{:S(2)}, u32[]{:S(2)}) collective-permute-start(bf16[256,640]{1,0:T(8,128)(2,1)S(1)} %get-tuple-element.18.refs_1_), channel_id=1, source_target_pairs={{0,3},{1,0},{2,1},{3,2},{4,7},{5,4},{6,5},{7,6},{8,11},{9,8},{10,9... | collective-permute-start | bytes 983048 | tf_op jit(solution)/shard_map/ppermute | solution.py:29
  89.2 1.6 slice.110
  90.8 0.7 slice.109
  91.6 2.0 %collective-permute-start.9 = (bf16[256,384]{1,0:T(8,128)(2,1)}, bf16[256,384]{1,0:T(8,128)(2,1)}, u32[]{:S(2)}, u32[]{:S(2)}) collective-permute-start(bf16[256,384]{1,0:T(8,128)(2,1)} %slice.109), channel_id=1, source_target_pairs={{0,1},{1,2},{2,3},{3,0},{4,5},{5,6},{6,7},{7,4},{8,9},{9,10},{10,1... | collective-permute-start | bytes 589832 | tf_op jit(solution)/shard_map/ppermute | solution.py:29
  93.6 0.7 fusion.78
  94.3 1.9 collective-permute-start
  96.3 0.6 copy.26
  97.0 7.5 %shard_map.176.near_ref = bf16[512,768]{1,0:T(8,128)(2,1)} custom-call(bf16[512,2048]{1,0:T(8,128)(2,1)} %bitcast.7.rows_ref, bf16[2048,256]{1,0:T(8,128)(2,1)} %bitcast.131, bf16[2048,256]{1,0:T(8,128)(2,1)} %bitcast.134, bf16[2048,256]{1,0:T(8,128)(2,1)} %collective-permute-done.1.refs_2_, bf16[2048,256]{1,0:T(8,128)(2,1)} %collective-permute-done.2.refs_3_, ...), custom_call_target="tpu_custom_call" | custom-call | tf_op jit(solution)/shard_map/pallas_call | solution.py:220
  104.5 4.2 %shard_map.177.far_ref = bf16[512,256]{1,0:T(8,128)(2,1)} custom-call(bf16[512,2048]{1,0:T(8,128)(2,1)} %bitcast.7.rows_ref, bf16[2048,256]{1,0:T(8,128)(2,1)} %copy-done.9, bf16[2048,256]{1,0:T(8,128)(2,1)} %copy-done.10), custom_call_target="tpu_custom_call" | custom-call | tf_op jit(solution)/shard_map/pallas_call | solution.py:220
  108.7 0.1 collective-permute-start.14
  108.9 3.2 %collective-permute-start.15 = (bf16[256,640]{1,0:T(8,128)(2,1)S(1)}, bf16[256,640]{1,0:T(8,128)(2,1)}, u32[]{:S(2)}, u32[]{:S(2)}) collective-permute-start(bf16[256,640]{1,0:T(8,128)(2,1)S(1)} %get-tuple-element.19.refs_0_), channel_id=1, source_target_pairs={{0,3},{1,0},{2,1},{3,2},{4,7},{5,4},{6,5},{7,6},{8,11},{9,8},{10,9... | collective-permute-start | bytes 983048 | tf_op jit(solution)/shard_map/ppermute | solution.py:29
  112.1 3.2 %collective-permute-start.18 = (bf16[256,640]{1,0:T(8,128)(2,1)}, bf16[256,640]{1,0:T(8,128)(2,1)}, u32[]{:S(2)}, u32[]{:S(2)}) collective-permute-start(bf16[256,640]{1,0:T(8,128)(2,1)} %collective-permute-done.16.refs_5_), channel_id=1, source_target_pairs={{0,3},{1,0},{2,1},{3,2},{4,7},{5,4},{6,5},{7,6},{8,11},{9,8},{10,9... | collective-permute-start | bytes 983048 | tf_op jit(solution)/shard_map/ppermute | solution.py:29
  115.3 3.7 %down.2 = bf16[512,768]{1,0:T(8,128)(2,1)} custom-call(bf16[512,768]{1,0:T(8,128)(2,1)} %shard_map.176.near_ref, bf16[512,256]{1,0:T(8,128)(2,1)} %shard_map.177.far_ref, bf16[256,768]{1,0:T(8,128)(2,1)} %copy-done.6, bf16[256,768]{1,0:T(8,128)(2,1)} %copy-done.12, bf16[256,768]{1,0:T(8,128)(2,1)} %collective-permute-done.8.refs_2_, ...), custom_call_target="tpu_custom_call" | custom-call | tf_op jit(solution)/shard_map/down/pallas_call | solution.py:265
  119.0 12.2 %all-to-all-start.1 = ((bf16[64,8,768]{2,1,0:T(8,128)(2,1)}), bf16[64,8,768]{2,1,0:T(8,128)(2,1)S(1)}, u32[]{:S(2)}, u32[]{:S(2)}) async-start(bf16[64,8,768]{2,1,0:T(8,128)(2,1)} %bitcast.125), calls=%async_computation.1 | async-start | bytes 1572864 | tf_op jit(solution)/shard_map/all_to_all | solution.py:38
  131.3 0.2 collective-permute-start.19
  131.6 1.7 fusion.8
  133.4 0.7 fusion.6
  134.1 1.0 fusion.17
  135.1 0.3 copy.33
  135.5 0.8 constant_dynamic-slice_fusion.4
  136.2 1.7 convolution_convert_fusion
  138.0 4.7 %down.3 = bf16[512,1280]{1,0:T(8,128)(2,1)} custom-call(bf16[512,768]{1,0:T(8,128)(2,1)} %shard_map.176.near_ref, bf16[512,256]{1,0:T(8,128)(2,1)} %shard_map.177.far_ref, bf16[256,640]{1,0:T(8,128)(2,1)} %copy-done.8, bf16[256,640]{1,0:T(8,128)(2,1)} %copy-done.7, bf16[256,640]{1,0:T(8,128)(2,1)} %collective-permute-done.13.refs_2_, ...), custom_call_target="tpu_custom_call" | custom-call | tf_op jit(solution)/shard_map/down/pallas_call | solution.py:265
  142.7 11.7 %all-to-all-done.1 = bf16[64,8,768]{2,1,0:T(8,128)(2,1)S(1)} async-done(((bf16[64,8,768]{2,1,0:T(8,128)(2,1)}), bf16[64,8,768]{2,1,0:T(8,128)(2,1)S(1)}, u32[]{:S(2)}, u32[]{:S(2)}) %all-to-all-start.1) | async-done | bytes 786464 | tf_op jit(solution)/shard_map/all_to_all | solution.py:38
  154.4 0.3 fusion.24
  154.7 5.8 %all-to-all-start.2 = ((bf16[64,8,1280]{2,1,0:T(8,128)(2,1)}), bf16[64,8,1280]{2,1,0:T(8,128)(2,1)S(1)}, u32[]{:S(2)}, u32[]{:S(2)}) async-start(bf16[64,8,1280]{2,1,0:T(8,128)(2,1)} %bitcast.124), calls=%async_computation.2 | async-start | bytes 2621440 | tf_op jit(solution)/shard_map/all_to_all | solution.py:38
  160.5 1.9 convert_add_fusion
  162.7 0.7 collective-permute-done.11
  163.4 2.0 convert_add_fusion.1
  165.4 3.8 %collective-permute-start.12 = (bf16[128,2048]{1,0:T(8,128)(2,1)S(1)}, bf16[128,2048]{1,0:T(8,128)(2,1)S(1)}, u32[]{:S(2)}, u32[]{:S(2)}) collective-permute-start(bf16[128,2048]{1,0:T(8,128)(2,1)S(1)} %slice.154), channel_id=1, source_target_pairs={{0,3},{1,2},{2,1},{3,0},{4,7},{5,6},{6,5},{7,4},{8,11},{9,10},{10,... | collective-permute-start | bytes 1572872 | tf_op jit(solution)/shard_map/ppermute | solution.py:33
  169.2 7.4 %collective-permute-done.20 = bf16[128,2048]{1,0:T(8,128)(2,1)S(1)} collective-permute-done((bf16[128,2048]{1,0:T(8,128)(2,1)S(1)}, bf16[128,2048]{1,0:T(8,128)(2,1)S(1)}, u32[]{:S(2)}, u32[]{:S(2)}) %collective-permute-start.20) | collective-permute-done | bytes 524320 | tf_op jit(solution)/shard_map/ppermute | solution.py:33
  176.6 0.1 slice_add_fusion
  176.8 3.1 %collective-permute-done.12 = bf16[128,2048]{1,0:T(8,128)(2,1)S(1)} collective-permute-done((bf16[128,2048]{1,0:T(8,128)(2,1)S(1)}, bf16[128,2048]{1,0:T(8,128)(2,1)S(1)}, u32[]{:S(2)}, u32[]{:S(2)}) %collective-permute-start.12) | collective-permute-done | bytes 524320 | tf_op jit(solution)/shard_map/ppermute | solution.py:33
  180.0 0.9 fusion.23
  180.9 14.0 %all-to-all-done.2 = bf16[64,8,1280]{2,1,0:T(8,128)(2,1)S(1)} async-done(((bf16[64,8,1280]{2,1,0:T(8,128)(2,1)}), bf16[64,8,1280]{2,1,0:T(8,128)(2,1)S(1)}, u32[]{:S(2)}, u32[]{:S(2)}) %all-to-all-start.2) | async-done | bytes 1310752 | tf_op jit(solution)/shard_map/all_to_all | solution.py:38
  194.9 1.5 fusion.35
  196.4 0.8 copy-done.14
  (112 shorter events, 1.2 us)
Async XLA Ops:
  0.6 135.6 %copy-start = (bf16[384,2048]{1,0:T(8,128)(2,1)S(1)}, bf16[384,2048]{1,0:T(8,128)(2,1)}, u32[]{:S(2)}) copy-start(bf16[384,2048]{1,0:T(8,128)(2,1)} %param.25) | copy-start | bytes 4718596
  0.6 52.6 %collective-permute-start.4 = (bf16[2048,256]{1,0:T(8,128)(2,1)}, bf16[2048,256]{1,0:T(8,128)(2,1)}, u32[]{:S(2)}, u32[]{:S(2)}) collective-permute-start(bf16[2048,256]{1,0:T(8,128)(2,1)} %bitcast.132), channel_id=1, source_target_pairs={{0,3},{1,0},{2,1},{3,2},{4,7},{5,4},{6,5},{7,6},{8,11},{9,8},{10,9... | collective-permute-start | bytes 3145736 | tf_op jit(solution)/shard_map/ppermute | solution.py:29
  3.7 82.2 %collective-permute-start.2 = (bf16[2048,256]{1,0:T(8,128)(2,1)}, bf16[2048,256]{1,0:T(8,128)(2,1)}, u32[]{:S(2)}, u32[]{:S(2)}) collective-permute-start(bf16[2048,256]{1,0:T(8,128)(2,1)} %bitcast.133), channel_id=1, source_target_pairs={{0,1},{1,2},{2,3},{3,0},{4,5},{5,6},{6,7},{7,4},{8,9},{9,10},{10,1... | collective-permute-start | bytes 3145736 | tf_op jit(solution)/shard_map/ppermute | solution.py:29
  3.7 48.6 %collective-permute-start.1 = (bf16[2048,256]{1,0:T(8,128)(2,1)}, bf16[2048,256]{1,0:T(8,128)(2,1)}, u32[]{:S(2)}, u32[]{:S(2)}) collective-permute-start(bf16[2048,256]{1,0:T(8,128)(2,1)} %bitcast.129), channel_id=1, source_target_pairs={{0,1},{1,2},{2,3},{3,0},{4,5},{5,6},{6,7},{7,4},{8,9},{9,10},{10,1... | collective-permute-start | bytes 3145736 | tf_op jit(solution)/shard_map/ppermute | solution.py:29
  4.3 87.2 %collective-permute-start.3 = (bf16[2048,256]{1,0:T(8,128)(2,1)}, bf16[2048,256]{1,0:T(8,128)(2,1)}, u32[]{:S(2)}, u32[]{:S(2)}) collective-permute-start(bf16[2048,256]{1,0:T(8,128)(2,1)} %bitcast.130), channel_id=1, source_target_pairs={{0,3},{1,0},{2,1},{3,2},{4,7},{5,4},{6,5},{7,6},{8,11},{9,8},{10,9... | collective-permute-start | bytes 3145736 | tf_op jit(solution)/shard_map/ppermute | solution.py:29
  10.3 86.6 %all-to-all-start = ((bf16[64,8,2048]{2,1,0:T(8,128)(2,1)}), bf16[64,8,2048]{2,1,0:T(8,128)(2,1)}, u32[]{:S(2)}, u32[]{:S(2)}) async-start(bf16[64,8,2048]{2,1,0:T(8,128)(2,1)} %bitcast.126), calls=%async_computation | async-start | bytes 4194304 | tf_op jit(solution)/shard_map/all_to_all | solution.py:38
  23.6 34.8 %copy-start.6 = (bf16[256,768]{1,0:T(8,128)(2,1)}, bf16[256,768]{1,0:T(8,128)(2,1)S(1)}, u32[]{:S(2)}) copy-start(bf16[256,768]{1,0:T(8,128)(2,1)S(1)} %slice.108.refs_0_) | copy-start | bytes 1179652
  23.6 34.8 %collective-permute-start.8 = (bf16[256,768]{1,0:T(8,128)(2,1)S(1)}, bf16[256,768]{1,0:T(8,128)(2,1)}, u32[]{:S(2)}, u32[]{:S(2)}) collective-permute-start(bf16[256,768]{1,0:T(8,128)(2,1)S(1)} %slice.108.refs_0_), channel_id=1, source_target_pairs={{0,3},{1,0},{2,1},{3,2},{4,7},{5,4},{6,5},{7,6},{8,11},{9,8},{10,9... | collective-permute-start | bytes 1179656 | tf_op jit(solution)/shard_map/ppermute | solution.py:29
  25.7 4.4 %copy-start.31 = (f32[2048]{0:T(1024)S(1)}, f32[2048]{0:T(1024)}, u32[]{:S(2)}) copy-start(f32[2048]{0:T(1024)} %param.19) | copy-start | bytes 24580
  27.8 2.3 %copy-start.4 = (bf16[512,2048]{1,0:T(8,128)(2,1)S(1)}, bf16[512,2048]{1,0:T(8,128)(2,1)}, u32[]{:S(2)}) copy-start(bf16[512,2048]{1,0:T(8,128)(2,1)} %param.17) | copy-start | bytes 6291460
  30.1 2.8 %copy-start.25 = (f32[2048]{0:T(1024)S(1)}, f32[2048]{0:T(1024)}, u32[]{:S(2)}) copy-start(f32[2048]{0:T(1024)} %param.20) | copy-start | bytes 24580
  30.1 2.8 %copy-start.27 = (bf16[2048,128]{1,0:T(8,128)(2,1)S(1)}, bf16[2048,128]{1,0:T(8,128)(2,1)}, u32[]{:S(2)}) copy-start(bf16[2048,128]{1,0:T(8,128)(2,1)} %param.31) | copy-start | bytes 1572868
  32.9 2.5 %copy-start.1 = (bf16[512,2048]{1,0:T(8,128)(2,1)S(1)}, bf16[512,2048]{1,0:T(8,128)(2,1)}, u32[]{:S(2)}) copy-start(bf16[512,2048]{1,0:T(8,128)(2,1)} %rows_ref.1) | copy-start | bytes 6291460
  32.9 2.5 %copy-start.28 = (bf16[2048,128]{1,0:T(8,128)(2,1)S(1)}, bf16[2048,128]{1,0:T(8,128)(2,1)}, u32[]{:S(2)}) copy-start(bf16[2048,128]{1,0:T(8,128)(2,1)} %param.32) | copy-start | bytes 1572868
  36.2 1.4 copy-start.3
  36.2 2.9 %copy-start.11 = (bf16[1,256,2048]{2,1,0:T(8,128)(2,1)S(1)}, bf16[1,256,2048]{2,1,0:T(8,128)(2,1)}, u32[]{:S(2)}) copy-start(bf16[1,256,2048]{2,1,0:T(8,128)(2,1)} %param.30) | copy-start | bytes 3145732
  36.8 2.4 %copy-start.5 = (bf16[512,2048]{1,0:T(8,128)(2,1)S(1)}, bf16[512,2048]{1,0:T(8,128)(2,1)}, u32[]{:S(2)}) copy-start(bf16[512,2048]{1,0:T(8,128)(2,1)} %param.17) | copy-start | bytes 6291460
  36.8 2.4 %copy-start.29 = (bf16[2048,64]{0,1:T(8,128)(2,1)S(1)}, bf16[2048,64]{0,1:T(8,128)(2,1)}, u32[]{:S(2)}) copy-start(bf16[2048,64]{0,1:T(8,128)(2,1)} %param.23) | copy-start | bytes 786436
  39.2 69.5 %copy-start.7 = (bf16[256,640]{1,0:T(8,128)(2,1)}, bf16[256,640]{1,0:T(8,128)(2,1)S(1)}, u32[]{:S(2)}) copy-start(bf16[256,640]{1,0:T(8,128)(2,1)S(1)} %get-tuple-element.18.refs_1_) | copy-start | bytes 983044
  39.2 69.6 %copy-start.8 = (bf16[256,640]{1,0:T(8,128)(2,1)}, bf16[256,640]{1,0:T(8,128)(2,1)S(1)}, u32[]{:S(2)}) copy-start(bf16[256,640]{1,0:T(8,128)(2,1)S(1)} %get-tuple-element.19.refs_0_) | copy-start | bytes 983044
  39.2 1.2 copy-start.30
  40.4 55.9 %copy-start.21 = (bf16[512,64]{0,1:T(8,128)(2,1)}, bf16[512,64]{0,1:T(8,128)(2,1)S(1)}, u32[]{:S(2)}) copy-start(bf16[512,64]{0,1:T(8,128)(2,1)S(1)} %convolution_convert_fusion.5) | copy-start | bytes 196612
  41.2 55.0 %copy-start.23 = (bf16[2,512,128]{2,1,0:T(8,128)(2,1)S(1)}, bf16[2,512,128]{2,1,0:T(8,128)(2,1)}, u32[]{:S(2)}) copy-start(bf16[2,512,128]{2,1,0:T(8,128)(2,1)} %get-tuple-element.13) | copy-start | bytes 786436
  52.4 39.2 %collective-permute-start.5 = (bf16[2048,256]{1,0:T(8,128)(2,1)}, bf16[2048,256]{1,0:T(8,128)(2,1)S(1)}, u32[]{:S(2)}, u32[]{:S(2)}) collective-permute-start(bf16[2048,256]{1,0:T(8,128)(2,1)} %collective-permute-done.1.refs_2_), channel_id=1, source_target_pairs={{0,1},{1,2},{2,3},{3,0},{4,5},{5,6},{6,7},{7,4},{8,9},{9,10},{10,1... | collective-permute-start | bytes 3145736 | tf_op jit(solution)/shard_map/ppermute | solution.py:29
  53.2 41.0 %collective-permute-start.6 = (bf16[2048,256]{1,0:T(8,128)(2,1)}, bf16[2048,256]{1,0:T(8,128)(2,1)S(1)}, u32[]{:S(2)}, u32[]{:S(2)}) collective-permute-start(bf16[2048,256]{1,0:T(8,128)(2,1)} %collective-permute-done.4.refs_5_), channel_id=1, source_target_pairs={{0,3},{1,0},{2,1},{3,2},{4,7},{5,4},{6,5},{7,6},{8,11},{9,8},{10,9... | collective-permute-start | bytes 3145736 | tf_op jit(solution)/shard_map/ppermute | solution.py:29
  56.8 47.7 %copy-start.15 = (bf16[512,1,32]{0,2,1:T(8,128)(2,1)}, bf16[512,1,32]{0,2,1:T(8,128)(2,1)S(1)}, u32[]{:S(2)}) copy-start(bf16[512,1,32]{0,2,1:T(8,128)(2,1)S(1)} %get-tuple-element.26) | copy-start | bytes 98308
  56.8 47.7 %copy-start.17 = (bf16[512,1,32]{0,2,1:T(8,128)(2,1)}, bf16[512,1,32]{0,2,1:T(8,128)(2,1)S(1)}, u32[]{:S(2)}) copy-start(bf16[512,1,32]{0,2,1:T(8,128)(2,1)S(1)} %get-tuple-element.27) | copy-start | bytes 98308
  58.4 27.6 %collective-permute-start.7 = (bf16[256,768]{1,0:T(8,128)(2,1)S(1)}, bf16[256,768]{1,0:T(8,128)(2,1)S(1)}, u32[]{:S(2)}, u32[]{:S(2)}) collective-permute-start(bf16[256,768]{1,0:T(8,128)(2,1)S(1)} %slice.108.refs_0_), channel_id=1, source_target_pairs={{0,1},{1,2},{2,3},{3,0},{4,5},{5,6},{6,7},{7,4},{8,9},{9,10},{10,1... | collective-permute-start | bytes 1179656 | tf_op jit(solution)/shard_map/ppermute | solution.py:29
  86.0 18.5 %copy-start.12 = (bf16[256,768]{1,0:T(8,128)(2,1)}, bf16[256,768]{1,0:T(8,128)(2,1)S(1)}, u32[]{:S(2)}) copy-start(bf16[256,768]{1,0:T(8,128)(2,1)S(1)} %collective-permute-done.7.refs_1_) | copy-start | bytes 1179652
  86.0 22.8 %collective-permute-start.13 = (bf16[256,640]{1,0:T(8,128)(2,1)S(1)}, bf16[256,640]{1,0:T(8,128)(2,1)}, u32[]{:S(2)}, u32[]{:S(2)}) collective-permute-start(bf16[256,640]{1,0:T(8,128)(2,1)S(1)} %get-tuple-element.19.refs_0_), channel_id=1, source_target_pairs={{0,1},{1,2},{2,3},{3,0},{4,5},{5,6},{6,7},{7,4},{8,9},{9,10},{10,1... | collective-permute-start | bytes 983048 | tf_op jit(solution)/shard_map/ppermute | solution.py:29
  86.0 22.9 %collective-permute-start.16 = (bf16[256,640]{1,0:T(8,128)(2,1)S(1)}, bf16[256,640]{1,0:T(8,128)(2,1)}, u32[]{:S(2)}, u32[]{:S(2)}) collective-permute-start(bf16[256,640]{1,0:T(8,128)(2,1)S(1)} %get-tuple-element.18.refs_1_), channel_id=1, source_target_pairs={{0,3},{1,0},{2,1},{3,2},{4,7},{5,4},{6,5},{7,6},{8,11},{9,8},{10,9... | collective-permute-start | bytes 983048 | tf_op jit(solution)/shard_map/ppermute | solution.py:29
  91.6 20.5 %collective-permute-start.10 = (bf16[256,384]{1,0:T(8,128)(2,1)}, bf16[256,384]{1,0:T(8,128)(2,1)}, u32[]{:S(2)}, u32[]{:S(2)}) collective-permute-start(bf16[256,384]{1,0:T(8,128)(2,1)} %slice.110), channel_id=1, source_target_pairs={{0,3},{1,0},{2,1},{3,2},{4,7},{5,4},{6,5},{7,6},{8,11},{9,8},{10,9... | collective-permute-start | bytes 589832 | tf_op jit(solution)/shard_map/ppermute | solution.py:29
  91.6 4.6 %copy-start.9 = (bf16[2048,256]{1,0:T(8,128)(2,1)}, bf16[2048,256]{1,0:T(8,128)(2,1)S(1)}, u32[]{:S(2)}) copy-start(bf16[2048,256]{1,0:T(8,128)(2,1)S(1)} %collective-permute-done.5.refs_0_) | copy-start | bytes 3145732
  91.6 20.5 %collective-permute-start.9 = (bf16[256,384]{1,0:T(8,128)(2,1)}, bf16[256,384]{1,0:T(8,128)(2,1)}, u32[]{:S(2)}, u32[]{:S(2)}) collective-permute-start(bf16[256,384]{1,0:T(8,128)(2,1)} %slice.109), channel_id=1, source_target_pairs={{0,1},{1,2},{2,3},{3,0},{4,5},{5,6},{6,7},{7,4},{8,9},{9,10},{10,1... | collective-permute-start | bytes 589832 | tf_op jit(solution)/shard_map/ppermute | solution.py:29
  94.3 1.9 copy-start.10
  94.3 37.0 %collective-permute-start = (bf16[128,128]{0,1:T(8,128)(2,1)S(1)}, bf16[128,128]{0,1:T(8,128)(2,1)S(1)}, u32[]{:S(2)}, u32[]{:S(2)}) collective-permute-start(bf16[128,128]{0,1:T(8,128)(2,1)S(1)} %pad_maximum_fusion.3), channel_id=1, source_target_pairs={{0,4},{4,8},{8,12},{12,16},{16,20},{20,24},{24,28},{28,32},{32,36}... | collective-permute-start | bytes 98312 | tf_op jit(solution)/shard_map/ppermute | solution.py:24
  108.7 22.8 %copy-start.16 = (bf16[512,1,32]{0,2,1:T(8,128)(2,1)S(1)}, bf16[512,1,32]{0,2,1:T(8,128)(2,1)}, u32[]{:S(2)}) copy-start(bf16[512,1,32]{0,2,1:T(8,128)(2,1)} %copy-done.15) | copy-start | bytes 98308
  108.7 22.8 %copy-start.18 = (bf16[512,1,32]{0,2,1:T(8,128)(2,1)S(1)}, bf16[512,1,32]{0,2,1:T(8,128)(2,1)}, u32[]{:S(2)}) copy-start(bf16[512,1,32]{0,2,1:T(8,128)(2,1)} %copy-done.17) | copy-start | bytes 98308
  108.7 22.8 %copy-start.22 = (bf16[512,64]{0,1:T(8,128)(2,1)S(1)}, bf16[512,64]{0,1:T(8,128)(2,1)}, u32[]{:S(2)}) copy-start(bf16[512,64]{0,1:T(8,128)(2,1)} %copy-done.21) | copy-start | bytes 196612
  108.7 22.8 %copy-start.13 = (pred[4,128,256]{1,2,0:T(8,128)(4,1)S(1)}, pred[4,128,256]{1,2,0:T(8,128)(4,1)}, u32[]{:S(2)}) copy-start(pred[4,128,256]{1,2,0:T(8,128)(4,1)} %broadcast_and_fusion) | copy-start | bytes 393220
  108.7 29.2 %collective-permute-start.14 = (bf16[256,640]{1,0:T(8,128)(2,1)S(1)}, bf16[256,640]{1,0:T(8,128)(2,1)}, u32[]{:S(2)}, u32[]{:S(2)}) collective-permute-start(bf16[256,640]{1,0:T(8,128)(2,1)S(1)} %get-tuple-element.18.refs_1_), channel_id=1, source_target_pairs={{0,1},{1,2},{2,3},{3,0},{4,5},{5,6},{6,7},{7,4},{8,9},{9,10},{10,1... | collective-permute-start | bytes 983048 | tf_op jit(solution)/shard_map/ppermute | solution.py:29
  108.9 29.1 %collective-permute-start.15 = (bf16[256,640]{1,0:T(8,128)(2,1)S(1)}, bf16[256,640]{1,0:T(8,128)(2,1)}, u32[]{:S(2)}, u32[]{:S(2)}) collective-permute-start(bf16[256,640]{1,0:T(8,128)(2,1)S(1)} %get-tuple-element.19.refs_0_), channel_id=1, source_target_pairs={{0,3},{1,0},{2,1},{3,2},{4,7},{5,4},{6,5},{7,6},{8,11},{9,8},{10,9... | collective-permute-start | bytes 983048 | tf_op jit(solution)/shard_map/ppermute | solution.py:29
  112.1 25.9 %collective-permute-start.17 = (bf16[256,640]{1,0:T(8,128)(2,1)}, bf16[256,640]{1,0:T(8,128)(2,1)}, u32[]{:S(2)}, u32[]{:S(2)}) collective-permute-start(bf16[256,640]{1,0:T(8,128)(2,1)} %collective-permute-done.13.refs_2_), channel_id=1, source_target_pairs={{0,1},{1,2},{2,3},{3,0},{4,5},{5,6},{6,7},{7,4},{8,9},{9,10},{10,1... | collective-permute-start | bytes 983048 | tf_op jit(solution)/shard_map/ppermute | solution.py:29
  112.1 25.9 %collective-permute-start.18 = (bf16[256,640]{1,0:T(8,128)(2,1)}, bf16[256,640]{1,0:T(8,128)(2,1)}, u32[]{:S(2)}, u32[]{:S(2)}) collective-permute-start(bf16[256,640]{1,0:T(8,128)(2,1)} %collective-permute-done.16.refs_5_), channel_id=1, source_target_pairs={{0,3},{1,0},{2,1},{3,2},{4,7},{5,4},{6,5},{7,6},{8,11},{9,8},{10,9... | collective-permute-start | bytes 983048 | tf_op jit(solution)/shard_map/ppermute | solution.py:29
  119.0 35.4 %all-to-all-start.1 = ((bf16[64,8,768]{2,1,0:T(8,128)(2,1)}), bf16[64,8,768]{2,1,0:T(8,128)(2,1)S(1)}, u32[]{:S(2)}, u32[]{:S(2)}) async-start(bf16[64,8,768]{2,1,0:T(8,128)(2,1)} %bitcast.125), calls=%async_computation.1 | async-start | bytes 1572864 | tf_op jit(solution)/shard_map/all_to_all | solution.py:38
  131.3 29.2 %collective-permute-start.19 = (bf16[256,2048]{1,0:T(8,128)(2,1)}, bf16[256,2048]{1,0:T(8,128)(2,1)}, u32[]{:S(2)}, u32[]{:S(2)}) collective-permute-start(bf16[256,2048]{1,0:T(8,128)(2,1)} %convolution_convert_fusion.3), channel_id=1, source_target_pairs={{0,3},{1,2},{2,1},{3,0},{4,7},{5,6},{6,5},{7,4},{8,11},{9,10},{10,... | collective-permute-start | bytes 3145736 | tf_op jit(solution)/shard_map/ppermute | solution.py:33
  131.5 1.7 copy-start.26
  133.3 0.9 copy-start.24
  137.9 25.4 %collective-permute-start.11 = (bf16[256,2048]{1,0:T(8,128)(2,1)}, bf16[256,2048]{1,0:T(8,128)(2,1)}, u32[]{:S(2)}, u32[]{:S(2)}) collective-permute-start(bf16[256,2048]{1,0:T(8,128)(2,1)} %convolution_convert_fusion), channel_id=1, source_target_pairs={{0,1},{1,0},{2,3},{3,2},{4,5},{5,4},{6,7},{7,6},{8,9},{9,8},{10,11... | collective-permute-start | bytes 3145736 | tf_op jit(solution)/shard_map/ppermute | solution.py:33
  154.7 40.2 %all-to-all-start.2 = ((bf16[64,8,1280]{2,1,0:T(8,128)(2,1)}), bf16[64,8,1280]{2,1,0:T(8,128)(2,1)S(1)}, u32[]{:S(2)}, u32[]{:S(2)}) async-start(bf16[64,8,1280]{2,1,0:T(8,128)(2,1)} %bitcast.124), calls=%async_computation.2 | async-start | bytes 2621440 | tf_op jit(solution)/shard_map/all_to_all | solution.py:38
  160.5 2.9 %copy-start.19 = (bf16[128,384]{0,1:T(8,128)(2,1)S(1)}, bf16[128,384]{0,1:T(8,128)(2,1)}, u32[]{:S(2)}) copy-start(bf16[128,384]{0,1:T(8,128)(2,1)} %get-tuple-element.22) | copy-start | bytes 294916
  160.5 2.9 %copy-start.20 = (bf16[128,384]{0,1:T(8,128)(2,1)S(1)}, bf16[128,384]{0,1:T(8,128)(2,1)}, u32[]{:S(2)}) copy-start(bf16[128,384]{0,1:T(8,128)(2,1)} %get-tuple-element.25) | copy-start | bytes 294916
  162.6 14.0 %collective-permute-start.20 = (bf16[128,2048]{1,0:T(8,128)(2,1)S(1)}, bf16[128,2048]{1,0:T(8,128)(2,1)S(1)}, u32[]{:S(2)}, u32[]{:S(2)}) collective-permute-start(bf16[128,2048]{1,0:T(8,128)(2,1)S(1)} %slice.153), channel_id=1, source_target_pairs={{0,1},{1,0},{2,3},{3,2},{4,5},{5,4},{6,7},{7,6},{8,9},{9,8},{10,11... | collective-permute-start | bytes 1572872 | tf_op jit(solution)/shard_map/ppermute | solution.py:33
  165.4 14.5 %collective-permute-start.12 = (bf16[128,2048]{1,0:T(8,128)(2,1)S(1)}, bf16[128,2048]{1,0:T(8,128)(2,1)S(1)}, u32[]{:S(2)}, u32[]{:S(2)}) collective-permute-start(bf16[128,2048]{1,0:T(8,128)(2,1)S(1)} %slice.154), channel_id=1, source_target_pairs={{0,3},{1,2},{2,1},{3,0},{4,7},{5,6},{6,5},{7,4},{8,11},{9,10},{10,... | collective-permute-start | bytes 1572872 | tf_op jit(solution)/shard_map/ppermute | solution.py:33
  176.7 3.2 %copy-start.2 = (f32[128,2048]{1,0:T(8,128)}, f32[128,2048]{1,0:T(8,128)S(1)}, u32[]{:S(2)}) copy-start(f32[128,2048]{1,0:T(8,128)S(1)} %slice_add_fusion) | copy-start | bytes 3145732
  196.3 0.8 copy-start.14
